TPU v7x, 512 devices: a whole 4x4x16 slice. The times are simulated.
512 devices in a mesh: fs: 16 (over y, x), tp: 32 (over z, core).
Axes of the slice: x: 4, y: 4, z: 16, core: 2. Of those that a mesh axis runs over, the one named last changes fastest.
Arguments:
- saved_input: bfloat16 [16384, 4096], P('fs', 'tp'), may hold values from -6 to 6
- query_cot: bfloat16 [16384, 4096], P('fs', 'tp'), may hold values from -6 to 6
- key_cot: bfloat16 [16384, 4096], P('fs', 'tp'), may hold values from -6 to 6
- query_master: float32 [4096, 4096], P('fs', 'tp'), may hold values from -0.09375 to 0.09375
- key_master: float32 [4096, 4096], P('fs', 'tp'), may hold values from -0.09375 to 0.09375
- query_basis: bfloat16 [4096, 256], P('fs'), may hold values from -3 to 3
- key_basis: bfloat16 [4096, 256], P('fs'), may hold values from -3 to 3
- query_first: float32 [256, 4096], P('fs', 'tp'), may hold values from -240 to 240
- query_second: float32 [256, 4096], P('fs', 'tp'), may hold values from 1000 to 20000
- key_first: float32 [256, 4096], P('fs', 'tp'), may hold values from -240 to 240
- key_second: float32 [256, 4096], P('fs', 'tp'), may hold values from 1000 to 20000
Outputs:
- query_step: float32 [4096, 4096], P('fs', 'tp')
- query_weight: float32 [4096, 4096], P('fs', 'tp')
- query_copy: bfloat16 [4096, 4096], P(None, 'tp')
- query_first_new: float32 [256, 4096], P('fs', 'tp')
- query_second_new: float32 [256, 4096], P('fs', 'tp')
- key_step: float32 [4096, 4096], P('fs', 'tp')
- key_weight: float32 [4096, 4096], P('fs', 'tp')
- key_copy: bfloat16 [4096, 4096], P(None, 'tp')
- key_first_new: float32 [256, 4096], P('fs', 'tp')
- key_second_new: float32 [256, 4096], P('fs', 'tp')
All inputs are finite; a program needn't handle non-finite values.
Results may differ from a plain program's by a relative error of at most 0.0065.
Values may be sent and summed in bfloat16 or wider, within the bound.
No kernel may reach another device: no remote copies, remote signals or barrier semaphores. Data moves between devices by JAX's collectives and lax.ppermute only.
A program may use at most 64 MiB of HBM per device.

v0:
```python
import jax
import jax.numpy as jnp
from jax import lax
from jax.sharding import Mesh
from jax.sharding import PartitionSpec as P

D = 4096
HD = 128
FS = ("fs_0", "fs_1")


moment_decay = 0.8
square_decay = 0.9
square_floor = 1.0
norm_floor = 0.01
step_rate = 0.01


def in_one_piece(arrays, axis, dim, along):
    widths = [a.shape[along] for a in arrays]
    both = jnp.concatenate(arrays, axis=along)
    out = lax.all_gather(both, axis, axis=dim, tiled=True)
    return tuple(jnp.split(out, [sum(widths[:k]) for k in range(1, len(widths))], axis=along))


def cut_along(x, dim, count):
    lengths = x.shape
    pieces = x.reshape(*lengths[:dim], count, lengths[dim] // count, *lengths[dim + 1 :])
    return jnp.moveaxis(pieces, dim, 0)


def sent_and_summed(x, axis, dim):
    count = lax.axis_size(axis)
    pieces = lax.all_to_all(cut_along(x, dim, count), axis, 0, 0, tiled=True)
    return jnp.sum(pieces, axis=0)


def sent_to_all(x, axis):
    count = lax.axis_size(axis)
    return lax.all_to_all(jnp.broadcast_to(x[None], (count, *x.shape)), axis, 0, 0, tiled=True)


def in_order(pieces, dim):
    lengths = list(pieces.shape[1:])
    lengths[dim] *= pieces.shape[0]
    return jnp.moveaxis(pieces, 0, dim).reshape(lengths)


def gathered_copies(x, axis, dim):
    pieces = sent_to_all(x, axis)
    return in_order(pieces, dim)


def by_axis(x, axes):
    for axis in axes:
        x = lax.psum(x, axis)
    return x


def split_product(low_part, cot_part):
    upper = low_part.astype(jnp.bfloat16)
    lower = (low_part - upper.astype(jnp.float32)).astype(jnp.bfloat16)
    return jnp.dot(upper.T, cot_part, preferred_element_type=jnp.float32) + jnp.dot(
        lower.T, cot_part, preferred_element_type=jnp.float32
    )


def cot_rows(query_low, key_low, cot_wide, width):

    def low_rows(start, count):
        return jnp.concatenate(
            [
                split_product(query_low, cot_wide[:, :width]),
                split_product(key_low, cot_wide[:, width:]),
            ],
            axis=1,
        )

    return low_rows


def head_squares(update):
    by_head = update.reshape(update.shape[0], -1, HD)
    return jnp.sum(by_head * by_head, axis=(0, 2))


def apply_scale(update, total):
    scale = 1.0 / jnp.sqrt(total / (D * HD) + norm_floor)
    by_head = update.reshape(update.shape[0], -1, HD)
    return (by_head * scale[None, :, None]).reshape(update.shape)


def body(
    saved_input,
    query_cot,
    key_cot,
    query_master,
    key_master,
    query_basis,
    key_basis,
    query_first,
    query_second,
    key_first,
    key_second,
):
    width = query_cot.shape[1]
    low_count = query_first.shape[0]
    cotangents = jnp.concatenate([query_cot, key_cot], axis=1)
    inputs = lax.all_gather(saved_input, "tp", axis=1, tiled=True)
    bases = in_one_piece((query_basis, key_basis), FS, 0, 1)
    query_low = jnp.dot(inputs, bases[0], preferred_element_type=jnp.float32)
    key_low = jnp.dot(inputs, bases[1], preferred_element_type=jnp.float32)
    low_rows = cot_rows(query_low, key_low, cotangents, width)
    projected = sent_and_summed(low_rows(jnp.int32(0), low_count * lax.axis_size(FS)), FS, 0)
    firsts = jnp.concatenate([query_first, key_first], axis=1)
    seconds = jnp.concatenate([query_second, key_second], axis=1)
    first_new = moment_decay * firsts + (1.0 - moment_decay) * projected
    second_new = square_decay * seconds + (1.0 - square_decay) * projected * projected
    ratio = (first_new / jnp.sqrt(second_new + square_floor)).astype(jnp.bfloat16)
    piece = gathered_copies(ratio, FS, 0)
    query_update = jnp.dot(query_basis, piece[:, :width], preferred_element_type=jnp.float32)
    key_update = jnp.dot(key_basis, piece[:, width:], preferred_element_type=jnp.float32)
    query_total, key_total = (
        by_axis(head_squares(query_update), FS),
        by_axis(head_squares(key_update), FS),
    )
    query_step = apply_scale(query_update, query_total)
    key_step = apply_scale(key_update, key_total)
    query_weight = query_master - step_rate * query_step
    key_weight = key_master - step_rate * key_step
    copies = in_one_piece(
        (query_weight.astype(jnp.bfloat16), key_weight.astype(jnp.bfloat16)), FS, 0, 1
    )
    return (
        query_step,
        query_weight,
        copies[0],
        first_new[:, :width],
        second_new[:, :width],
        key_step,
        key_weight,
        copies[1],
        first_new[:, width:],
        second_new[:, width:],
    )


def solution(mesh):
    torus = Mesh(mesh.devices.reshape(4, 4, mesh.shape["tp"]), ("fs_0", "fs_1", "tp"))
    in_specs = (
        P(FS, "tp"),
        P(FS, "tp"),
        P(FS, "tp"),
        P(FS, "tp"),
        P(FS, "tp"),
        P(FS, None),
        P(FS, None),
        P(FS, "tp"),
        P(FS, "tp"),
        P(FS, "tp"),
        P(FS, "tp"),
    )
    out_specs = (
        P(FS, "tp"),
        P(FS, "tp"),
        P(None, "tp"),
        P(FS, "tp"),
        P(FS, "tp"),
        P(FS, "tp"),
        P(FS, "tp"),
        P(None, "tp"),
        P(FS, "tp"),
        P(FS, "tp"),
    )
    return jax.shard_map(body, mesh=torus, in_specs=in_specs, out_specs=out_specs, check_vma=False)
```

profile of v0, /device:TPU:1, one launch (start us, length us, event | category | flops | bytes accessed | tf_op | source)
XLA Modules:
  0.0 306.6 jit_solution(4869370095504522026)
XLA Ops:
  7.2 0.0 copy-start
  7.2 0.0 all-gather.4.cloned.1.call-start
  7.2 1.7 pad_maximum_fusion
  9.0 0.0 all-gather.4.cloned.1.call-update
  9.0 0.0 all-gather.6.cloned.1.call-start
  9.0 0.7 all-gather.6.cloned.1.call-update
  9.7 73.7 %all-gather.4.cloned.1.call-done = bf16[4096,512]{1,0:T(8,128)(2,1)} async-done(((bf16[256,512]{1,0:T(8,128)(2,1)}), bf16[4096,512]{1,0:T(8,128)(2,1)}) %all-gather.4.cloned.1.call-update) | async-done | bytes 4194320 | tf_op jit(solution)/shard_map/all_gather | solution.py:22
  83.5 98.0 %all-gather.6.cloned.1.call-done = bf16[1024,4096]{1,0:T(8,128)(2,1)} async-done(((bf16[1024,128]{1,0:T(8,128)(2,1)}), bf16[1024,4096]{1,0:T(8,128)(2,1)}) %all-gather.6.cloned.1.call-update) | async-done | bytes 8388624 | tf_op jit(solution)/shard_map/all_gather | solution.py:109
  181.5 0.0 copy-start.10
  181.5 0.0 copy-start.11
  181.5 6.5 %fusion.4 = f32[1024,256]{0,1:T(8,128)S(1)} fusion(bf16[1024,4096]{1,0:T(8,128)(2,1)} %all-gather.6.cloned.1.call-done, bf16[4096,512]{1,0:T(8,128)(2,1)} %all-gather.4.cloned.1.call-done), kind=kOutput, calls=%fused_computation.4 | convolution fusion | flops 2147483648 | bytes 11534336 | tf_op jit(solution)/shard_map/dot_general | solution.py:111
  188.0 0.0 copy-done
  188.1 0.3 fusion.14
  188.4 0.3 convolution_add_fusion.1
  188.7 0.0 copy-done.10
  188.7 0.4 copy-done.11
  189.1 0.0 copy-start.1
  189.1 2.4 fusion.7
  191.5 0.0 copy-done.1
  191.5 0.0 copy-start.6
  191.5 0.0 copy-start.7
  191.5 0.0 copy-start.8
  191.5 0.0 copy-start.9
  191.5 0.0 copy-start.4
  191.5 0.0 copy-start.5
  191.6 0.0 copy-start.2
  191.6 0.0 copy-start.3
  191.6 0.3 fusion.11
  191.9 0.3 convolution_add_fusion
  192.3 0.1 copy.29
  192.4 14.6 %all_to_all.10 = f32[16,16,256]{2,1,0:T(8,128)S(1)} all-to-all(f32[16,16,256]{2,1,0:T(8,128)S(1)} %bitcast.24), channel_id=1, replica_groups=mesh['fs_0'=4,'fs_1'=4,'tp'=32] {'fs_0','fs_1'}, dimensions={0} | all-to-all | bytes 524288 | tf_op jit(solution)/shard_map/all_to_all | solution.py:34
  207.0 0.0 copy-done.6
  207.0 0.0 copy-done.7
  207.0 0.0 copy-done.8
  207.0 0.0 copy-done.9
  207.0 0.7 broadcast_in_dim.2
  207.7 3.5 %all-to-all-start.1 = ((bf16[16,16,256]{2,1,0:T(8,128)(2,1)}), bf16[16,16,256]{2,1,0:T(8,128)(2,1)S(1)}, u32[]{:S(2)}, u32[]{:S(2)}) async-start(bf16[16,16,256]{2,1,0:T(8,128)(2,1)} %broadcast_in_dim.2), calls=%async_computation.1 | async-start | bytes 262144 | tf_op jit(solution)/shard_map/all_to_all | solution.py:40
  211.2 0.0 all-gather.8.cloned.1.call-start
  211.3 0.0 copy-done.4
  211.3 0.1 copy.30
  211.4 0.0 copy-done.5
  211.4 0.1 copy.31
  211.5 6.6 %all-to-all-done.1 = bf16[16,16,256]{2,1,0:T(8,128)(2,1)S(1)} async-done(((bf16[16,16,256]{2,1,0:T(8,128)(2,1)}), bf16[16,16,256]{2,1,0:T(8,128)(2,1)S(1)}, u32[]{:S(2)}, u32[]{:S(2)}) %all-to-all-start.1) | async-done | bytes 131104 | tf_op jit(solution)/shard_map/all_to_all | solution.py:40
  218.1 0.0 copy-done.2
  218.1 0.8 multiply_reduce_fusion.1
  218.9 0.0 copy-done.3
  218.9 0.8 multiply_reduce_fusion
  219.7 7.1 %all-reduce.1 = (f32[1]{0:T(128)}, f32[1]{0:T(128)}) all-reduce(f32[1]{0:T(128)} %bitcast.4, f32[1]{0:T(128)} %bitcast.7), channel_id=1, replica_groups=mesh['fs_0'=4,'fs_1'=4,'tp'=32] {'fs_0'}, use_global_device_ids=true, to_apply=%region_2.0 | all-reduce | flops 2 | bytes 16 | tf_op jit(solution)/shard_map/psum | solution.py:56
  226.9 7.5 %all-reduce = (f32[1]{0:T(128)}, f32[1]{0:T(128)}) all-reduce(f32[1]{0:T(128)} %get-tuple-element.32, f32[1]{0:T(128)} %get-tuple-element.33), channel_id=1, replica_groups=mesh['fs_0'=4,'fs_1'=4,'tp'=32] {'fs_1'}, use_global_device_ids=true, to_apply=%region_3.0 | all-reduce | flops 2 | bytes 16 | tf_op jit(solution)/shard_map/psum | solution.py:56
  235.8 0.1 fusion.22
  235.8 0.7 pad_maximum_fusion.2
  236.5 0.0 all-gather.8.cloned.1.call-update
  236.5 0.6 fusion.27
  237.1 0.8 copy.32
  237.9 0.8 copy.33
  238.6 0.8 copy.35
  239.4 0.8 copy.36
  240.2 55.6 %all-gather.8.cloned.1.call-done = bf16[4096,256]{0,1:T(8,128)(2,1)} async-done(((bf16[256,256]{0,1:T(8,128)(2,1)}), bf16[4096,256]{0,1:T(8,128)(2,1)}) %all-gather.8.cloned.1.call-update) | async-done | bytes 2097168 | tf_op jit(solution)/shard_map/all_gather | solution.py:22
  295.8 1.7 fusion.26
  297.4 1.3 copy.34
  298.7 1.3 copy.37
  (3 shorter events, 0.1 us)
Async XLA Ops:
  7.2 180.9 %copy-start = (bf16[1024,128]{1,0:T(8,128)(2,1)S(1)}, bf16[1024,128]{1,0:T(8,128)(2,1)}, u32[]{:S(2)}) copy-start(bf16[1024,128]{1,0:T(8,128)(2,1)} %param.12) | copy-start | bytes 786436
  7.2 76.3 %all-gather.4.cloned.1.call-start = ((), (), s32[]{:S(2)}) async-start(), calls=%async_computation.2 | async-start | bytes 4456448 | tf_op jit(solution)/shard_map/all_gather | solution.py:22
  9.0 172.5 %all-gather.6.cloned.1.call-start = ((), (), s32[]{:S(2)}) async-start(), calls=%async_computation.3 | async-start | bytes 8650752 | tf_op jit(solution)/shard_map/all_gather | solution.py:109
  181.5 7.2 %copy-start.10 = (bf16[1024,4096]{1,0:T(8,128)(2,1)S(1)}, bf16[1024,4096]{1,0:T(8,128)(2,1)}, u32[]{:S(2)}) copy-start(bf16[1024,4096]{1,0:T(8,128)(2,1)} %all-gather.6.cloned.1.call-done) | copy-start | bytes 25165828
  181.5 7.6 %copy-start.11 = (bf16[4096,512]{1,0:T(8,128)(2,1)S(1)}, bf16[4096,512]{1,0:T(8,128)(2,1)}, u32[]{:S(2)}) copy-start(bf16[4096,512]{1,0:T(8,128)(2,1)} %all-gather.4.cloned.1.call-done) | copy-start | bytes 12582916
  189.1 2.4 copy-start.1
  191.5 15.5 %copy-start.6 = (f32[16,128]{1,0:T(8,128)S(1)}, f32[16,128]{1,0:T(8,128)}, u32[]{:S(2)}) copy-start(f32[16,128]{1,0:T(8,128)} %param.21) | copy-start | bytes 24580
  191.5 15.5 %copy-start.7 = (f32[16,128]{1,0:T(8,128)S(1)}, f32[16,128]{1,0:T(8,128)}, u32[]{:S(2)}) copy-start(f32[16,128]{1,0:T(8,128)} %param.19) | copy-start | bytes 24580
  191.5 15.5 %copy-start.8 = (f32[16,128]{1,0:T(8,128)S(1)}, f32[16,128]{1,0:T(8,128)}, u32[]{:S(2)}) copy-start(f32[16,128]{1,0:T(8,128)} %param.20) | copy-start | bytes 24580
  191.5 15.5 %copy-start.9 = (f32[16,128]{1,0:T(8,128)S(1)}, f32[16,128]{1,0:T(8,128)}, u32[]{:S(2)}) copy-start(f32[16,128]{1,0:T(8,128)} %param.18) | copy-start | bytes 24580
  191.5 19.7 %copy-start.4 = (f32[256,128]{1,0:T(8,128)S(1)}, f32[256,128]{1,0:T(8,128)}, u32[]{:S(2)}) copy-start(f32[256,128]{1,0:T(8,128)} %param.14) | copy-start | bytes 393220
  191.5 19.8 %copy-start.5 = (f32[256,128]{1,0:T(8,128)S(1)}, f32[256,128]{1,0:T(8,128)}, u32[]{:S(2)}) copy-start(f32[256,128]{1,0:T(8,128)} %param.15) | copy-start | bytes 393220
  191.6 26.5 %copy-start.2 = (bf16[256,256]{1,0:T(8,128)(2,1)S(1)}, bf16[256,256]{1,0:T(8,128)(2,1)}, u32[]{:S(2)}) copy-start(bf16[256,256]{1,0:T(8,128)(2,1)} %param.16) | copy-start | bytes 393220
  191.6 27.4 %copy-start.3 = (bf16[256,256]{1,0:T(8,128)(2,1)S(1)}, bf16[256,256]{1,0:T(8,128)(2,1)}, u32[]{:S(2)}) copy-start(bf16[256,256]{1,0:T(8,128)(2,1)} %param.17) | copy-start | bytes 393220
  207.7 10.4 %all-to-all-start.1 = ((bf16[16,16,256]{2,1,0:T(8,128)(2,1)}), bf16[16,16,256]{2,1,0:T(8,128)(2,1)S(1)}, u32[]{:S(2)}, u32[]{:S(2)}) async-start(bf16[16,16,256]{2,1,0:T(8,128)(2,1)} %broadcast_in_dim.2), calls=%async_computation.1 | async-start | bytes 262144 | tf_op jit(solution)/shard_map/all_to_all | solution.py:40
  211.2 84.5 %all-gather.8.cloned.1.call-start = ((), (), s32[]{:S(2)}) async-start(), calls=%async_computation.4 | async-start | bytes 2228224 | tf_op jit(solution)/shard_map/all_gather | solution.py:22
Sparse Core Ops, SparseCore 0:
  11.6 71.8 all-gather.3
  85.5 95.9 all-gather.5
  236.6 59.0 all-gather.7
where the time goes:
time: 307 us
  waiting for transfers between devices  235 us (77%)
  blocking collectives  29.2 us (10%)
  between operations  15.4 us (5%)
  matrix products  11.8 us (4%)
  local copies, waits for them, and re-layouts  9.34 us (3%)
  starting transfers between devices  3.63 us (1%)
    all_gather x2, waiting for transfers between devices, in_one_piece(): out = lax.all_gather(both, axis, axis=dim, tiled=True)  129 us
    all_gather x1, waiting for transfers between devices, body(): inputs = lax.all_gather(saved_input, 'tp', axis=1, tiled=True)  98 us
    psum x2, blocking collectives, by_axis(): x = lax.psum(x, axis)  14.7 us
    all_to_all x1, blocking collectives, sent_and_summed(): pieces = lax.all_to_all(cut_along(x, dim, count), axis, 0, 0, tiled=True)  14.6 us
    all_to_all x1, waiting for transfers between devices, sent_to_all(): lax.all_to_all(jnp.broadcast_to(x[None], (count, *x.shape)), axis, 0, 0,...  6.6 us
    dot_general x1, matrix products, body(): query_low = jnp.dot(inputs, bases[0], preferred_element_type=jnp.float32)  6.54 us
    unnamed x32, local copies, waits for them, and re-layouts  6.25 us
  transfers between devices with their start and end apart: 4, of which 4 were waited for; matrix products, arithmetic and copies ran while one was open for 1% of the time, Pallas kernels for 0%

commit v1 on v0

v1 whole, which is shorter than its diff:
```python
import jax
import jax.numpy as jnp
from jax import lax
from jax.sharding import Mesh
from jax.sharding import PartitionSpec as P

D = 4096
HD = 128
FS = ("y", "x")


moment_decay = 0.8
square_decay = 0.9
square_floor = 1.0
norm_floor = 0.01
step_rate = 0.01


def sent_to_all(x, axis):
    count = lax.axis_size(axis)
    return lax.all_to_all(jnp.broadcast_to(x[None], (count, *x.shape)), axis, 0, 0, tiled=True)


def body(
    saved_input,
    query_cot,
    key_cot,
    query_master,
    key_master,
    query_basis,
    key_basis,
    query_first,
    query_second,
    key_first,
    key_second,
):
    rows = lax.axis_size(FS)
    depth = lax.axis_size("z")
    tokens, width = query_cot.shape
    low_count = query_first.shape[0]
    share = tokens // depth
    first_core = lax.axis_index("c") == 0

    own_basis = jnp.where(first_core, query_basis, key_basis)
    basis = sent_to_all(own_basis, FS).reshape(D, -1)
    pieces = lax.all_to_all(saved_input.reshape(depth, share, width), "z", 0, 0, tiled=True)
    pieces = lax.all_gather(pieces, "c", axis=0, tiled=False)
    inputs = pieces.transpose(2, 1, 0, 3).reshape(share, D)
    low = jnp.dot(inputs, basis, preferred_element_type=jnp.float32).astype(jnp.bfloat16)
    low = lax.all_gather(low, "z", axis=0, tiled=True)
    cots = lax.all_to_all(jnp.stack([query_cot, key_cot]), "c", 0, 0, tiled=True)
    partial = [
        lax.dot_general(low, cots[h], (((0,), (0,)), ((), ())), preferred_element_type=jnp.float32)
        .reshape(rows, low_count, width)
        for h in range(2)
    ]
    partial = jnp.stack(partial, axis=1).reshape(2 * rows, low_count, width)
    partial = lax.all_to_all(partial, (*FS, "c"), 0, 0, tiled=True)
    projected = jnp.sum(partial.reshape(rows, 2, low_count, width), axis=0)

    firsts = jnp.stack([query_first, key_first])
    seconds = jnp.stack([query_second, key_second])
    first_new = moment_decay * firsts + (1.0 - moment_decay) * projected
    second_new = square_decay * seconds + (1.0 - square_decay) * projected * projected
    ratio = (first_new / jnp.sqrt(second_new + square_floor)).astype(jnp.bfloat16)
    ratio = sent_to_all(ratio, FS).transpose(1, 0, 2, 3).reshape(2, rows * low_count, width)

    bases = sent_to_all(basis, "c")
    masters = sent_to_all(jnp.stack([query_master, key_master]).astype(jnp.bfloat16), FS)
    outs = []
    for k, (own, master) in enumerate(((query_basis, query_master), (key_basis, key_master))):
        update = jnp.dot(bases[k], ratio[k], preferred_element_type=jnp.float32)
        scale = 1.0 / jnp.sqrt(jnp.sum(update * update) / (D * HD) + norm_floor)
        whole = masters[:, k].reshape(D, width).astype(jnp.float32)
        copy = (whole - step_rate * (update * scale)).astype(jnp.bfloat16)
        step = jnp.dot(own, ratio[k], preferred_element_type=jnp.float32) * scale
        weight = master - step_rate * step
        outs += [step, weight, copy, first_new[k], second_new[k]]
    return tuple(outs)


def solution(mesh):
    torus = Mesh(mesh.devices.reshape(4, 4, 16, 2), ("y", "x", "z", "c"))
    tp = ("z", "c")
    split = P(FS, tp)
    rows = P(FS, None)
    copied = P(None, tp)
    in_specs = (split,) * 5 + (rows,) * 2 + (split,) * 4
    out_specs = (split, split, copied, split, split) * 2
    return jax.shard_map(body, mesh=torus, in_specs=in_specs, out_specs=out_specs, check_vma=False)
```

time: 307 us -> 193 us (0.63)
  waiting for transfers between devices: 235 us -> 54.9 us
  starting transfers between devices: 3.63 us -> 46.1 us
  blocking collectives: 29.2 us -> 49.3 us
  between operations: 15.4 us -> 2.22 us
  local copies, waits for them, and re-layouts: 9.34 us -> 20.6 us
  other arithmetic: 2.5 us -> 6.05 us
    all_gather x3 -> x0, waiting for transfers between devices: 227 us -> none  [the longest x2 129 us: in_one_piece(): out = lax.all_gather(both, axis, axis=dim, tiled=True)]
    all_gather x0 -> x2, blocking collectives: none -> 38.7 us  [the longest x1 30.4 us: body(): low = lax.all_gather(low, 'z', axis=0, tiled=True)]
    all_to_all x1 -> x4, waiting for transfers between devices: 6.6 us -> 34.7 us  [sent_to_all(): lax.all_to_all(jnp.broadcast_to(x[None], (count, *x.shape)), axis, 0, 0,...]
    all_to_all x0 -> x2, starting transfers between devices: none -> 23.5 us  [the longest x1 13.9 us: body(): partial = lax.all_to_all(partial, (*FS, 'c'), 0, 0, tiled=True)]
    all_to_all x0 -> x2, waiting for transfers between devices: none -> 20.1 us  [the longest x1 14 us: body(): lax.all_to_all(saved_input.reshape(depth, share, width), 'z', 0, 0, tiled...]
    all_to_all x1 -> x4, starting transfers between devices: 3.51 us -> 22.6 us  [sent_to_all(): lax.all_to_all(jnp.broadcast_to(x[None], (count, *x.shape)), axis, 0, 0,...]
    psum x2 -> x0, blocking collectives: 14.7 us -> none  [by_axis(): x = lax.psum(x, axis)]
    broadcast_in_dim x1 -> x4, local copies, waits for them, and re-layouts: 0.66 us -> 6.26 us  [sent_to_all(): jnp.broadcast_to(x[None], (count, *x.shape))]
  transfers between devices with their start and end apart: 4 -> 6, of which waited for: 4 -> 5; matrix products, arithmetic and copies ran while one was open for 1% -> 6% of each run, Pallas kernels for 0% -> 0%
where the time goes in v1:
time: 193 us; the launch traced here: 192 us
  waiting for transfers between devices  54.9 us (28%)
  blocking collectives  49.3 us (26%)
  starting transfers between devices  46.1 us (24%)
  local copies, waits for them, and re-layouts  20.6 us (11%)
  matrix products  13.3 us (7%)
  other arithmetic  6.05 us (3%)
  between operations  2.22 us (1%)
    all_to_all x4, waiting for transfers between devices, sent_to_all(): lax.all_to_all(jnp.broadcast_to(x[None], (count, *x.shape)), axis, 0, 0,...  34.7 us
    all_gather x1, blocking collectives, body(): low = lax.all_gather(low, 'z', axis=0, tiled=True)  30.4 us
    all_to_all x4, starting transfers between devices, sent_to_all(): lax.all_to_all(jnp.broadcast_to(x[None], (count, *x.shape)), axis, 0, 0,...  22.6 us
    all_to_all x1, waiting for transfers between devices, body(): lax.all_to_all(saved_input.reshape(depth, share, width), 'z', 0, 0, tiled...  14 us
    all_to_all x1, starting transfers between devices, body(): partial = lax.all_to_all(partial, (*FS, 'c'), 0, 0, tiled=True)  13.9 us
    all_to_all x1, blocking collectives, body(): lax.all_to_all(jnp.stack([query_cot, key_cot]), 'c', 0, 0, tiled=True)  10.6 us
    all_to_all x1, starting transfers between devices, body(): lax.all_to_all(saved_input.reshape(depth, share, width), 'z', 0, 0, tiled...  9.57 us
    all_gather x1, blocking collectives, body(): pieces = lax.all_gather(pieces, 'c', axis=0, tiled=False)  8.28 us
  transfers between devices with their start and end apart: 6, of which 5 were waited for; matrix products, arithmetic and copies ran while one was open for 6% of the time, Pallas kernels for 0%

profile of v1, /device:TPU:1, one launch (start us, length us, event | category | flops | bytes accessed | tf_op | source)
XLA Modules:
  0.0 192.4 jit_solution(2961061514629770844)
XLA Ops:
  0.6 0.0 copy-start.4
  0.7 0.0 copy-start.3
  0.7 1.1 pad_maximum_fusion
  1.8 10.6 %all_to_all.35 = bf16[2,1024,128]{2,1,0:T(8,128)(2,1)S(1)} all-to-all(bf16[2,1024,128]{2,1,0:T(8,128)(2,1)S(1)} %pad_maximum_fusion), channel_id=1, replica_groups=mesh['y'=4,'x'=4,'z'=16,'c'=2] {'c'}, dimensions={0} | all-to-all | bytes 1048576 | tf_op jit(solution)/shard_map/all_to_all | solution.py:51
  12.4 9.6 %all-to-all-start.1 = ((bf16[16,64,128]{2,1,0:T(8,128)(2,1)}), bf16[16,64,128]{2,1,0:T(8,128)(2,1)S(1)}, u32[]{:S(2)}, u32[]{:S(2)}) async-start(bf16[16,64,128]{2,1,0:T(8,128)(2,1)} %bitcast.3), calls=%async_computation.1 | async-start | bytes 524288 | tf_op jit(solution)/shard_map/all_to_all | solution.py:46
  22.0 0.0 copy-done.4
  22.0 0.0 copy-done.3
  22.0 14.0 %all-to-all-done.1 = bf16[16,64,128]{2,1,0:T(8,128)(2,1)S(1)} async-done(((bf16[16,64,128]{2,1,0:T(8,128)(2,1)}), bf16[16,64,128]{2,1,0:T(8,128)(2,1)S(1)}, u32[]{:S(2)}, u32[]{:S(2)}) %all-to-all-start.1) | async-done | bytes 262176 | tf_op jit(solution)/shard_map/all_to_all | solution.py:46
  36.0 1.5 broadcast_in_dim.8
  37.5 0.0 copy-start.1
  37.5 0.0 copy-start.2
  37.5 6.9 %all-to-all-start = ((bf16[16,256,256]{2,1,0:T(8,128)(2,1)}), bf16[16,256,256]{2,1,0:T(8,128)(2,1)S(1)}, u32[]{:S(2)}, u32[]{:S(2)}) async-start(bf16[16,256,256]{2,1,0:T(8,128)(2,1)} %broadcast_in_dim.8), calls=%async_computation | async-start | bytes 4194304 | tf_op jit(solution)/shard_map/all_to_all | solution.py:21
  44.4 0.0 copy-done.1
  44.5 0.0 copy-done.2
  44.5 24.1 %all-to-all-done = bf16[16,256,256]{2,1,0:T(8,128)(2,1)S(1)} async-done(((bf16[16,256,256]{2,1,0:T(8,128)(2,1)}), bf16[16,256,256]{2,1,0:T(8,128)(2,1)S(1)}, u32[]{:S(2)}, u32[]{:S(2)}) %all-to-all-start) | async-done | bytes 2097184 | tf_op jit(solution)/shard_map/all_to_all | solution.py:21
  68.6 1.8 broadcast_in_dim.11
  70.4 5.5 %all-to-all-start.6 = ((bf16[16,2,256,128]{3,2,1,0:T(8,128)(2,1)}), bf16[16,2,256,128]{3,2,1,0:T(8,128)(2,1)}, u32[]{:S(2)}, u32[]{:S(2)}) async-start(bf16[16,2,256,128]{3,2,1,0:T(8,128)(2,1)} %broadcast_in_dim.11), calls=%async_computation.6 | async-start | bytes 4194304 | tf_op jit(solution)/shard_map/all_to_all | solution.py:21
  76.0 0.8 copy.50
  76.7 0.8 copy.49
  77.5 8.3 %all-gather = bf16[32,64,128]{2,1,0:T(8,128)(2,1)S(1)} all-gather(bf16[16,64,128]{2,1,0:T(8,128)(2,1)S(1)} %all-to-all-done.1), channel_id=2, replica_groups=mesh['y'=4,'x'=4,'z'=16,'c'=2] {'c'}, dimensions={0}, use_global_device_ids=true | all-gather | bytes 786432 | tf_op jit(solution)/shard_map/all_gather | solution.py:47
  85.8 0.5 copy.46
  86.3 1.2 reshape.122
  87.5 1.5 fusion.6
  89.0 30.4 %all_gather.11 = bf16[1024,256]{1,0:T(8,128)(2,1)} all-gather(bf16[64,256]{1,0:T(8,128)(2,1)S(1)} %fusion.6), channel_id=1, replica_groups=mesh['y'=4,'x'=4,'z'=16,'c'=2] {'z'}, dimensions={0}, use_global_device_ids=true | all-gather | bytes 557056 | tf_op jit(solution)/shard_map/all_gather | solution.py:50
  119.4 1.2 copy.47
  120.7 0.3 convolution_bitcast_fusion
  121.0 0.3 convolution_bitcast_fusion.1
  121.3 0.7 copy.48
  122.0 0.0 all-to-all-done.6
  122.0 13.9 %all-to-all-start.3 = ((f32[32,16,128]{2,1,0:T(8,128)}), f32[32,16,128]{2,1,0:T(8,128)S(1)}, u32[]{:S(2)}, u32[]{:S(2)}) async-start(f32[32,16,128]{2,1,0:T(8,128)} %bitcast.17), calls=%async_computation.3 | async-start | bytes 524288 | tf_op jit(solution)/shard_map/all_to_all | solution.py:58
  135.9 2.7 %fusion.11 = (bf16[16,1,256,128]{3,2,1,0:T(8,128)(2,1)}, bf16[16,1,256,128]{3,2,1,0:T(8,128)(2,1)S(1)}) fusion(bf16[16,2,256,128]{3,2,1,0:T(8,128)(2,1)} %all-to-all-done.6), kind=kLoop, calls=%fused_computation.38 | loop fusion | bytes 4194304 | tf_op jit(solution)/shard_map/slice | solution.py:74
  138.6 6.2 %all-to-all-done.3 = f32[32,16,128]{2,1,0:T(8,128)S(1)} async-done(((f32[32,16,128]{2,1,0:T(8,128)}), f32[32,16,128]{2,1,0:T(8,128)S(1)}, u32[]{:S(2)}, u32[]{:S(2)}) %all-to-all-start.3) | async-done | bytes 262176 | tf_op jit(solution)/shard_map/all_to_all | solution.py:58
  144.8 0.8 multiply_convert_fusion
  145.6 0.7 broadcast_in_dim.9
  146.3 3.5 %all-to-all-start.4 = ((bf16[16,2,16,128]{3,2,1,0:T(8,128)(2,1)}), bf16[16,2,16,128]{3,2,1,0:T(8,128)(2,1)S(1)}, u32[]{:S(2)}, u32[]{:S(2)}) async-start(bf16[16,2,16,128]{3,2,1,0:T(8,128)(2,1)} %broadcast_in_dim.9), calls=%async_computation.4 | async-start | bytes 262144 | tf_op jit(solution)/shard_map/all_to_all | solution.py:21
  149.8 0.6 slice_bitcast_fusion.8
  150.4 6.5 %all-to-all-done.4 = bf16[16,2,16,128]{3,2,1,0:T(8,128)(2,1)S(1)} async-done(((bf16[16,2,16,128]{3,2,1,0:T(8,128)(2,1)}), bf16[16,2,16,128]{3,2,1,0:T(8,128)(2,1)S(1)}, u32[]{:S(2)}, u32[]{:S(2)}) %all-to-all-start.4) | async-done | bytes 131104 | tf_op jit(solution)/shard_map/all_to_all | solution.py:21
  156.9 2.3 %broadcast_in_dim.10 = bf16[2,4096,256]{2,1,0:T(8,128)(2,1)} broadcast(bf16[4096,256]{1,0:T(8,128)(2,1)S(1)} %bitcast.75), dimensions={1,2} | broadcast | bytes 6291456 | tf_op jit(solution)/shard_map/broadcast_in_dim | solution.py:21
  159.2 6.7 %all-to-all-start.5 = ((bf16[2,4096,256]{2,1,0:T(8,128)(2,1)}), bf16[2,4096,256]{2,1,0:T(8,128)(2,1)}, u32[]{:S(2)}, u32[]{:S(2)}) async-start(bf16[2,4096,256]{2,1,0:T(8,128)(2,1)} %broadcast_in_dim.10), calls=%async_computation.5 | async-start | bytes 8388608 | tf_op jit(solution)/shard_map/all_to_all | solution.py:21
  165.9 4.1 %all-to-all-done.5 = bf16[2,4096,256]{2,1,0:T(8,128)(2,1)} async-done(((bf16[2,4096,256]{2,1,0:T(8,128)(2,1)}), bf16[2,4096,256]{2,1,0:T(8,128)(2,1)}, u32[]{:S(2)}, u32[]{:S(2)}) %all-to-all-start.5) | async-done | bytes 4194336 | tf_op jit(solution)/shard_map/all_to_all | solution.py:21
  170.0 3.2 %multiply_reduce_fusion = (f32[]{:T(128)}, f32[4096,128]{1,0:T(8,128)S(1)}) fusion(bf16[256,128]{1,0:T(8,128)(2,1)S(1)} %bitcast.83, bf16[2,4096,256]{2,1,0:T(8,128)(2,1)} %all-to-all-done.5), kind=kOutput, calls=%fused_computation.8 | convolution fusion | flops 269484032 | bytes 4259844 | tf_op jit(solution)/shard_map/dot_general | solution.py:72
  173.8 0.0 copy-start.5
  173.8 4.5 %multiply_reduce_fusion.1 = (f32[]{:T(128)}, f32[4096,128]{1,0:T(8,128)}) fusion(bf16[256,128]{1,0:T(8,128)(2,1)S(1)} %bitcast.81, bf16[2,4096,256]{2,1,0:T(8,128)(2,1)} %all-to-all-done.5), kind=kOutput, calls=%fused_computation.9 | convolution fusion | flops 269484032 | bytes 4259844 | tf_op jit(solution)/shard_map/dot_general | solution.py:72
  179.0 1.8 multiply_subtract_fusion
  180.8 1.7 copy.53
  182.5 1.7 copy.54
  184.1 0.0 copy-done.5
  184.1 1.8 multiply_subtract_fusion.1
  185.9 1.7 copy.51
  187.5 0.8 copy.52
  188.3 0.0 copy-start
  188.3 2.7 %fusion.2 = bf16[4096,128]{1,0:T(8,128)(2,1)} fusion(f32[4096,128]{1,0:T(8,128)S(1)} %get-tuple-element.66, bf16[16,1,256,128]{3,2,1,0:T(8,128)(2,1)} %get-tuple-element.53, f32[]{:T(128)S(6)} %sqrt.11), kind=kLoop, calls=%fused_computation.5 | loop fusion | flops 2621440 | bytes 4194308 | tf_op jit(solution)/shard_map/convert_element_type | solution.py:75
  191.0 0.0 copy-done
  191.0 1.4 fusion.3
  (6 shorter events, 0.1 us)
Async XLA Ops:
  0.6 21.4 %copy-start.4 = (bf16[256,256]{1,0:T(8,128)(2,1)S(1)}, bf16[256,256]{1,0:T(8,128)(2,1)}, u32[]{:S(2)}) copy-start(bf16[256,256]{1,0:T(8,128)(2,1)} %param.16) | copy-start | bytes 393220
  0.7 21.3 %copy-start.3 = (bf16[256,256]{1,0:T(8,128)(2,1)S(1)}, bf16[256,256]{1,0:T(8,128)(2,1)}, u32[]{:S(2)}) copy-start(bf16[256,256]{1,0:T(8,128)(2,1)} %param.17) | copy-start | bytes 393220
  12.4 23.6 %all-to-all-start.1 = ((bf16[16,64,128]{2,1,0:T(8,128)(2,1)}), bf16[16,64,128]{2,1,0:T(8,128)(2,1)S(1)}, u32[]{:S(2)}, u32[]{:S(2)}) async-start(bf16[16,64,128]{2,1,0:T(8,128)(2,1)} %bitcast.3), calls=%async_computation.1 | async-start | bytes 524288 | tf_op jit(solution)/shard_map/all_to_all | solution.py:46
  37.5 6.9 %copy-start.1 = (f32[256,128]{1,0:T(8,128)S(1)}, f32[256,128]{1,0:T(8,128)}, u32[]{:S(2)}) copy-start(f32[256,128]{1,0:T(8,128)} %param.15) | copy-start | bytes 393220
  37.5 6.9 %copy-start.2 = (f32[256,128]{1,0:T(8,128)S(1)}, f32[256,128]{1,0:T(8,128)}, u32[]{:S(2)}) copy-start(f32[256,128]{1,0:T(8,128)} %param.14) | copy-start | bytes 393220
  37.5 31.1 %all-to-all-start = ((bf16[16,256,256]{2,1,0:T(8,128)(2,1)}), bf16[16,256,256]{2,1,0:T(8,128)(2,1)S(1)}, u32[]{:S(2)}, u32[]{:S(2)}) async-start(bf16[16,256,256]{2,1,0:T(8,128)(2,1)} %broadcast_in_dim.8), calls=%async_computation | async-start | bytes 4194304 | tf_op jit(solution)/shard_map/all_to_all | solution.py:21
  70.4 51.6 %all-to-all-start.6 = ((bf16[16,2,256,128]{3,2,1,0:T(8,128)(2,1)}), bf16[16,2,256,128]{3,2,1,0:T(8,128)(2,1)}, u32[]{:S(2)}, u32[]{:S(2)}) async-start(bf16[16,2,256,128]{3,2,1,0:T(8,128)(2,1)} %broadcast_in_dim.11), calls=%async_computation.6 | async-start | bytes 4194304 | tf_op jit(solution)/shard_map/all_to_all | solution.py:21
  122.0 22.8 %all-to-all-start.3 = ((f32[32,16,128]{2,1,0:T(8,128)}), f32[32,16,128]{2,1,0:T(8,128)S(1)}, u32[]{:S(2)}, u32[]{:S(2)}) async-start(f32[32,16,128]{2,1,0:T(8,128)} %bitcast.17), calls=%async_computation.3 | async-start | bytes 524288 | tf_op jit(solution)/shard_map/all_to_all | solution.py:58
  146.3 10.6 %all-to-all-start.4 = ((bf16[16,2,16,128]{3,2,1,0:T(8,128)(2,1)}), bf16[16,2,16,128]{3,2,1,0:T(8,128)(2,1)S(1)}, u32[]{:S(2)}, u32[]{:S(2)}) async-start(bf16[16,2,16,128]{3,2,1,0:T(8,128)(2,1)} %broadcast_in_dim.9), calls=%async_computation.4 | async-start | bytes 262144 | tf_op jit(solution)/shard_map/all_to_all | solution.py:21
  159.2 10.8 %all-to-all-start.5 = ((bf16[2,4096,256]{2,1,0:T(8,128)(2,1)}), bf16[2,4096,256]{2,1,0:T(8,128)(2,1)}, u32[]{:S(2)}, u32[]{:S(2)}) async-start(bf16[2,4096,256]{2,1,0:T(8,128)(2,1)} %broadcast_in_dim.10), calls=%async_computation.5 | async-start | bytes 8388608 | tf_op jit(solution)/shard_map/all_to_all | solution.py:21
  173.8 10.3 %copy-start.5 = (bf16[256,256]{1,0:T(8,128)(2,1)S(1)}, bf16[256,256]{1,0:T(8,128)(2,1)}, u32[]{:S(2)}) copy-start(bf16[256,256]{1,0:T(8,128)(2,1)} %param.16) | copy-start | bytes 393220
  188.3 2.7 %copy-start = (f32[4096,128]{1,0:T(8,128)S(1)}, f32[4096,128]{1,0:T(8,128)}, u32[]{:S(2)}) copy-start(f32[4096,128]{1,0:T(8,128)} %get-tuple-element.62) | copy-start | bytes 6291460

commit v2 on v1

v2 whole, which is shorter than its diff:
```python
import jax
import jax.numpy as jnp
from jax import lax
from jax.experimental import pallas as pl
from jax.experimental.pallas import tpu as pltpu
from jax.sharding import Mesh
from jax.sharding import PartitionSpec as P


D = 4096
HD = 128
FS = ("y", "x")
BF = jnp.bfloat16
F32 = jnp.float32

moment_decay = 0.8
square_decay = 0.9
square_floor = 1.0
norm_floor = 0.01
step_rate = 0.01

VMEM = pltpu.CompilerParams(vmem_limit_bytes=48 * 1024 * 1024)


def sent_to_all(x, axis):
    count = lax.axis_size(axis)
    return lax.all_to_all(jnp.broadcast_to(x[None], (count, *x.shape)), axis, 0, 0, tiled=True)


def swapped(x, axis):
    count = lax.axis_size(axis)
    return lax.ppermute(x, axis, [(i, i ^ 1) for i in range(count)])


def product_kernel(core_ref, own_ref, other_ref, basis_ref, out_ref):
    core = core_ref[0]
    total = jnp.zeros(out_ref.shape, F32)
    for z in range(own_ref.shape[0]):
        total += jnp.dot(own_ref[z], basis_ref[z, core], preferred_element_type=F32)
        total += jnp.dot(other_ref[z], basis_ref[z, 1 - core], preferred_element_type=F32)
    out_ref[...] = total.astype(out_ref.dtype)


def product(core, own, other, basis):
    depth, share, width = own.shape
    basis = basis.reshape(depth, 2, width, basis.shape[-1])
    return pl.pallas_call(
        product_kernel,
        out_shape=jax.ShapeDtypeStruct((share, basis.shape[-1]), BF),
        in_specs=[pl.BlockSpec(memory_space=pltpu.SMEM)] + [pl.BlockSpec(memory_space=pltpu.VMEM)] * 3,
        compiler_params=VMEM,
        name="product",
    )(core, own, other, basis)


def partial_kernel(core_ref, low_ref, own_ref, other_ref, out_ref):
    core = core_ref[0]
    chunks, halves, share, ranks = low_ref.shape
    rows, _, count, width = out_ref.shape
    per = rows // halves
    for half in range(halves):
        mine = jnp.zeros((ranks, width), F32)
        theirs = jnp.zeros((ranks, width), F32)
        for chunk in range(chunks):
            part = low_ref[chunk, half]
            span = pl.ds(chunk * share, share)
            contract = (((0,), (0,)), ((), ()))
            mine += lax.dot_general(part, own_ref[span, :], contract, preferred_element_type=F32)
            theirs += lax.dot_general(part, other_ref[span, :], contract, preferred_element_type=F32)
        span = pl.ds(half * per, per)
        out_ref[span, core] = mine.reshape(per, count, width).astype(out_ref.dtype)
        out_ref[span, 1 - core] = theirs.reshape(per, count, width).astype(out_ref.dtype)


def partials(core, low, own, other, rows, count):
    return pl.pallas_call(
        partial_kernel,
        out_shape=jax.ShapeDtypeStruct((rows, 2, count, own.shape[-1]), BF),
        in_specs=[pl.BlockSpec(memory_space=pltpu.SMEM)] + [pl.BlockSpec(memory_space=pltpu.VMEM)] * 3,
        compiler_params=VMEM,
        name="partials",
    )(core, low, own, other)


BLOCK = 512


def finish_kernel(
    place_ref,
    ratio_ref,
    own_a_ref,
    own_b_ref,
    other_a_ref,
    other_b_ref,
    masters_ref,
    query_master_ref,
    key_master_ref,
    query_step_ref,
    query_weight_ref,
    query_copy_ref,
    key_step_ref,
    key_weight_ref,
    key_copy_ref,
    update_ref,
):
    core, half, row = place_ref[0], place_ref[1], place_ref[2]
    rows, _, count, width = ratio_ref.shape
    own_rows = query_step_ref.shape[0]
    ranks = rows * count
    outs = (
        (query_master_ref, query_step_ref, query_weight_ref, query_copy_ref),
        (key_master_ref, key_step_ref, key_weight_ref, key_copy_ref),
    )

    def whole(first_ref, second_ref, k):
        upto = rows // 2
        first = ratio_ref[pl.ds(half * upto, upto), k].reshape(ranks // 2, width)
        second = ratio_ref[pl.ds((1 - half) * upto, upto), k].reshape(ranks // 2, width)

        def some(i, total):
            span = pl.ds(pl.multiple_of(i * BLOCK, BLOCK), BLOCK)
            update = jnp.dot(first_ref[span, :], first, preferred_element_type=F32)
            update += jnp.dot(second_ref[span, :], second, preferred_element_type=F32)
            update_ref[k, span, :] = update
            return total + jnp.sum((update * update).reshape(BLOCK // 8, 8, width), axis=0)

        return lax.fori_loop(0, D // BLOCK, some, jnp.zeros((8, width), F32))

    for k in range(2):
        total = lax.cond(
            core == k,
            lambda: whole(own_a_ref, own_b_ref, k),
            lambda: whole(other_a_ref, other_b_ref, k),
        )
        scale = 1.0 / jnp.sqrt(jnp.sum(total, keepdims=True) / (D * HD) + norm_floor)
        master_ref, step_ref, weight_ref, copy_ref = outs[k]

        def some(i, carry):
            span = pl.ds(pl.multiple_of(i * own_rows, own_rows), own_rows)
            step = update_ref[k, span, :] * scale
            copy_ref[span, :] = (masters_ref[i, k].astype(F32) - step_rate * step).astype(BF)
            return carry

        lax.fori_loop(0, D // own_rows, some, 0)
        span = pl.ds(pl.multiple_of(row * own_rows, own_rows), own_rows)
        step = update_ref[k, span, :] * scale
        step_ref[...] = step
        weight_ref[...] = master_ref[...] - step_rate * step


def finish(place, ratio, own_a, own_b, other_a, other_b, masters, query_master, key_master):
    own_rows, width = query_master.shape
    mine = jax.ShapeDtypeStruct((own_rows, width), F32)
    copied = jax.ShapeDtypeStruct((D, width), BF)
    return pl.pallas_call(
        finish_kernel,
        out_shape=(mine, mine, copied) * 2,
        in_specs=[pl.BlockSpec(memory_space=pltpu.SMEM)] + [pl.BlockSpec(memory_space=pltpu.VMEM)] * 8,
        scratch_shapes=[pltpu.VMEM((2, D, width), F32)],
        compiler_params=VMEM,
        name="finish",
    )(place, ratio, own_a, own_b, other_a, other_b, masters, query_master, key_master)


def body(
    saved_input,
    query_cot,
    key_cot,
    query_master,
    key_master,
    query_basis,
    key_basis,
    query_first,
    query_second,
    key_first,
    key_second,
):
    rows = lax.axis_size(FS)
    depth = lax.axis_size("z")
    tokens, width = query_cot.shape
    low_count = query_first.shape[0]
    ranks = query_basis.shape[1]
    pairs = depth // 2
    share = tokens // pairs
    core = lax.axis_index("c")
    half = lax.axis_index("z") % 2
    place = jnp.stack([core, half, lax.axis_index(FS)]).astype(jnp.int32)
    first_core = core == 0

    pieces = saved_input.reshape(pairs, 1, share, width)
    pieces = jnp.broadcast_to(pieces, (pairs, 2, share, width)).reshape(depth, share, width)
    pieces = lax.all_to_all(pieces, "z", 0, 0, tiled=True)
    own_basis = jnp.where(first_core, query_basis, key_basis)
    own_half = jnp.where(half == 0, own_basis[:, : ranks // 2], own_basis[:, ranks // 2 :])
    basis = sent_to_all(own_half, FS)
    other_pieces = swapped(pieces, "c")
    own_cot = jnp.where(first_core, query_cot, key_cot)
    other_cot = swapped(jnp.where(first_core, key_cot, query_cot), "c")
    low = product(place, pieces, other_pieces, basis)
    low = lax.all_gather(low, "z", axis=0, tiled=True)
    low = low.reshape(pairs, 2, share, ranks // 2)
    masters = sent_to_all(jnp.stack([query_master, key_master]).astype(BF), FS)

    partial = partials(place, low, own_cot, other_cot, rows, low_count)
    partial = partial.reshape(2 * rows, low_count, width)
    partial = lax.all_to_all(partial, (*FS, "c"), 0, 0, tiled=True)
    projected = jnp.sum(partial.reshape(rows, 2, low_count, width).astype(F32), axis=0)
    firsts = jnp.stack([query_first, key_first])
    seconds = jnp.stack([query_second, key_second])
    first_new = moment_decay * firsts + (1.0 - moment_decay) * projected
    second_new = square_decay * seconds + (1.0 - square_decay) * projected * projected
    ratio = (first_new / jnp.sqrt(second_new + square_floor)).astype(BF)
    ratio = sent_to_all(ratio, FS).reshape(rows, 2, low_count, width)

    basis = basis.reshape(D, ranks // 2)
    pair_basis = swapped(basis, "z")
    other_basis = swapped(basis, "c")
    other_pair_basis = swapped(pair_basis, "c")
    query_step, query_weight, query_copy, key_step, key_weight, key_copy = finish(
        place,
        ratio,
        basis,
        pair_basis,
        other_basis,
        other_pair_basis,
        masters.reshape(rows, 2, -1, width),
        query_master,
        key_master,
    )
    return (
        query_step,
        query_weight,
        query_copy,
        first_new[0],
        second_new[0],
        key_step,
        key_weight,
        key_copy,
        first_new[1],
        second_new[1],
    )


def solution(mesh):
    torus = Mesh(mesh.devices.reshape(4, 4, 16, 2), ("y", "x", "z", "c"))
    tp = ("z", "c")
    split = P(FS, tp)
    rows = P(FS, None)
    copied = P(None, tp)
    in_specs = (split,) * 5 + (rows,) * 2 + (split,) * 4
    out_specs = (split, split, copied, split, split) * 2

    return jax.shard_map(body, mesh=torus, in_specs=in_specs, out_specs=out_specs, check_vma=False)
```

time: 193 us -> 177 us (0.917)
  blocking collectives: 49.3 us -> 31 us
  starting transfers between devices: 46.1 us -> 64.2 us
  local copies, waits for them, and re-layouts: 20.6 us -> 6.86 us
  matrix products: 13.3 us -> 0 us
  Pallas kernels: 0 us -> 10.6 us
  waiting for transfers between devices: 54.9 us -> 60.1 us
  other arithmetic: 6.05 us -> 2.55 us
    all_to_all x4 -> x3, waiting for transfers between devices: 34.7 us -> 8.46 us  [sent_to_all(): lax.all_to_all(jnp.broadcast_to(x[None], (count, *x.shape)), axis, 0, 0,...]
    ppermute x0 -> x5, waiting for transfers between devices: none -> 22 us  [swapped(): return lax.ppermute(x, axis, [(i, i ^ 1) for i in range(count)])]
    ppermute x0 -> x5, starting transfers between devices: none -> 18.6 us  [swapped(): return lax.ppermute(x, axis, [(i, i ^ 1) for i in range(count)])]
    dot_general x7 -> x0, matrix products: 13.3 us -> none  [the longest x2 7.63 us: body(): update = jnp.dot(bases[k], ratio[k], preferred_element_type=jnp.float32)]
    all_to_all x1 -> x0, blocking collectives: 10.6 us -> none  [body(): lax.all_to_all(jnp.stack([query_cot, key_cot]), 'c', 0, 0, tiled=True)]
    pallas_call x0 -> x3, Pallas kernels: none -> 10.6 us  [the longest x1 7.93 us: finish(): pl.pallas_call(finish_kernel, out_shape=(mine, mine, copied) * 2, in_spec...]
    all_gather x1 -> x0, blocking collectives: 8.28 us -> none  [body(): pieces = lax.all_gather(pieces, 'c', axis=0, tiled=False)]
    all_to_all x1, waiting for transfers between devices: 14 us -> 22 us  [body(): pieces = lax.all_to_all(pieces, 'z', 0, 0, tiled=True)]
  transfers between devices with their start and end apart: 6 -> 10, of which waited for: 5 -> 6; matrix products, arithmetic and copies ran while one was open for 6% -> 3% of each run, Pallas kernels for 0% -> 1%
where the time goes in v2:
time: 177 us; the launch traced here: 176 us
  starting transfers between devices  64.2 us (36%)
  waiting for transfers between devices  60.1 us (34%)
  blocking collectives  31 us (18%)
  Pallas kernels  10.6 us (6%)
  local copies, waits for them, and re-layouts  6.86 us (4%)
  other arithmetic  2.55 us (1%)
    all_gather x1, blocking collectives, body(): low = lax.all_gather(low, 'z', axis=0, tiled=True)  31 us
    ppermute x5, waiting for transfers between devices, swapped(): return lax.ppermute(x, axis, [(i, i ^ 1) for i in range(count)])  22 us
    all_to_all x1, waiting for transfers between devices, body(): pieces = lax.all_to_all(pieces, 'z', 0, 0, tiled=True)  22 us
    ppermute x5, starting transfers between devices, swapped(): return lax.ppermute(x, axis, [(i, i ^ 1) for i in range(count)])  18.6 us
    all_to_all x1, starting transfers between devices, body(): pieces = lax.all_to_all(pieces, 'z', 0, 0, tiled=True)  15.7 us
    all_to_all x3, starting transfers between devices, sent_to_all(): lax.all_to_all(jnp.broadcast_to(x[None], (count, *x.shape)), axis, 0, 0,...  15.7 us
    all_to_all x1, starting transfers between devices, body(): partial = lax.all_to_all(partial, (*FS, 'c'), 0, 0, tiled=True)  14.2 us
    all_to_all x3, waiting for transfers between devices, sent_to_all(): lax.all_to_all(jnp.broadcast_to(x[None], (count, *x.shape)), axis, 0, 0,...  8.46 us
  transfers between devices with their start and end apart: 10, of which 6 were waited for; matrix products, arithmetic and copies ran while one was open for 3% of the time, Pallas kernels for 1%

profile of v2, /device:TPU:1, one launch (start us, length us, event | category | flops | bytes accessed | tf_op | source)
XLA Modules:
  0.0 176.1 jit_solution(2639583859580251543)
XLA Ops:
  0.6 1.8 %broadcast_in_dim.11 = bf16[8,2,128,128]{3,2,1,0:T(8,128)(2,1)} broadcast(bf16[8,128,128]{2,1,0:T(8,128)(2,1)} %bitcast.33), dimensions={0,2,3} | broadcast | bytes 786432 | tf_op jit(solution)/shard_map/broadcast_in_dim | solution.py:191
  2.5 15.7 %all-to-all-start = ((bf16[16,128,128]{2,1,0:T(8,128)(2,1)}), bf16[16,128,128]{2,1,0:T(8,128)(2,1)S(1)}, u32[]{:S(2)}, u32[]{:S(2)}) async-start(bf16[16,128,128]{2,1,0:T(8,128)(2,1)} %bitcast.6), calls=%async_computation | async-start | bytes 1048576 | tf_op jit(solution)/shard_map/all_to_all | solution.py:192
  18.2 0.0 copy-start.2
  18.2 0.0 copy-start.3
  18.3 1.0 broadcast_select_fusion.2
  19.3 22.0 %all-to-all-done.own_ref = bf16[16,128,128]{2,1,0:T(8,128)(2,1)S(1)} async-done(((bf16[16,128,128]{2,1,0:T(8,128)(2,1)}), bf16[16,128,128]{2,1,0:T(8,128)(2,1)S(1)}, u32[]{:S(2)}, u32[]{:S(2)}) %all-to-all-start) | async-done | bytes 524320 | tf_op jit(solution)/shard_map/all_to_all | solution.py:192
  41.2 1.2 broadcast_in_dim.12
  42.4 6.8 %all-to-all-start.1 = ((bf16[16,256,128]{2,1,0:T(8,128)(2,1)}), bf16[16,256,128]{2,1,0:T(8,128)(2,1)S(1)}, u32[]{:S(2)}, u32[]{:S(2)}) async-start(bf16[16,256,128]{2,1,0:T(8,128)(2,1)} %broadcast_in_dim.12), calls=%async_computation.1 | async-start | bytes 2097152 | tf_op jit(solution)/shard_map/all_to_all | solution.py:27
  49.2 9.2 %collective-permute-start = (bf16[16,128,128]{2,1,0:T(8,128)(2,1)S(1)}, bf16[16,128,128]{2,1,0:T(8,128)(2,1)S(1)}, u32[]{:S(2)}, u32[]{:S(2)}) collective-permute-start(bf16[16,128,128]{2,1,0:T(8,128)(2,1)S(1)} %all-to-all-done.own_ref), channel_id=1, source_target_pairs={{0,1},{1,0},{2,3},{3,2},{4,5},{5,4},{6,7},{7,6},{8,9},{9,8},{10,11... | collective-permute-start | bytes 1572872 | tf_op jit(solution)/shard_map/ppermute | solution.py:32
  58.4 0.0 copy-done.2
  58.4 0.0 copy-done.3
  58.4 0.1 broadcast_select_fusion
  58.5 0.0 copy-start
  58.5 0.0 copy-start.1
  58.5 2.1 %collective-permute-start.1 = (bf16[1024,128]{1,0:T(8,128)(2,1)S(1)}, bf16[1024,128]{1,0:T(8,128)(2,1)S(1)}, u32[]{:S(2)}, u32[]{:S(2)}) collective-permute-start(bf16[1024,128]{1,0:T(8,128)(2,1)S(1)} %get-tuple-element.25), channel_id=1, source_target_pairs={{0,1},{1,0},{2,3},{3,2},{4,5},{5,4},{6,7},{7,6},{8,9},{9,8},{10,11... | collective-permute-start | bytes 786440 | tf_op jit(solution)/shard_map/ppermute | solution.py:32
  60.6 0.1 pad_add_fusion.core_ref.place_ref
  60.6 0.8 all-to-all-done.1
  61.5 0.0 collective-permute-done.other_ref
  61.5 1.0 product.1
  62.4 31.0 %all_gather.3 = bf16[2048,128]{1,0:T(8,128)(2,1)S(1)} all-gather(bf16[128,128]{1,0:T(8,128)(2,1)S(1)} %product.1), channel_id=1, replica_groups=mesh['y'=4,'x'=4,'z'=16,'c'=2] {'z'}, dimensions={0}, use_global_device_ids=true | all-gather | bytes 557056 | tf_op jit(solution)/shard_map/all_gather | solution.py:200
  93.4 0.0 collective-permute-done.1.other_ref
  93.4 1.7 partials.1
  95.1 14.2 %all-to-all-start.2 = ((bf16[32,16,128]{2,1,0:T(8,128)(2,1)}), bf16[32,16,128]{2,1,0:T(8,128)(2,1)S(1)}, u32[]{:S(2)}, u32[]{:S(2)}) async-start(bf16[32,16,128]{2,1,0:T(8,128)(2,1)} %bitcast.9), calls=%async_computation.2 | async-start | bytes 262144 | tf_op jit(solution)/shard_map/all_to_all | solution.py:206
  109.3 0.0 copy-done
  109.3 0.0 copy-done.1
  109.3 7.6 %all-to-all-done.2 = bf16[32,16,128]{2,1,0:T(8,128)(2,1)S(1)} async-done(((bf16[32,16,128]{2,1,0:T(8,128)(2,1)}), bf16[32,16,128]{2,1,0:T(8,128)(2,1)S(1)}, u32[]{:S(2)}, u32[]{:S(2)}) %all-to-all-start.2) | async-done | bytes 131104 | tf_op jit(solution)/shard_map/all_to_all | solution.py:206
  117.0 1.8 %broadcast_in_dim.14 = bf16[16,2,256,128]{3,2,1,0:T(8,128)(2,1)} broadcast(bf16[2,256,128]{2,1,0:T(8,128)(2,1)S(1)} %pad_maximum_fusion), dimensions={1,2,3} | broadcast | bytes 2228224 | tf_op jit(solution)/shard_map/broadcast_in_dim | solution.py:27
  118.8 0.0 copy-start.4
  118.8 4.6 %all-to-all-start.4 = ((bf16[16,2,256,128]{3,2,1,0:T(8,128)(2,1)}), bf16[16,2,256,128]{3,2,1,0:T(8,128)(2,1)}, u32[]{:S(2)}, u32[]{:S(2)}) async-start(bf16[16,2,256,128]{3,2,1,0:T(8,128)(2,1)} %broadcast_in_dim.14), calls=%async_computation.4 | async-start | bytes 4194304 | tf_op jit(solution)/shard_map/all_to_all | solution.py:27
  123.3 1.9 %collective-permute-start.2 = (bf16[4096,128]{1,0:T(8,128)(2,1)S(1)}, bf16[4096,128]{1,0:T(8,128)(2,1)S(1)}, u32[]{:S(2)}, u32[]{:S(2)}) collective-permute-start(bf16[4096,128]{1,0:T(8,128)(2,1)S(1)} %bitcast.28), channel_id=1, source_target_pairs={{0,2},{2,0},{4,6},{6,4},{8,10},{10,8},{12,14},{14,12},{16,18},{18,... | collective-permute-start | bytes 3145736 | tf_op jit(solution)/shard_map/ppermute | solution.py:32
  125.3 2.3 %collective-permute-start.3 = (bf16[4096,128]{1,0:T(8,128)(2,1)S(1)}, bf16[4096,128]{1,0:T(8,128)(2,1)S(1)}, u32[]{:S(2)}, u32[]{:S(2)}) collective-permute-start(bf16[4096,128]{1,0:T(8,128)(2,1)S(1)} %bitcast.29), channel_id=1, source_target_pairs={{0,1},{1,0},{2,3},{3,2},{4,5},{5,4},{6,7},{7,6},{8,9},{9,8},{10,11... | collective-permute-start | bytes 3145736 | tf_op jit(solution)/shard_map/ppermute | solution.py:32
  127.6 22.0 %collective-permute-done.2.own_b_ref = bf16[4096,128]{1,0:T(8,128)(2,1)S(1)} collective-permute-done((bf16[4096,128]{1,0:T(8,128)(2,1)S(1)}, bf16[4096,128]{1,0:T(8,128)(2,1)S(1)}, u32[]{:S(2)}, u32[]{:S(2)}) %collective-permute-start.2) | collective-permute-done | bytes 1048608 | tf_op jit(solution)/shard_map/ppermute | solution.py:32
  149.6 3.1 %collective-permute-start.4 = (bf16[4096,128]{1,0:T(8,128)(2,1)S(1)}, bf16[4096,128]{1,0:T(8,128)(2,1)}, u32[]{:S(2)}, u32[]{:S(2)}) collective-permute-start(bf16[4096,128]{1,0:T(8,128)(2,1)S(1)} %collective-permute-done.2.own_b_ref), channel_id=1, source_target_pairs={{0,1},{1,0},{2,3},{3,2},{4,5},{5,4},{6,7},{7,6},{8,9},{9,8},{10,11... | collective-permute-start | bytes 3145736 | tf_op jit(solution)/shard_map/ppermute | solution.py:32
  152.7 0.0 copy-done.4
  152.8 1.4 multiply_convert_fusion
  154.1 2.2 %all-to-all-done.4.masters_ref = bf16[16,2,256,128]{3,2,1,0:T(8,128)(2,1)} async-done(((bf16[16,2,256,128]{3,2,1,0:T(8,128)(2,1)}), bf16[16,2,256,128]{3,2,1,0:T(8,128)(2,1)}, u32[]{:S(2)}, u32[]{:S(2)}) %all-to-all-start.4) | async-done | bytes 2097184 | tf_op jit(solution)/shard_map/all_to_all | solution.py:27
  156.3 0.7 broadcast_in_dim.13
  156.9 4.4 %all-to-all-start.3 = ((bf16[16,2,16,128]{3,2,1,0:T(8,128)(2,1)}), bf16[16,2,16,128]{3,2,1,0:T(8,128)(2,1)S(1)}, u32[]{:S(2)}, u32[]{:S(2)}) async-start(bf16[16,2,16,128]{3,2,1,0:T(8,128)(2,1)} %broadcast_in_dim.13), calls=%async_computation.3 | async-start | bytes 262144 | tf_op jit(solution)/shard_map/all_to_all | solution.py:27
  161.3 1.4 slice_bitcast_fusion
  162.7 0.0 collective-permute-done.3.other_a_ref
  162.7 5.5 %all-to-all-done.3.ratio_ref = bf16[16,2,16,128]{3,2,1,0:T(8,128)(2,1)S(1)} async-done(((bf16[16,2,16,128]{3,2,1,0:T(8,128)(2,1)}), bf16[16,2,16,128]{3,2,1,0:T(8,128)(2,1)S(1)}, u32[]{:S(2)}, u32[]{:S(2)}) %all-to-all-start.3) | async-done | bytes 131104 | tf_op jit(solution)/shard_map/all_to_all | solution.py:27
  168.2 0.0 collective-permute-done.4.other_b_ref
  168.2 7.9 %finish.1 = (f32[256,128]{1,0:T(8,128)}, f32[256,128]{1,0:T(8,128)}, bf16[4096,128]{1,0:T(8,128)(2,1)}, f32[256,128]{1,0:T(8,128)}, f32[256,128]{1,0:T(8,128)}, /*index=5*/bf16[4096,128]{1,0:T(8,128)(2,1)}) custom-call(s32[3]{0:T(128)S(1)} %pad_add_fusion.core_ref.place_ref, bf16[16,2,16,128]{3,2,1,0:T(8,128)(2,1)S(1)} %all-to-all-done.3.ratio_ref, ...), custom_call_target="tpu_custom_call" | custom-call | tf_op jit(solution)/shard_map/finish/pallas_call | solution.py:155
  (4 shorter events, 0.1 us)
Async XLA Ops:
  2.5 38.7 %all-to-all-start = ((bf16[16,128,128]{2,1,0:T(8,128)(2,1)}), bf16[16,128,128]{2,1,0:T(8,128)(2,1)S(1)}, u32[]{:S(2)}, u32[]{:S(2)}) async-start(bf16[16,128,128]{2,1,0:T(8,128)(2,1)} %bitcast.6), calls=%async_computation | async-start | bytes 1048576 | tf_op jit(solution)/shard_map/all_to_all | solution.py:192
  18.2 40.2 %copy-start.2 = (bf16[1024,128]{1,0:T(8,128)(2,1)S(1)}, bf16[1024,128]{1,0:T(8,128)(2,1)}, u32[]{:S(2)}) copy-start(bf16[1024,128]{1,0:T(8,128)(2,1)} %param.13) | copy-start | bytes 786436
  18.2 40.2 %copy-start.3 = (bf16[1024,128]{1,0:T(8,128)(2,1)S(1)}, bf16[1024,128]{1,0:T(8,128)(2,1)}, u32[]{:S(2)}) copy-start(bf16[1024,128]{1,0:T(8,128)(2,1)} %param.12) | copy-start | bytes 786436
  42.4 19.1 %all-to-all-start.1 = ((bf16[16,256,128]{2,1,0:T(8,128)(2,1)}), bf16[16,256,128]{2,1,0:T(8,128)(2,1)S(1)}, u32[]{:S(2)}, u32[]{:S(2)}) async-start(bf16[16,256,128]{2,1,0:T(8,128)(2,1)} %broadcast_in_dim.12), calls=%async_computation.1 | async-start | bytes 2097152 | tf_op jit(solution)/shard_map/all_to_all | solution.py:27
  49.2 12.3 %collective-permute-start = (bf16[16,128,128]{2,1,0:T(8,128)(2,1)S(1)}, bf16[16,128,128]{2,1,0:T(8,128)(2,1)S(1)}, u32[]{:S(2)}, u32[]{:S(2)}) collective-permute-start(bf16[16,128,128]{2,1,0:T(8,128)(2,1)S(1)} %all-to-all-done.own_ref), channel_id=1, source_target_pairs={{0,1},{1,0},{2,3},{3,2},{4,5},{5,4},{6,7},{7,6},{8,9},{9,8},{10,11... | collective-permute-start | bytes 1572872 | tf_op jit(solution)/shard_map/ppermute | solution.py:32
  58.5 50.8 %copy-start = (f32[256,128]{1,0:T(8,128)S(1)}, f32[256,128]{1,0:T(8,128)}, u32[]{:S(2)}) copy-start(f32[256,128]{1,0:T(8,128)} %key_master_ref.1) | copy-start | bytes 393220
  58.5 50.8 %copy-start.1 = (f32[256,128]{1,0:T(8,128)S(1)}, f32[256,128]{1,0:T(8,128)}, u32[]{:S(2)}) copy-start(f32[256,128]{1,0:T(8,128)} %query_master_ref.1) | copy-start | bytes 393220
  58.5 34.9 %collective-permute-start.1 = (bf16[1024,128]{1,0:T(8,128)(2,1)S(1)}, bf16[1024,128]{1,0:T(8,128)(2,1)S(1)}, u32[]{:S(2)}, u32[]{:S(2)}) collective-permute-start(bf16[1024,128]{1,0:T(8,128)(2,1)S(1)} %get-tuple-element.25), channel_id=1, source_target_pairs={{0,1},{1,0},{2,3},{3,2},{4,5},{5,4},{6,7},{7,6},{8,9},{9,8},{10,11... | collective-permute-start | bytes 786440 | tf_op jit(solution)/shard_map/ppermute | solution.py:32
  95.1 21.9 %all-to-all-start.2 = ((bf16[32,16,128]{2,1,0:T(8,128)(2,1)}), bf16[32,16,128]{2,1,0:T(8,128)(2,1)S(1)}, u32[]{:S(2)}, u32[]{:S(2)}) async-start(bf16[32,16,128]{2,1,0:T(8,128)(2,1)} %bitcast.9), calls=%async_computation.2 | async-start | bytes 262144 | tf_op jit(solution)/shard_map/all_to_all | solution.py:206
  118.8 34.0 %copy-start.4 = (f32[16,128]{1,0:T(8,128)S(1)}, f32[16,128]{1,0:T(8,128)}, u32[]{:S(2)}) copy-start(f32[16,128]{1,0:T(8,128)} %param.21) | copy-start | bytes 24580
  118.8 37.5 %all-to-all-start.4 = ((bf16[16,2,256,128]{3,2,1,0:T(8,128)(2,1)}), bf16[16,2,256,128]{3,2,1,0:T(8,128)(2,1)}, u32[]{:S(2)}, u32[]{:S(2)}) async-start(bf16[16,2,256,128]{3,2,1,0:T(8,128)(2,1)} %broadcast_in_dim.14), calls=%async_computation.4 | async-start | bytes 4194304 | tf_op jit(solution)/shard_map/all_to_all | solution.py:27
  123.3 26.2 %collective-permute-start.2 = (bf16[4096,128]{1,0:T(8,128)(2,1)S(1)}, bf16[4096,128]{1,0:T(8,128)(2,1)S(1)}, u32[]{:S(2)}, u32[]{:S(2)}) collective-permute-start(bf16[4096,128]{1,0:T(8,128)(2,1)S(1)} %bitcast.28), channel_id=1, source_target_pairs={{0,2},{2,0},{4,6},{6,4},{8,10},{10,8},{12,14},{14,12},{16,18},{18,... | collective-permute-start | bytes 3145736 | tf_op jit(solution)/shard_map/ppermute | solution.py:32
  125.3 37.4 %collective-permute-start.3 = (bf16[4096,128]{1,0:T(8,128)(2,1)S(1)}, bf16[4096,128]{1,0:T(8,128)(2,1)S(1)}, u32[]{:S(2)}, u32[]{:S(2)}) collective-permute-start(bf16[4096,128]{1,0:T(8,128)(2,1)S(1)} %bitcast.29), channel_id=1, source_target_pairs={{0,1},{1,0},{2,3},{3,2},{4,5},{5,4},{6,7},{7,6},{8,9},{9,8},{10,11... | collective-permute-start | bytes 3145736 | tf_op jit(solution)/shard_map/ppermute | solution.py:32
  149.6 18.6 %collective-permute-start.4 = (bf16[4096,128]{1,0:T(8,128)(2,1)S(1)}, bf16[4096,128]{1,0:T(8,128)(2,1)}, u32[]{:S(2)}, u32[]{:S(2)}) collective-permute-start(bf16[4096,128]{1,0:T(8,128)(2,1)S(1)} %collective-permute-done.2.own_b_ref), channel_id=1, source_target_pairs={{0,1},{1,0},{2,3},{3,2},{4,5},{5,4},{6,7},{7,6},{8,9},{9,8},{10,11... | collective-permute-start | bytes 3145736 | tf_op jit(solution)/shard_map/ppermute | solution.py:32
  156.9 11.2 %all-to-all-start.3 = ((bf16[16,2,16,128]{3,2,1,0:T(8,128)(2,1)}), bf16[16,2,16,128]{3,2,1,0:T(8,128)(2,1)S(1)}, u32[]{:S(2)}, u32[]{:S(2)}) async-start(bf16[16,2,16,128]{3,2,1,0:T(8,128)(2,1)} %broadcast_in_dim.13), calls=%async_computation.3 | async-start | bytes 262144 | tf_op jit(solution)/shard_map/all_to_all | solution.py:27

commit v3 on v2

v3 whole, which is shorter than its diff:
```python
import jax
import jax.numpy as jnp
from jax import lax
from jax.experimental import pallas as pl
from jax.experimental.pallas import tpu as pltpu
from jax.sharding import Mesh
from jax.sharding import PartitionSpec as P


D = 4096
HD = 128
FS = ("y", "x")
BF = jnp.bfloat16
F32 = jnp.float32

moment_decay = 0.8
square_decay = 0.9
square_floor = 1.0
norm_floor = 0.01
step_rate = 0.01

VMEM = pltpu.CompilerParams(vmem_limit_bytes=48 * 1024 * 1024)


def sent_to_all(x, axis):
    count = lax.axis_size(axis)
    return lax.all_to_all(jnp.broadcast_to(x[None], (count, *x.shape)), axis, 0, 0, tiled=True)


def swapped(x, axis):
    count = lax.axis_size(axis)
    return lax.ppermute(x, axis, [(i, i ^ 1) for i in range(count)])


def product_kernel(core_ref, own_ref, other_ref, top_ref, rest_ref, out_ref):
    core = core_ref[0]
    cut = top_ref.shape[1]
    first = core == 0

    def some(z, total):
        own, other = own_ref[z], other_ref[z]
        left = jnp.where(first, own, other)
        right = jnp.where(first, other, own)
        total += jnp.dot(left[:, :cut], top_ref[z], preferred_element_type=F32)
        both = jnp.concatenate([left[:, cut:], right], axis=1)
        return total + jnp.dot(both, rest_ref[z], preferred_element_type=F32)

    total = lax.fori_loop(0, own_ref.shape[0], some, jnp.zeros(out_ref.shape, F32), unroll=4)
    out_ref[...] = total.astype(out_ref.dtype)


def product(core, own, other, top, rest):
    return pl.pallas_call(
        product_kernel,
        out_shape=jax.ShapeDtypeStruct((own.shape[1], top.shape[-1]), BF),
        in_specs=[pl.BlockSpec(memory_space=pltpu.SMEM)] + [pl.BlockSpec(memory_space=pltpu.VMEM)] * 4,
        compiler_params=VMEM,
        name="product",
    )(core, own, other, top, rest)


def partial_kernel(core_ref, low_ref, own_ref, other_ref, out_ref):
    core = core_ref[0]
    rows, _, count, width = out_ref.shape
    contract = (((0,), (0,)), ((), ()))
    mine = lax.dot_general(low_ref[...], own_ref[...], contract, preferred_element_type=F32)
    theirs = lax.dot_general(low_ref[...], other_ref[...], contract, preferred_element_type=F32)
    out_ref[:, core] = mine.reshape(rows, count, width).astype(out_ref.dtype)
    out_ref[:, 1 - core] = theirs.reshape(rows, count, width).astype(out_ref.dtype)


def partials(core, low, own, other, rows, count):
    return pl.pallas_call(
        partial_kernel,
        out_shape=jax.ShapeDtypeStruct((rows, 2, count, own.shape[-1]), BF),
        in_specs=[pl.BlockSpec(memory_space=pltpu.SMEM)] + [pl.BlockSpec(memory_space=pltpu.VMEM)] * 3,
        compiler_params=VMEM,
        name="partials",
    )(core, low, own, other)


GROUP = 4


def finish_kernel(
    place_ref,
    ratio_ref,
    own_top_ref,
    own_rest_ref,
    other_top_hbm,
    other_rest_hbm,
    masters_hbm,
    query_master_ref,
    key_master_ref,
    query_step_ref,
    query_weight_ref,
    query_copy_hbm,
    key_step_ref,
    key_weight_ref,
    key_copy_hbm,
    other_top_ref,
    other_rest_ref,
    masters_ref,
    update_top_ref,
    update_rest_ref,
    copies_ref,
    scales_ref,
    arrived,
    left,
):
    core, row = place_ref[0], place_ref[1]
    rows, _, count, width = ratio_ref.shape
    ranks = rows * count
    top, rest = own_top_ref.shape[1], own_rest_ref.shape[1]
    tops, rests = pl.ds(0, top), pl.ds(top, rest)
    incoming = [
        pltpu.make_async_copy(other_top_hbm, other_top_ref, arrived.at[0]),
        pltpu.make_async_copy(other_rest_hbm, other_rest_ref, arrived.at[1]),
        pltpu.make_async_copy(masters_hbm, masters_ref, arrived.at[2]),
    ]
    outgoing = [
        pltpu.make_async_copy(copies_ref.at[0], query_copy_hbm, left.at[0]),
        pltpu.make_async_copy(copies_ref.at[1], key_copy_hbm, left.at[1]),
    ]
    for copy in incoming:
        copy.start()

    def whole(top_ref, rest_ref, k):
        ratio = ratio_ref[:, k].reshape(ranks, width)

        def some(i, total):
            span = pl.ds(i * GROUP, GROUP)
            for part_ref, update_ref, size in ((top_ref, update_top_ref, top), (rest_ref, update_rest_ref, rest)):
                part = part_ref[span].reshape(GROUP * size, ranks)
                update = jnp.dot(part, ratio, preferred_element_type=F32)
                update_ref[k, span] = update.reshape(GROUP, size, width)
                total += jnp.sum((update * update).reshape(GROUP * size // 8, 8, width), axis=0)
            return total

        total = lax.fori_loop(0, rows // GROUP, some, jnp.zeros((8, width), F32))
        scale = 1.0 / jnp.sqrt(jnp.sum(total, keepdims=True) / (D * HD) + norm_floor)
        scales_ref[k] = jnp.broadcast_to(scale, (8, width))

    def copied(k):
        scale = scales_ref[k][:1]

        def some(f, carry):
            step = update_top_ref[k, f] * scale
            copies_ref[k, f, tops, :] = (masters_ref[f, k, tops, :].astype(F32) - step_rate * step).astype(BF)
            step = update_rest_ref[k, f] * scale
            copies_ref[k, f, rests, :] = (masters_ref[f, k, rests, :].astype(F32) - step_rate * step).astype(BF)
            return carry

        lax.fori_loop(0, rows, some, 0)
        for n in range(2):
            pl.when(k == n)(outgoing[n].start)

    whole(own_top_ref, own_rest_ref, core)
    incoming[2].wait()
    copied(core)
    incoming[0].wait()
    incoming[1].wait()
    whole(other_top_ref, other_rest_ref, 1 - core)
    copied(1 - core)
    outs = (
        (query_master_ref, query_step_ref, query_weight_ref),
        (key_master_ref, key_step_ref, key_weight_ref),
    )
    for k, (master_ref, step_ref, weight_ref) in enumerate(outs):
        scale = scales_ref[k][:1]
        for span, update_ref in ((tops, update_top_ref), (rests, update_rest_ref)):
            step = update_ref[k, row] * scale
            step_ref[span, :] = step
            weight_ref[span, :] = master_ref[span, :] - step_rate * step
    for copy in outgoing:
        copy.wait()


def finish(place, ratio, own_top, own_rest, other_top, other_rest, masters, query_master, key_master):
    own_rows, width = query_master.shape
    rows = ratio.shape[0]
    top, rest = own_top.shape[1], own_rest.shape[1]
    mine = jax.ShapeDtypeStruct((own_rows, width), F32)
    copied = jax.ShapeDtypeStruct((rows, own_rows, width), BF)
    smem, vmem, anywhere = (
        pl.BlockSpec(memory_space=pltpu.SMEM),
        pl.BlockSpec(memory_space=pltpu.VMEM),
        pl.BlockSpec(memory_space=pl.ANY),
    )
    return pl.pallas_call(
        finish_kernel,
        out_shape=(mine, mine, copied) * 2,
        in_specs=[smem, vmem, vmem, vmem, anywhere, anywhere, anywhere, vmem, vmem],
        out_specs=(vmem, vmem, anywhere) * 2,
        scratch_shapes=[
            pltpu.VMEM(other_top.shape, BF),
            pltpu.VMEM(other_rest.shape, BF),
            pltpu.VMEM(masters.shape, BF),
            pltpu.VMEM((2, rows, top, width), F32),
            pltpu.VMEM((2, rows, rest, width), F32),
            pltpu.VMEM((2, rows, own_rows, width), BF),
            pltpu.VMEM((2, 8, width), F32),
            pltpu.SemaphoreType.DMA((3,)),
            pltpu.SemaphoreType.DMA((2,)),
        ],
        compiler_params=VMEM,
        name="finish",
    )(place, ratio, own_top, own_rest, other_top, other_rest, masters, query_master, key_master)


TOP = 112


def body(
    saved_input,
    query_cot,
    key_cot,
    query_master,
    key_master,
    query_basis,
    key_basis,
    query_first,
    query_second,
    key_first,
    key_second,
):
    rows = lax.axis_size(FS)
    depth = lax.axis_size("z")
    tokens, width = query_cot.shape
    low_count = query_first.shape[0]
    ranks = query_basis.shape[1]
    share = tokens // depth
    core = lax.axis_index("c")
    place = jnp.stack([core, lax.axis_index(FS)]).astype(jnp.int32)
    first_core = core == 0

    pieces = lax.all_to_all(saved_input.reshape(depth, share, width), "z", 0, 0, tiled=True)
    own_basis = jnp.where(first_core, query_basis, key_basis)
    top = lax.all_gather(own_basis[:TOP], FS, axis=0, tiled=True).reshape(rows, TOP, ranks)
    rest = sent_to_all(own_basis[TOP:], FS)
    rest = rest.reshape(rows, -1, ranks)
    other_pieces = swapped(pieces, "c")
    own_cot = jnp.where(first_core, query_cot, key_cot)
    other_cot = swapped(jnp.where(first_core, key_cot, query_cot), "c")
    low = product(place, pieces, other_pieces, top, rest)
    low = lax.all_gather(low, "z", axis=0, tiled=True)
    masters = sent_to_all(jnp.stack([query_master, key_master]).astype(BF), FS)

    partial = partials(place, low, own_cot, other_cot, rows, low_count)
    partial = partial.reshape(2 * rows, low_count, width)
    partial = lax.all_to_all(partial, (*FS, "c"), 0, 0, tiled=True)
    projected = jnp.sum(partial.reshape(rows, 2, low_count, width).astype(F32), axis=0)
    firsts = jnp.stack([query_first, key_first])
    seconds = jnp.stack([query_second, key_second])
    first_new = moment_decay * firsts + (1.0 - moment_decay) * projected
    second_new = square_decay * seconds + (1.0 - square_decay) * projected * projected
    ratio = (first_new / jnp.sqrt(second_new + square_floor)).astype(BF)
    ratio = sent_to_all(ratio, FS).reshape(rows, 2, low_count, width)

    other_top = swapped(top, "c")
    other_rest = swapped(rest, "c")
    query_step, query_weight, query_copy, key_step, key_weight, key_copy = finish(
        place,
        ratio,
        top,
        rest,
        other_top,
        other_rest,
        masters.reshape(rows, 2, -1, width),
        query_master,
        key_master,
    )
    return (
        query_step,
        query_weight,
        query_copy.reshape(D, width),
        first_new[0],
        second_new[0],
        key_step,
        key_weight,
        key_copy.reshape(D, width),
        first_new[1],
        second_new[1],
    )


def solution(mesh):
    torus = Mesh(mesh.devices.reshape(4, 4, 16, 2), ("y", "x", "z", "c"))
    tp = ("z", "c")
    split = P(FS, tp)
    rows = P(FS, None)
    copied = P(None, tp)
    in_specs = (split,) * 5 + (rows,) * 2 + (split,) * 4
    out_specs = (split, split, copied, split, split) * 2

    return jax.shard_map(body, mesh=torus, in_specs=in_specs, out_specs=out_specs, check_vma=False)
```

time: 177 us -> 181 us (1.023)
  blocking collectives: 31 us -> 73.3 us
  waiting for transfers between devices: 60.1 us -> 40.8 us
  starting transfers between devices: 64.2 us -> 45.6 us
    all_to_all x0 -> x1, blocking collectives: none -> 22.9 us  [body(): partial = lax.all_to_all(partial, (*FS, 'c'), 0, 0, tiled=True)]
    all_gather x0 -> x1, blocking collectives: none -> 22.4 us  [body(): lax.all_gather(own_basis[:TOP], FS, axis=0, tiled=True)]
    ppermute x5 -> x4, waiting for transfers between devices: 22 us -> 1.08 us  [swapped(): return lax.ppermute(x, axis, [(i, i ^ 1) for i in range(count)])]
    all_to_all x3, waiting for transfers between devices: 8.46 us -> 26.9 us  [sent_to_all(): lax.all_to_all(jnp.broadcast_to(x[None], (count, *x.shape)), axis, 0, 0,...]
    all_to_all x2 -> x1, waiting for transfers between devices: 29.6 us -> 12.8 us  [body(): lax.all_to_all(saved_input.reshape(depth, share, width), 'z', 0, 0, tiled...]
    all_to_all x2 -> x1, starting transfers between devices: 29.9 us -> 15.7 us  [body(): lax.all_to_all(saved_input.reshape(depth, share, width), 'z', 0, 0, tiled...]
    ppermute x5 -> x4, starting transfers between devices: 18.6 us -> 15.1 us  [swapped(): return lax.ppermute(x, axis, [(i, i ^ 1) for i in range(count)])]
    unnamed x10 -> x24, local copies, waits for them, and re-layouts: 0.03 us -> 3.05 us
  transfers between devices with their start and end apart: 10 -> 8, of which waited for: 6 -> 4; matrix products, arithmetic and copies ran while one was open for 3% -> 1% of each run, Pallas kernels for 1% -> 1%
where the time goes in v3:
time: 181 us; the launch traced here: 180 us
  blocking collectives  73.3 us (40%)
  starting transfers between devices  45.6 us (25%)
  waiting for transfers between devices  40.8 us (23%)
  Pallas kernels  9.49 us (5%)
  local copies, waits for them, and re-layouts  8 us (4%)
    all_gather x1, blocking collectives, body(): low = lax.all_gather(low, 'z', axis=0, tiled=True)  28 us
    all_to_all x3, waiting for transfers between devices, sent_to_all(): lax.all_to_all(jnp.broadcast_to(x[None], (count, *x.shape)), axis, 0, 0,...  26.9 us
    all_to_all x1, blocking collectives, body(): partial = lax.all_to_all(partial, (*FS, 'c'), 0, 0, tiled=True)  22.9 us
    all_gather x1, blocking collectives, body(): lax.all_gather(own_basis[:TOP], FS, axis=0, tiled=True)  22.4 us
    all_to_all x1, starting transfers between devices, body(): lax.all_to_all(saved_input.reshape(depth, share, width), 'z', 0, 0, tiled...  15.7 us
    ppermute x4, starting transfers between devices, swapped(): return lax.ppermute(x, axis, [(i, i ^ 1) for i in range(count)])  15.1 us
    all_to_all x3, starting transfers between devices, sent_to_all(): lax.all_to_all(jnp.broadcast_to(x[None], (count, *x.shape)), axis, 0, 0,...  14.8 us
    all_to_all x1, waiting for transfers between devices, body(): lax.all_to_all(saved_input.reshape(depth, share, width), 'z', 0, 0, tiled...  12.8 us
  transfers between devices with their start and end apart: 8, of which 4 were waited for; matrix products, arithmetic and copies ran while one was open for 1% of the time, Pallas kernels for 1%

profile of v3, /device:TPU:1, one launch (start us, length us, event | category | flops | bytes accessed | tf_op | source)
XLA Modules:
  0.0 179.8 jit_solution(1219107730724349875)
XLA Ops:
  0.6 15.7 %all-to-all-start = ((bf16[16,64,128]{2,1,0:T(8,128)(2,1)}), bf16[16,64,128]{2,1,0:T(8,128)(2,1)S(1)}, u32[]{:S(2)}, u32[]{:S(2)}) async-start(bf16[16,64,128]{2,1,0:T(8,128)(2,1)} %bitcast.30), calls=%async_computation | async-start | bytes 524288 | tf_op jit(solution)/shard_map/all_to_all | solution.py:237
  16.4 0.9 broadcast_select_fusion.2
  17.4 12.8 %all-to-all-done.own_ref = bf16[16,64,128]{2,1,0:T(8,128)(2,1)S(1)} async-done(((bf16[16,64,128]{2,1,0:T(8,128)(2,1)}), bf16[16,64,128]{2,1,0:T(8,128)(2,1)S(1)}, u32[]{:S(2)}, u32[]{:S(2)}) %all-to-all-start) | async-done | bytes 262176 | tf_op jit(solution)/shard_map/all_to_all | solution.py:237
  30.2 1.1 broadcast_in_dim.6
  31.3 0.0 copy-start.6
  31.3 0.0 copy-start.7
  31.3 6.9 %all-to-all-start.1 = ((bf16[16,144,256]{2,1,0:T(8,128)(2,1)}), bf16[16,144,256]{2,1,0:T(8,128)(2,1)S(1)}, u32[]{:S(2)}, u32[]{:S(2)}) async-start(bf16[16,144,256]{2,1,0:T(8,128)(2,1)} %broadcast_in_dim.6), calls=%async_computation.1 | async-start | bytes 2359296 | tf_op jit(solution)/shard_map/all_to_all | solution.py:27
  38.2 0.0 copy-done.6
  38.2 0.0 copy-done.7
  38.3 7.8 %collective-permute-start.1 = (bf16[1024,128]{1,0:T(8,128)(2,1)S(1)}, bf16[1024,128]{1,0:T(8,128)(2,1)S(1)}, u32[]{:S(2)}, u32[]{:S(2)}) collective-permute-start(bf16[1024,128]{1,0:T(8,128)(2,1)S(1)} %get-tuple-element.25), channel_id=1, source_target_pairs={{0,1},{1,0},{2,3},{3,2},{4,5},{5,4},{6,7},{7,6},{8,9},{9,8},{10,11... | collective-permute-start | bytes 786440 | tf_op jit(solution)/shard_map/ppermute | solution.py:32
  46.0 1.9 %collective-permute-start = (bf16[16,64,128]{2,1,0:T(8,128)(2,1)S(1)}, bf16[16,64,128]{2,1,0:T(8,128)(2,1)S(1)}, u32[]{:S(2)}, u32[]{:S(2)}) collective-permute-start(bf16[16,64,128]{2,1,0:T(8,128)(2,1)S(1)} %all-to-all-done.own_ref), channel_id=1, source_target_pairs={{0,1},{1,0},{2,3},{3,2},{4,5},{5,4},{6,7},{7,6},{8,9},{9,8},{10,11... | collective-permute-start | bytes 786440 | tf_op jit(solution)/shard_map/ppermute | solution.py:32
  48.0 22.4 %all_gather.6 = bf16[1792,256]{1,0:T(8,128)(2,1)S(1)} all-gather(bf16[112,256]{1,0:T(8,128)(2,1)S(1)} %slice.24), channel_id=1, replica_groups=mesh['y'=4,'x'=4,'z'=16,'c'=2] {'y','x'}, dimensions={0}, use_global_device_ids=true | all-gather | bytes 974848 | tf_op jit(solution)/shard_map/all_gather | solution.py:239
  70.3 0.1 pad_add_fusion.core_ref.place_ref
  70.4 0.0 all-to-all-done.1.rest_ref.own_rest_ref
  70.4 0.0 collective-permute-done.other_ref
  70.4 1.6 product.1
  72.0 0.0 copy-start.8
  72.0 0.0 copy-start.9
  72.0 0.0 copy-start.10
  72.1 0.0 copy-start.11
  72.1 28.0 %all_gather.7.low_ref = bf16[1024,256]{1,0:T(8,128)(2,1)S(1)} all-gather(bf16[64,256]{1,0:T(8,128)(2,1)S(1)} %product.1), channel_id=1, replica_groups=mesh['y'=4,'x'=4,'z'=16,'c'=2] {'z'}, dimensions={0}, use_global_device_ids=true | all-gather | bytes 557056 | tf_op jit(solution)/shard_map/all_gather | solution.py:246
  100.1 0.0 copy-start.2
  100.1 0.0 copy-start.3
  100.1 0.0 collective-permute-done.1.other_ref
  100.1 1.0 partials.1
  101.1 22.9 %all_to_all.25 = bf16[32,16,128]{2,1,0:T(8,128)(2,1)S(1)} all-to-all(bf16[32,16,128]{2,1,0:T(8,128)(2,1)S(1)} %bitcast.28), channel_id=1, replica_groups=mesh['y'=4,'x'=4,'z'=16,'c'=2] {'y','x','c'}, dimensions={0} | all-to-all | bytes 262144 | tf_op jit(solution)/shard_map/all_to_all | solution.py:251
  124.0 0.0 copy-done.8
  124.1 0.0 copy-done.9
  124.1 0.0 copy-done.10
  124.1 0.0 copy-done.11
  124.1 0.6 multiply_convert_fusion
  124.7 0.7 broadcast_in_dim.7
  125.4 3.5 %all-to-all-start.3 = ((bf16[16,2,16,128]{3,2,1,0:T(8,128)(2,1)}), bf16[16,2,16,128]{3,2,1,0:T(8,128)(2,1)S(1)}, u32[]{:S(2)}, u32[]{:S(2)}) async-start(bf16[16,2,16,128]{3,2,1,0:T(8,128)(2,1)} %broadcast_in_dim.7), calls=%async_computation.3 | async-start | bytes 262144 | tf_op jit(solution)/shard_map/all_to_all | solution.py:27
  128.9 0.0 copy-done.2
  128.9 0.0 copy-done.3
  129.0 6.7 %all-to-all-done.3.ratio_ref = bf16[16,2,16,128]{3,2,1,0:T(8,128)(2,1)S(1)} async-done(((bf16[16,2,16,128]{3,2,1,0:T(8,128)(2,1)}), bf16[16,2,16,128]{3,2,1,0:T(8,128)(2,1)S(1)}, u32[]{:S(2)}, u32[]{:S(2)}) %all-to-all-start.3) | async-done | bytes 131104 | tf_op jit(solution)/shard_map/all_to_all | solution.py:27
  135.7 0.0 copy-start.4
  135.7 1.8 broadcast_in_dim.8
  137.5 0.0 copy-done.4
  137.5 4.4 %all-to-all-start.4 = ((bf16[16,2,256,128]{3,2,1,0:T(8,128)(2,1)}), bf16[16,2,256,128]{3,2,1,0:T(8,128)(2,1)}, u32[]{:S(2)}, u32[]{:S(2)}) async-start(bf16[16,2,256,128]{3,2,1,0:T(8,128)(2,1)} %broadcast_in_dim.8), calls=%async_computation.4 | async-start | bytes 4194304 | tf_op jit(solution)/shard_map/all_to_all | solution.py:27
  141.9 3.5 %collective-permute-start.3 = (bf16[16,144,256]{2,1,0:T(8,128)(2,1)S(1)}, bf16[16,144,256]{2,1,0:T(8,128)(2,1)S(1)}, u32[]{:S(2)}, u32[]{:S(2)}) collective-permute-start(bf16[16,144,256]{2,1,0:T(8,128)(2,1)S(1)} %all-to-all-done.1.rest_ref.own_rest_ref), channel_id=1, source_target_pairs={{0,1},{1,0},{2,3},{3,2},{4,5},{5,4},{6,7},{7,6},{8,9},{9,8},{10,11... | collective-permute-start | bytes 3538952 | tf_op jit(solution)/shard_map/ppermute | solution.py:32
  145.4 1.9 %collective-permute-start.2 = (bf16[16,112,256]{2,1,0:T(8,128)(2,1)S(1)}, bf16[16,112,256]{2,1,0:T(8,128)(2,1)S(1)}, u32[]{:S(2)}, u32[]{:S(2)}) collective-permute-start(bf16[16,112,256]{2,1,0:T(8,128)(2,1)S(1)} %bitcast.26), channel_id=1, source_target_pairs={{0,1},{1,0},{2,3},{3,2},{4,5},{5,4},{6,7},{7,6},{8,9},{9,8},{10,11... | collective-permute-start | bytes 2752520 | tf_op jit(solution)/shard_map/ppermute | solution.py:32
  147.3 1.4 slice_bitcast_fusion
  148.7 1.1 collective-permute-done.2.other_top_hbm
  149.8 0.0 copy-start
  149.8 0.9 copy-done
  150.7 20.1 %all-to-all-done.4.masters_hbm = bf16[16,2,256,128]{3,2,1,0:T(8,128)(2,1)} async-done(((bf16[16,2,256,128]{3,2,1,0:T(8,128)(2,1)}), bf16[16,2,256,128]{3,2,1,0:T(8,128)(2,1)}, u32[]{:S(2)}, u32[]{:S(2)}) %all-to-all-start.4) | async-done | bytes 2097184 | tf_op jit(solution)/shard_map/all_to_all | solution.py:27
  170.8 0.0 collective-permute-done.3.other_rest_hbm
  170.8 0.0 copy-start.1
  170.8 1.2 copy-done.1
  172.0 0.0 copy-start.5
  172.0 0.9 copy-done.5
  172.9 6.9 %finish.1 = (f32[256,128]{1,0:T(8,128)}, f32[256,128]{1,0:T(8,128)}, bf16[16,256,128]{2,1,0:T(8,128)(2,1)}, f32[256,128]{1,0:T(8,128)}, f32[256,128]{1,0:T(8,128)}, /*index=5*/bf16[16,256,128]{2,1,0:T(8,128)(2,1)}) custom-call(s32[2]{0:T(128)S(1)} %pad_add_fusion.core_ref.place_ref, bf16[16,2,16,128]{3,2,1,0:T(8,128)(2,1)S(1)} %copy-done.5, ...), custom_call_target="tpu_custom_call" | custom-call | tf_op jit(solution)/shard_map/finish/pallas_call | solution.py:190
  (6 shorter events, 0.1 us)
Async XLA Ops:
  0.6 29.5 %all-to-all-start = ((bf16[16,64,128]{2,1,0:T(8,128)(2,1)}), bf16[16,64,128]{2,1,0:T(8,128)(2,1)S(1)}, u32[]{:S(2)}, u32[]{:S(2)}) async-start(bf16[16,64,128]{2,1,0:T(8,128)(2,1)} %bitcast.30), calls=%async_computation | async-start | bytes 524288 | tf_op jit(solution)/shard_map/all_to_all | solution.py:237
  31.3 6.9 %copy-start.6 = (bf16[1024,128]{1,0:T(8,128)(2,1)S(1)}, bf16[1024,128]{1,0:T(8,128)(2,1)}, u32[]{:S(2)}) copy-start(bf16[1024,128]{1,0:T(8,128)(2,1)} %param.13) | copy-start | bytes 786436
  31.3 6.9 %copy-start.7 = (bf16[1024,128]{1,0:T(8,128)(2,1)S(1)}, bf16[1024,128]{1,0:T(8,128)(2,1)}, u32[]{:S(2)}) copy-start(bf16[1024,128]{1,0:T(8,128)(2,1)} %param.12) | copy-start | bytes 786436
  31.3 39.1 %all-to-all-start.1 = ((bf16[16,144,256]{2,1,0:T(8,128)(2,1)}), bf16[16,144,256]{2,1,0:T(8,128)(2,1)S(1)}, u32[]{:S(2)}, u32[]{:S(2)}) async-start(bf16[16,144,256]{2,1,0:T(8,128)(2,1)} %broadcast_in_dim.6), calls=%async_computation.1 | async-start | bytes 2359296 | tf_op jit(solution)/shard_map/all_to_all | solution.py:27
  38.3 61.8 %collective-permute-start.1 = (bf16[1024,128]{1,0:T(8,128)(2,1)S(1)}, bf16[1024,128]{1,0:T(8,128)(2,1)S(1)}, u32[]{:S(2)}, u32[]{:S(2)}) collective-permute-start(bf16[1024,128]{1,0:T(8,128)(2,1)S(1)} %get-tuple-element.25), channel_id=1, source_target_pairs={{0,1},{1,0},{2,3},{3,2},{4,5},{5,4},{6,7},{7,6},{8,9},{9,8},{10,11... | collective-permute-start | bytes 786440 | tf_op jit(solution)/shard_map/ppermute | solution.py:32
  46.0 24.4 %collective-permute-start = (bf16[16,64,128]{2,1,0:T(8,128)(2,1)S(1)}, bf16[16,64,128]{2,1,0:T(8,128)(2,1)S(1)}, u32[]{:S(2)}, u32[]{:S(2)}) collective-permute-start(bf16[16,64,128]{2,1,0:T(8,128)(2,1)S(1)} %all-to-all-done.own_ref), channel_id=1, source_target_pairs={{0,1},{1,0},{2,3},{3,2},{4,5},{5,4},{6,7},{7,6},{8,9},{9,8},{10,11... | collective-permute-start | bytes 786440 | tf_op jit(solution)/shard_map/ppermute | solution.py:32
  72.0 52.0 %copy-start.8 = (f32[16,128]{1,0:T(8,128)S(1)}, f32[16,128]{1,0:T(8,128)}, u32[]{:S(2)}) copy-start(f32[16,128]{1,0:T(8,128)} %param.21) | copy-start | bytes 24580
  72.0 52.0 %copy-start.9 = (f32[16,128]{1,0:T(8,128)S(1)}, f32[16,128]{1,0:T(8,128)}, u32[]{:S(2)}) copy-start(f32[16,128]{1,0:T(8,128)} %param.19) | copy-start | bytes 24580
  72.0 52.0 %copy-start.10 = (f32[16,128]{1,0:T(8,128)S(1)}, f32[16,128]{1,0:T(8,128)}, u32[]{:S(2)}) copy-start(f32[16,128]{1,0:T(8,128)} %param.20) | copy-start | bytes 24580
  72.1 52.0 %copy-start.11 = (f32[16,128]{1,0:T(8,128)S(1)}, f32[16,128]{1,0:T(8,128)}, u32[]{:S(2)}) copy-start(f32[16,128]{1,0:T(8,128)} %param.18) | copy-start | bytes 24580
  100.1 28.8 %copy-start.2 = (f32[256,128]{1,0:T(8,128)S(1)}, f32[256,128]{1,0:T(8,128)}, u32[]{:S(2)}) copy-start(f32[256,128]{1,0:T(8,128)} %key_master_ref.1) | copy-start | bytes 393220
  100.1 28.9 %copy-start.3 = (f32[256,128]{1,0:T(8,128)S(1)}, f32[256,128]{1,0:T(8,128)}, u32[]{:S(2)}) copy-start(f32[256,128]{1,0:T(8,128)} %query_master_ref.1) | copy-start | bytes 393220
  125.4 10.3 %all-to-all-start.3 = ((bf16[16,2,16,128]{3,2,1,0:T(8,128)(2,1)}), bf16[16,2,16,128]{3,2,1,0:T(8,128)(2,1)S(1)}, u32[]{:S(2)}, u32[]{:S(2)}) async-start(bf16[16,2,16,128]{3,2,1,0:T(8,128)(2,1)} %broadcast_in_dim.7), calls=%async_computation.3 | async-start | bytes 262144 | tf_op jit(solution)/shard_map/all_to_all | solution.py:27
  135.7 1.8 copy-start.4
  137.5 33.4 %all-to-all-start.4 = ((bf16[16,2,256,128]{3,2,1,0:T(8,128)(2,1)}), bf16[16,2,256,128]{3,2,1,0:T(8,128)(2,1)}, u32[]{:S(2)}, u32[]{:S(2)}) async-start(bf16[16,2,256,128]{3,2,1,0:T(8,128)(2,1)} %broadcast_in_dim.8), calls=%async_computation.4 | async-start | bytes 4194304 | tf_op jit(solution)/shard_map/all_to_all | solution.py:27
  141.9 28.9 %collective-permute-start.3 = (bf16[16,144,256]{2,1,0:T(8,128)(2,1)S(1)}, bf16[16,144,256]{2,1,0:T(8,128)(2,1)S(1)}, u32[]{:S(2)}, u32[]{:S(2)}) collective-permute-start(bf16[16,144,256]{2,1,0:T(8,128)(2,1)S(1)} %all-to-all-done.1.rest_ref.own_rest_ref), channel_id=1, source_target_pairs={{0,1},{1,0},{2,3},{3,2},{4,5},{5,4},{6,7},{7,6},{8,9},{9,8},{10,11... | collective-permute-start | bytes 3538952 | tf_op jit(solution)/shard_map/ppermute | solution.py:32
  145.4 4.4 %collective-permute-start.2 = (bf16[16,112,256]{2,1,0:T(8,128)(2,1)S(1)}, bf16[16,112,256]{2,1,0:T(8,128)(2,1)S(1)}, u32[]{:S(2)}, u32[]{:S(2)}) collective-permute-start(bf16[16,112,256]{2,1,0:T(8,128)(2,1)S(1)} %bitcast.26), channel_id=1, source_target_pairs={{0,1},{1,0},{2,3},{3,2},{4,5},{5,4},{6,7},{7,6},{8,9},{9,8},{10,11... | collective-permute-start | bytes 2752520 | tf_op jit(solution)/shard_map/ppermute | solution.py:32
  149.8 0.9 copy-start
  170.8 1.2 copy-start.1
  172.0 0.9 copy-start.5

commit v4 on v3

v4 whole, which is shorter than its diff:
```python
import jax
import jax.numpy as jnp
from jax import lax
from jax.experimental import pallas as pl
from jax.experimental.pallas import tpu as pltpu
from jax.sharding import Mesh
from jax.sharding import PartitionSpec as P


D = 4096
HD = 128
FS = ("y", "x")
BF = jnp.bfloat16
F32 = jnp.float32

moment_decay = 0.8
square_decay = 0.9
square_floor = 1.0
norm_floor = 0.01
step_rate = 0.01

VMEM = pltpu.CompilerParams(vmem_limit_bytes=48 * 1024 * 1024)


def sent_to_all(x, axis):
    count = lax.axis_size(axis)
    return lax.all_to_all(jnp.broadcast_to(x[None], (count, *x.shape)), axis, 0, 0, tiled=True)


def swapped(x, axis):
    count = lax.axis_size(axis)
    return lax.ppermute(x, axis, [(i, i ^ 1) for i in range(count)])


def product_kernel(own_ref, other_ref, top_ref, rest_ref, out_ref):
    core = lax.axis_index("c")
    cut = top_ref.shape[1]
    first = core == 0

    def some(z, total):
        own, other = own_ref[z], other_ref[z]
        left = jnp.where(first, own, other)
        right = jnp.where(first, other, own)
        total += jnp.dot(left[:, :cut], top_ref[z], preferred_element_type=F32)
        both = jnp.concatenate([left[:, cut:], right], axis=1)
        return total + jnp.dot(both, rest_ref[z], preferred_element_type=F32)

    total = lax.fori_loop(0, own_ref.shape[0], some, jnp.zeros(out_ref.shape, F32), unroll=4)
    out_ref[...] = total.astype(out_ref.dtype)


def product(own, other, top, rest):
    return pl.pallas_call(
        product_kernel,
        out_shape=jax.ShapeDtypeStruct((own.shape[1], top.shape[-1]), BF),
        in_specs=[pl.BlockSpec(memory_space=pltpu.VMEM)] * 4,
        compiler_params=VMEM,
        name="product",
    )(own, other, top, rest)


def partial_kernel(low_ref, own_ref, other_ref, out_ref):
    core = lax.axis_index("c")
    rows, _, count, width = out_ref.shape
    contract = (((0,), (0,)), ((), ()))
    cots = jnp.concatenate([own_ref[...], other_ref[...]], axis=1)
    both = lax.dot_general(low_ref[...], cots, contract, preferred_element_type=F32).astype(out_ref.dtype)
    out_ref[:, core] = both[:, :width].reshape(rows, count, width)
    out_ref[:, 1 - core] = both[:, width:].reshape(rows, count, width)


def partials(low, own, other, rows, count):
    return pl.pallas_call(
        partial_kernel,
        out_shape=jax.ShapeDtypeStruct((rows, 2, count, own.shape[-1]), BF),
        in_specs=[pl.BlockSpec(memory_space=pltpu.VMEM)] * 3,
        compiler_params=VMEM,
        name="partials",
    )(low, own, other)


def moments_kernel(
    parts_ref,
    query_first_hbm,
    query_second_hbm,
    key_first_hbm,
    key_second_hbm,
    query_first_new_ref,
    query_second_new_ref,
    key_first_new_ref,
    key_second_new_ref,
    ratio_ref,
    olds_ref,
    arrived,
):
    rows = ratio_ref.shape[0]
    outs = ((query_first_new_ref, query_second_new_ref), (key_first_new_ref, key_second_new_ref))
    olds = (query_first_hbm, query_second_hbm, key_first_hbm, key_second_hbm)
    incoming = [pltpu.make_async_copy(old, olds_ref.at[n], arrived.at[n]) for n, old in enumerate(olds)]
    for copy in incoming:
        copy.start()
    sums = []
    for k in range(2):
        projected = parts_ref[k].astype(F32)
        for f in range(1, rows):
            projected += parts_ref[2 * f + k].astype(F32)
        sums.append(projected)
    for copy in incoming:
        copy.wait()
    for k, projected in enumerate(sums):
        first_new = moment_decay * olds_ref[2 * k] + (1.0 - moment_decay) * projected
        second_new = square_decay * olds_ref[2 * k + 1] + (1.0 - square_decay) * projected * projected
        outs[k][0][...] = first_new
        outs[k][1][...] = second_new
        ratio = (first_new / jnp.sqrt(second_new + square_floor)).astype(BF)
        for f in range(rows):
            ratio_ref[f, k] = ratio


def moments(parts, query_first, query_second, key_first, key_second):
    count, width = query_first.shape
    own = jax.ShapeDtypeStruct((count, width), F32)
    ratios = jax.ShapeDtypeStruct((parts.shape[0] // 2, 2, count, width), BF)
    return pl.pallas_call(
        moments_kernel,
        out_shape=(own, own, own, own, ratios),
        in_specs=[pl.BlockSpec(memory_space=pltpu.VMEM)] + [pl.BlockSpec(memory_space=pl.ANY)] * 4,
        scratch_shapes=[pltpu.VMEM((4, count, width), F32), pltpu.SemaphoreType.DMA((4,))],
        compiler_params=VMEM,
        name="moments",
    )(parts, query_first, query_second, key_first, key_second)


GROUP = 4


def finish_kernel(
    ratio_ref,
    own_top_ref,
    own_rest_ref,
    other_top_hbm,
    other_rest_hbm,
    masters_hbm,
    query_master_ref,
    key_master_ref,
    query_step_ref,
    query_weight_ref,
    query_copy_hbm,
    key_step_ref,
    key_weight_ref,
    key_copy_hbm,
    other_top_ref,
    other_rest_ref,
    masters_ref,
    update_top_ref,
    update_rest_ref,
    copies_ref,
    scales_ref,
    arrived,
    left,
):
    core, row = lax.axis_index("c"), lax.axis_index(FS)
    rows, _, count, width = ratio_ref.shape
    ranks = rows * count
    top, rest = own_top_ref.shape[1], own_rest_ref.shape[1]
    tops, rests = pl.ds(0, top), pl.ds(top, rest)
    incoming = [
        pltpu.make_async_copy(other_top_hbm, other_top_ref, arrived.at[0]),
        pltpu.make_async_copy(other_rest_hbm, other_rest_ref, arrived.at[1]),
        pltpu.make_async_copy(masters_hbm, masters_ref, arrived.at[2]),
    ]
    copy_hbms = (query_copy_hbm, key_copy_hbm)

    def leaving(k, part):
        span = pl.ds(part * GROUP, GROUP)
        return pltpu.make_async_copy(copies_ref.at[k, span], copy_hbms[k].at[span], left.at[k, part])

    for copy in incoming:
        copy.start()

    def products(top_ref, rest_ref, k, ratio, part, total):
        span = pl.ds(part * GROUP, GROUP)
        for basis_ref, update_ref, size in ((top_ref, update_top_ref, top), (rest_ref, update_rest_ref, rest)):
            basis = basis_ref[span].reshape(GROUP * size, ranks)
            update = jnp.dot(basis, ratio, preferred_element_type=F32)
            update_ref[k, span] = update.reshape(GROUP, size, width)
            total += jnp.sum((update * update).reshape(GROUP * size // 8, 8, width), axis=0)
        return total

    def scaled(k, total):
        scale = 1.0 / jnp.sqrt(jnp.sum(total, keepdims=True) / (D * HD) + norm_floor)
        scales_ref[k] = jnp.broadcast_to(scale, (8, width))

    def copied(k, part):
        scale = scales_ref[k][:1]
        for n in range(GROUP):
            f = part * GROUP + n
            for span, update_ref in ((tops, update_top_ref), (rests, update_rest_ref)):
                step = update_ref[k, f] * scale
                copies_ref[k, f, span, :] = (masters_ref[f, k, span, :].astype(F32) - step_rate * step).astype(BF)

    def sent(k, part):
        for n in range(2):
            pl.when(k == n)(leaving(n, part).start)

    parts = rows // GROUP
    mine, theirs = core, 1 - core
    ratio = ratio_ref[:, mine].reshape(ranks, width)
    total = jnp.zeros((8, width), F32)
    for part in range(parts):
        total = products(own_top_ref, own_rest_ref, mine, ratio, part, total)
    scaled(mine, total)
    for copy in incoming:
        copy.wait()
    ratio = ratio_ref[:, theirs].reshape(ranks, width)
    total = jnp.zeros((8, width), F32)
    for part in range(parts):
        total = products(other_top_ref, other_rest_ref, theirs, ratio, part, total)
        copied(mine, part)
        sent(mine, part)
    scaled(theirs, total)
    for part in range(parts):
        copied(theirs, part)
        sent(theirs, part)
    outs = (
        (query_master_ref, query_step_ref, query_weight_ref),
        (key_master_ref, key_step_ref, key_weight_ref),
    )
    for k, (master_ref, step_ref, weight_ref) in enumerate(outs):
        scale = scales_ref[k][:1]
        for span, update_ref in ((tops, update_top_ref), (rests, update_rest_ref)):
            step = update_ref[k, row] * scale
            step_ref[span, :] = step
            weight_ref[span, :] = master_ref[span, :] - step_rate * step
    for k in range(2):
        for part in range(parts):
            leaving(k, part).wait()


def finish(ratio, own_top, own_rest, other_top, other_rest, masters, query_master, key_master):
    own_rows, width = query_master.shape
    rows = ratio.shape[0]
    top, rest = own_top.shape[1], own_rest.shape[1]
    mine = jax.ShapeDtypeStruct((own_rows, width), F32)
    copied = jax.ShapeDtypeStruct((rows, own_rows, width), BF)
    vmem, anywhere = pl.BlockSpec(memory_space=pltpu.VMEM), pl.BlockSpec(memory_space=pl.ANY)
    return pl.pallas_call(
        finish_kernel,
        out_shape=(mine, mine, copied) * 2,
        in_specs=[vmem, vmem, vmem, anywhere, anywhere, anywhere, vmem, vmem],
        out_specs=(vmem, vmem, anywhere) * 2,
        scratch_shapes=[
            pltpu.VMEM(other_top.shape, BF),
            pltpu.VMEM(other_rest.shape, BF),
            pltpu.VMEM(masters.shape, BF),
            pltpu.VMEM((2, rows, top, width), F32),
            pltpu.VMEM((2, rows, rest, width), F32),
            pltpu.VMEM((2, rows, own_rows, width), BF),
            pltpu.VMEM((2, 8, width), F32),
            pltpu.SemaphoreType.DMA((3,)),
            pltpu.SemaphoreType.DMA((2, rows // GROUP)),
        ],
        compiler_params=VMEM,
        name="finish",
    )(ratio, own_top, own_rest, other_top, other_rest, masters, query_master, key_master)


TOP = 112


def body(
    saved_input,
    query_cot,
    key_cot,
    query_master,
    key_master,
    query_basis,
    key_basis,
    query_first,
    query_second,
    key_first,
    key_second,
):
    rows = lax.axis_size(FS)
    depth = lax.axis_size("z")
    tokens, width = query_cot.shape
    low_count = query_first.shape[0]
    ranks = query_basis.shape[1]
    share = tokens // depth
    core = lax.axis_index("c")
    first_core = core == 0

    pieces = lax.all_to_all(saved_input.reshape(depth, share, width), "z", 0, 0, tiled=True)
    own_basis = jnp.where(first_core, query_basis, key_basis)
    top = lax.all_gather(own_basis[:TOP], FS, axis=0, tiled=True).reshape(rows, TOP, ranks)
    rest = sent_to_all(own_basis[TOP:], FS)
    rest = rest.reshape(rows, -1, ranks)
    other_pieces = swapped(pieces, "c")
    own_cot = jnp.where(first_core, query_cot, key_cot)
    other_cot = swapped(jnp.where(first_core, key_cot, query_cot), "c")
    low = product(pieces, other_pieces, top, rest)
    low = lax.all_gather(low, "z", axis=0, tiled=True)
    masters = sent_to_all(jnp.stack([query_master, key_master]).astype(BF), FS)

    partial = partials(low, own_cot, other_cot, rows, low_count)
    partial = partial.reshape(2 * rows, low_count, width)
    partial = lax.all_to_all(partial, (*FS, "c"), 0, 0, tiled=True)
    *news, ratio = moments(partial, query_first, query_second, key_first, key_second)
    ratio = lax.all_to_all(ratio, FS, 0, 0, tiled=True)

    other_top = swapped(top, "c")
    other_rest = swapped(rest, "c")
    query_step, query_weight, query_copy, key_step, key_weight, key_copy = finish(
        ratio,
        top,
        rest,
        other_top,
        other_rest,
        masters.reshape(rows, 2, -1, width),
        query_master,
        key_master,
    )
    return (
        query_step,
        query_weight,
        query_copy.reshape(D, width),
        news[0],
        news[1],
        key_step,
        key_weight,
        key_copy.reshape(D, width),
        news[2],
        news[3],
    )


def solution(mesh):
    torus = Mesh(mesh.devices.reshape(4, 4, 16, 2), ("y", "x", "z", "c"))
    tp = ("z", "c")
    split = P(FS, tp)
    rows = P(FS, None)
    copied = P(None, tp)
    in_specs = (split,) * 5 + (rows,) * 2 + (split,) * 4
    out_specs = (split, split, copied, split, split) * 2

    return jax.shard_map(body, mesh=torus, in_specs=in_specs, out_specs=out_specs, check_vma=False)
```

time: 181 us -> 178 us (0.983)
  local copies, waits for them, and re-layouts: 8 us -> 5.96 us
    all_to_all x0 -> x1, waiting for transfers between devices: none -> 6.73 us  [body(): ratio = lax.all_to_all(ratio, FS, 0, 0, tiled=True)]
    all_to_all x3 -> x2, waiting for transfers between devices: 26.9 us -> 20.1 us  [sent_to_all(): lax.all_to_all(jnp.broadcast_to(x[None], (count, *x.shape)), axis, 0, 0,...]
    all_to_all x0 -> x1, starting transfers between devices: none -> 3.52 us  [body(): ratio = lax.all_to_all(ratio, FS, 0, 0, tiled=True)]
    all_to_all x3 -> x2, starting transfers between devices: 14.8 us -> 11.3 us  [sent_to_all(): lax.all_to_all(jnp.broadcast_to(x[None], (count, *x.shape)), axis, 0, 0,...]
where the time goes in v4:
time: 178 us; the launch traced here: 177 us
  blocking collectives  73.3 us (41%)
  starting transfers between devices  45.6 us (26%)
  waiting for transfers between devices  42.1 us (24%)
  Pallas kernels  8.5 us (5%)
  local copies, waits for them, and re-layouts  5.96 us (3%)
    all_gather x1, blocking collectives, body(): low = lax.all_gather(low, 'z', axis=0, tiled=True)  28 us
    all_to_all x1, blocking collectives, body(): partial = lax.all_to_all(partial, (*FS, 'c'), 0, 0, tiled=True)  22.9 us
    all_gather x1, blocking collectives, body(): lax.all_gather(own_basis[:TOP], FS, axis=0, tiled=True)  22.3 us
    all_to_all x2, waiting for transfers between devices, sent_to_all(): lax.all_to_all(jnp.broadcast_to(x[None], (count, *x.shape)), axis, 0, 0,...  20.1 us
    all_to_all x1, starting transfers between devices, body(): lax.all_to_all(saved_input.reshape(depth, share, width), 'z', 0, 0, tiled...  15.7 us
    ppermute x4, starting transfers between devices, swapped(): return lax.ppermute(x, axis, [(i, i ^ 1) for i in range(count)])  15.1 us
    all_to_all x1, waiting for transfers between devices, body(): lax.all_to_all(saved_input.reshape(depth, share, width), 'z', 0, 0, tiled...  12.8 us
    all_to_all x2, starting transfers between devices, sent_to_all(): lax.all_to_all(jnp.broadcast_to(x[None], (count, *x.shape)), axis, 0, 0,...  11.3 us
  transfers between devices with their start and end apart: 8, of which 4 were waited for; matrix products, arithmetic and copies ran while one was open for 1% of the time, Pallas kernels for 1%

profile of v4, /device:TPU:1, one launch (start us, length us, event | category | flops | bytes accessed | tf_op | source)
XLA Modules:
  0.0 177.4 jit_solution(15848433390205267664)
XLA Ops:
  0.6 15.7 %all-to-all-start = ((bf16[16,64,128]{2,1,0:T(8,128)(2,1)}), bf16[16,64,128]{2,1,0:T(8,128)(2,1)S(1)}, u32[]{:S(2)}, u32[]{:S(2)}) async-start(bf16[16,64,128]{2,1,0:T(8,128)(2,1)} %bitcast.13), calls=%async_computation | async-start | bytes 524288 | tf_op jit(solution)/shard_map/all_to_all | solution.py:293
  16.4 0.9 broadcast_select_fusion.2
  17.4 12.8 %all-to-all-done.own_ref = bf16[16,64,128]{2,1,0:T(8,128)(2,1)S(1)} async-done(((bf16[16,64,128]{2,1,0:T(8,128)(2,1)}), bf16[16,64,128]{2,1,0:T(8,128)(2,1)S(1)}, u32[]{:S(2)}, u32[]{:S(2)}) %all-to-all-start) | async-done | bytes 262176 | tf_op jit(solution)/shard_map/all_to_all | solution.py:293
  30.2 1.1 broadcast_in_dim.4
  31.3 0.0 copy-start.10
  31.3 0.0 copy-start.11
  31.3 6.9 %all-to-all-start.1 = ((bf16[16,144,256]{2,1,0:T(8,128)(2,1)}), bf16[16,144,256]{2,1,0:T(8,128)(2,1)S(1)}, u32[]{:S(2)}, u32[]{:S(2)}) async-start(bf16[16,144,256]{2,1,0:T(8,128)(2,1)} %broadcast_in_dim.4), calls=%async_computation.1 | async-start | bytes 2359296 | tf_op jit(solution)/shard_map/all_to_all | solution.py:27
  38.2 7.8 %collective-permute-start = (bf16[16,64,128]{2,1,0:T(8,128)(2,1)S(1)}, bf16[16,64,128]{2,1,0:T(8,128)(2,1)S(1)}, u32[]{:S(2)}, u32[]{:S(2)}) collective-permute-start(bf16[16,64,128]{2,1,0:T(8,128)(2,1)S(1)} %all-to-all-done.own_ref), channel_id=1, source_target_pairs={{0,1},{1,0},{2,3},{3,2},{4,5},{5,4},{6,7},{7,6},{8,9},{9,8},{10,11... | collective-permute-start | bytes 786440 | tf_op jit(solution)/shard_map/ppermute | solution.py:32
  46.0 0.0 copy-done.10
  46.0 0.0 copy-done.11
  46.0 1.9 %collective-permute-start.1 = (bf16[1024,128]{1,0:T(8,128)(2,1)S(1)}, bf16[1024,128]{1,0:T(8,128)(2,1)S(1)}, u32[]{:S(2)}, u32[]{:S(2)}) collective-permute-start(bf16[1024,128]{1,0:T(8,128)(2,1)S(1)} %get-tuple-element.32), channel_id=1, source_target_pairs={{0,1},{1,0},{2,3},{3,2},{4,5},{5,4},{6,7},{7,6},{8,9},{9,8},{10,11... | collective-permute-start | bytes 786440 | tf_op jit(solution)/shard_map/ppermute | solution.py:32
  48.0 22.3 %all_gather.6 = bf16[1792,256]{1,0:T(8,128)(2,1)S(1)} all-gather(bf16[112,256]{1,0:T(8,128)(2,1)S(1)} %slice.8), channel_id=1, replica_groups=mesh['y'=4,'x'=4,'z'=16,'c'=2] {'y','x'}, dimensions={0}, use_global_device_ids=true | all-gather | bytes 974848 | tf_op jit(solution)/shard_map/all_gather | solution.py:295
  70.3 0.0 all-to-all-done.1.rest_ref.own_rest_ref
  70.3 0.0 collective-permute-done.other_ref
  70.3 1.0 product.1
  71.4 0.0 copy-start.6
  71.4 0.0 copy-start.7
  71.4 0.0 copy-start.8
  71.4 0.0 copy-start.9
  71.4 0.0 copy-start.2
  71.4 0.0 copy-start.3
  71.4 28.0 %all_gather.7.low_ref = bf16[1024,256]{1,0:T(8,128)(2,1)S(1)} all-gather(bf16[64,256]{1,0:T(8,128)(2,1)S(1)} %product.1), channel_id=1, replica_groups=mesh['y'=4,'x'=4,'z'=16,'c'=2] {'z'}, dimensions={0}, use_global_device_ids=true | all-gather | bytes 557056 | tf_op jit(solution)/shard_map/all_gather | solution.py:302
  99.5 0.0 collective-permute-done.1.other_ref
  99.5 0.3 partials.1
  99.8 22.9 %all_to_all.25.parts_ref = bf16[32,16,128]{2,1,0:T(8,128)(2,1)S(1)} all-to-all(bf16[32,16,128]{2,1,0:T(8,128)(2,1)S(1)} %bitcast.12), channel_id=1, replica_groups=mesh['y'=4,'x'=4,'z'=16,'c'=2] {'y','x','c'}, dimensions={0} | all-to-all | bytes 262144 | tf_op jit(solution)/shard_map/all_to_all | solution.py:307
  122.7 0.0 copy-done.6
  122.7 0.0 copy-done.7
  122.8 0.0 copy-done.8
  122.8 0.0 copy-done.9
  122.8 0.8 moments.1
  123.6 3.5 %all-to-all-start.3 = ((bf16[16,2,16,128]{3,2,1,0:T(8,128)(2,1)}), bf16[16,2,16,128]{3,2,1,0:T(8,128)(2,1)S(1)}, u32[]{:S(2)}, u32[]{:S(2)}) async-start(bf16[16,2,16,128]{3,2,1,0:T(8,128)(2,1)} %get-tuple-element.21), calls=%async_computation.3 | async-start | bytes 262144 | tf_op jit(solution)/shard_map/all_to_all | solution.py:309
  127.1 0.0 copy-done.2
  127.1 0.0 copy-done.3
  127.2 6.7 %all-to-all-done.3.ratio_ref = bf16[16,2,16,128]{3,2,1,0:T(8,128)(2,1)S(1)} async-done(((bf16[16,2,16,128]{3,2,1,0:T(8,128)(2,1)}), bf16[16,2,16,128]{3,2,1,0:T(8,128)(2,1)S(1)}, u32[]{:S(2)}, u32[]{:S(2)}) %all-to-all-start.3) | async-done | bytes 131104 | tf_op jit(solution)/shard_map/all_to_all | solution.py:309
  133.9 0.0 copy-start.4
  133.9 1.8 broadcast_in_dim.5
  135.7 0.0 copy-done.4
  135.7 4.4 %all-to-all-start.4 = ((bf16[16,2,256,128]{3,2,1,0:T(8,128)(2,1)}), bf16[16,2,256,128]{3,2,1,0:T(8,128)(2,1)}, u32[]{:S(2)}, u32[]{:S(2)}) async-start(bf16[16,2,256,128]{3,2,1,0:T(8,128)(2,1)} %broadcast_in_dim.5), calls=%async_computation.4 | async-start | bytes 4194304 | tf_op jit(solution)/shard_map/all_to_all | solution.py:27
  140.1 3.5 %collective-permute-start.3 = (bf16[16,144,256]{2,1,0:T(8,128)(2,1)S(1)}, bf16[16,144,256]{2,1,0:T(8,128)(2,1)S(1)}, u32[]{:S(2)}, u32[]{:S(2)}) collective-permute-start(bf16[16,144,256]{2,1,0:T(8,128)(2,1)S(1)} %all-to-all-done.1.rest_ref.own_rest_ref), channel_id=1, source_target_pairs={{0,1},{1,0},{2,3},{3,2},{4,5},{5,4},{6,7},{7,6},{8,9},{9,8},{10,11... | collective-permute-start | bytes 3538952 | tf_op jit(solution)/shard_map/ppermute | solution.py:32
  143.6 1.9 %collective-permute-start.2 = (bf16[16,112,256]{2,1,0:T(8,128)(2,1)S(1)}, bf16[16,112,256]{2,1,0:T(8,128)(2,1)S(1)}, u32[]{:S(2)}, u32[]{:S(2)}) collective-permute-start(bf16[16,112,256]{2,1,0:T(8,128)(2,1)S(1)} %bitcast.10), channel_id=1, source_target_pairs={{0,1},{1,0},{2,3},{3,2},{4,5},{5,4},{6,7},{7,6},{8,9},{9,8},{10,11... | collective-permute-start | bytes 2752520 | tf_op jit(solution)/shard_map/ppermute | solution.py:32
  145.5 2.4 %collective-permute-done.2.other_top_hbm = bf16[16,112,256]{2,1,0:T(8,128)(2,1)S(1)} collective-permute-done((bf16[16,112,256]{2,1,0:T(8,128)(2,1)S(1)}, bf16[16,112,256]{2,1,0:T(8,128)(2,1)S(1)}, u32[]{:S(2)}, u32[]{:S(2)}) %collective-permute-start.2) | collective-permute-done | bytes 917536 | tf_op jit(solution)/shard_map/ppermute | solution.py:32
  148.0 0.0 copy-start
  148.0 0.9 copy-done
  148.9 20.1 %all-to-all-done.4.masters_hbm = bf16[16,2,256,128]{3,2,1,0:T(8,128)(2,1)} async-done(((bf16[16,2,256,128]{3,2,1,0:T(8,128)(2,1)}), bf16[16,2,256,128]{3,2,1,0:T(8,128)(2,1)}, u32[]{:S(2)}, u32[]{:S(2)}) %all-to-all-start.4) | async-done | bytes 2097184 | tf_op jit(solution)/shard_map/all_to_all | solution.py:27
  169.0 0.0 collective-permute-done.3.other_rest_hbm
  169.0 0.0 copy-start.1
  169.0 1.2 copy-done.1
  170.2 0.0 copy-start.5
  170.2 0.9 copy-done.5
  171.1 6.3 %finish.1 = (f32[256,128]{1,0:T(8,128)}, f32[256,128]{1,0:T(8,128)}, bf16[16,256,128]{2,1,0:T(8,128)(2,1)}, f32[256,128]{1,0:T(8,128)}, f32[256,128]{1,0:T(8,128)}, /*index=5*/bf16[16,256,128]{2,1,0:T(8,128)(2,1)}) custom-call(bf16[16,2,16,128]{3,2,1,0:T(8,128)(2,1)S(1)} %copy-done.5, bf16[16,112,256]{2,1,0:T(8,128)(2,1)S(1)} %bitcast.11, ...), custom_call_target="tpu_custom_call" | custom-call | tf_op jit(solution)/shard_map/finish/pallas_call | solution.py:247
  (5 shorter events, 0.1 us)
Async XLA Ops:
  0.6 29.5 %all-to-all-start = ((bf16[16,64,128]{2,1,0:T(8,128)(2,1)}), bf16[16,64,128]{2,1,0:T(8,128)(2,1)S(1)}, u32[]{:S(2)}, u32[]{:S(2)}) async-start(bf16[16,64,128]{2,1,0:T(8,128)(2,1)} %bitcast.13), calls=%async_computation | async-start | bytes 524288 | tf_op jit(solution)/shard_map/all_to_all | solution.py:293
  31.3 14.7 %copy-start.10 = (bf16[1024,128]{1,0:T(8,128)(2,1)S(1)}, bf16[1024,128]{1,0:T(8,128)(2,1)}, u32[]{:S(2)}) copy-start(bf16[1024,128]{1,0:T(8,128)(2,1)} %param.13) | copy-start | bytes 786436
  31.3 14.7 %copy-start.11 = (bf16[1024,128]{1,0:T(8,128)(2,1)S(1)}, bf16[1024,128]{1,0:T(8,128)(2,1)}, u32[]{:S(2)}) copy-start(bf16[1024,128]{1,0:T(8,128)(2,1)} %param.12) | copy-start | bytes 786436
  31.3 39.0 %all-to-all-start.1 = ((bf16[16,144,256]{2,1,0:T(8,128)(2,1)}), bf16[16,144,256]{2,1,0:T(8,128)(2,1)S(1)}, u32[]{:S(2)}, u32[]{:S(2)}) async-start(bf16[16,144,256]{2,1,0:T(8,128)(2,1)} %broadcast_in_dim.4), calls=%async_computation.1 | async-start | bytes 2359296 | tf_op jit(solution)/shard_map/all_to_all | solution.py:27
  38.2 32.1 %collective-permute-start = (bf16[16,64,128]{2,1,0:T(8,128)(2,1)S(1)}, bf16[16,64,128]{2,1,0:T(8,128)(2,1)S(1)}, u32[]{:S(2)}, u32[]{:S(2)}) collective-permute-start(bf16[16,64,128]{2,1,0:T(8,128)(2,1)S(1)} %all-to-all-done.own_ref), channel_id=1, source_target_pairs={{0,1},{1,0},{2,3},{3,2},{4,5},{5,4},{6,7},{7,6},{8,9},{9,8},{10,11... | collective-permute-start | bytes 786440 | tf_op jit(solution)/shard_map/ppermute | solution.py:32
  46.0 53.4 %collective-permute-start.1 = (bf16[1024,128]{1,0:T(8,128)(2,1)S(1)}, bf16[1024,128]{1,0:T(8,128)(2,1)S(1)}, u32[]{:S(2)}, u32[]{:S(2)}) collective-permute-start(bf16[1024,128]{1,0:T(8,128)(2,1)S(1)} %get-tuple-element.32), channel_id=1, source_target_pairs={{0,1},{1,0},{2,3},{3,2},{4,5},{5,4},{6,7},{7,6},{8,9},{9,8},{10,11... | collective-permute-start | bytes 786440 | tf_op jit(solution)/shard_map/ppermute | solution.py:32
  71.4 51.4 %copy-start.6 = (f32[16,128]{1,0:T(8,128)S(1)}, f32[16,128]{1,0:T(8,128)}, u32[]{:S(2)}) copy-start(f32[16,128]{1,0:T(8,128)} %query_first_hbm.1) | copy-start | bytes 24580
  71.4 51.4 %copy-start.7 = (f32[16,128]{1,0:T(8,128)S(1)}, f32[16,128]{1,0:T(8,128)}, u32[]{:S(2)}) copy-start(f32[16,128]{1,0:T(8,128)} %query_second_hbm.1) | copy-start | bytes 24580
  71.4 51.4 %copy-start.8 = (f32[16,128]{1,0:T(8,128)S(1)}, f32[16,128]{1,0:T(8,128)}, u32[]{:S(2)}) copy-start(f32[16,128]{1,0:T(8,128)} %key_first_hbm.1) | copy-start | bytes 24580
  71.4 51.4 %copy-start.9 = (f32[16,128]{1,0:T(8,128)S(1)}, f32[16,128]{1,0:T(8,128)}, u32[]{:S(2)}) copy-start(f32[16,128]{1,0:T(8,128)} %key_second_hbm.1) | copy-start | bytes 24580
  71.4 55.7 %copy-start.2 = (f32[256,128]{1,0:T(8,128)S(1)}, f32[256,128]{1,0:T(8,128)}, u32[]{:S(2)}) copy-start(f32[256,128]{1,0:T(8,128)} %key_master_ref.1) | copy-start | bytes 393220
  71.4 55.7 %copy-start.3 = (f32[256,128]{1,0:T(8,128)S(1)}, f32[256,128]{1,0:T(8,128)}, u32[]{:S(2)}) copy-start(f32[256,128]{1,0:T(8,128)} %query_master_ref.1) | copy-start | bytes 393220
  123.6 10.3 %all-to-all-start.3 = ((bf16[16,2,16,128]{3,2,1,0:T(8,128)(2,1)}), bf16[16,2,16,128]{3,2,1,0:T(8,128)(2,1)S(1)}, u32[]{:S(2)}, u32[]{:S(2)}) async-start(bf16[16,2,16,128]{3,2,1,0:T(8,128)(2,1)} %get-tuple-element.21), calls=%async_computation.3 | async-start | bytes 262144 | tf_op jit(solution)/shard_map/all_to_all | solution.py:309
  133.9 1.8 copy-start.4
  135.7 33.3 %all-to-all-start.4 = ((bf16[16,2,256,128]{3,2,1,0:T(8,128)(2,1)}), bf16[16,2,256,128]{3,2,1,0:T(8,128)(2,1)}, u32[]{:S(2)}, u32[]{:S(2)}) async-start(bf16[16,2,256,128]{3,2,1,0:T(8,128)(2,1)} %broadcast_in_dim.5), calls=%async_computation.4 | async-start | bytes 4194304 | tf_op jit(solution)/shard_map/all_to_all | solution.py:27
  140.1 28.9 %collective-permute-start.3 = (bf16[16,144,256]{2,1,0:T(8,128)(2,1)S(1)}, bf16[16,144,256]{2,1,0:T(8,128)(2,1)S(1)}, u32[]{:S(2)}, u32[]{:S(2)}) collective-permute-start(bf16[16,144,256]{2,1,0:T(8,128)(2,1)S(1)} %all-to-all-done.1.rest_ref.own_rest_ref), channel_id=1, source_target_pairs={{0,1},{1,0},{2,3},{3,2},{4,5},{5,4},{6,7},{7,6},{8,9},{9,8},{10,11... | collective-permute-start | bytes 3538952 | tf_op jit(solution)/shard_map/ppermute | solution.py:32
  143.6 4.4 %collective-permute-start.2 = (bf16[16,112,256]{2,1,0:T(8,128)(2,1)S(1)}, bf16[16,112,256]{2,1,0:T(8,128)(2,1)S(1)}, u32[]{:S(2)}, u32[]{:S(2)}) collective-permute-start(bf16[16,112,256]{2,1,0:T(8,128)(2,1)S(1)} %bitcast.10), channel_id=1, source_target_pairs={{0,1},{1,0},{2,3},{3,2},{4,5},{5,4},{6,7},{7,6},{8,9},{9,8},{10,11... | collective-permute-start | bytes 2752520 | tf_op jit(solution)/shard_map/ppermute | solution.py:32
  148.0 0.9 copy-start
  169.0 1.2 copy-start.1
  170.2 0.9 copy-start.5

commit v5 on v4

v5 whole, which is shorter than its diff:
```python
import jax
import jax.numpy as jnp
from jax import lax
from jax.experimental import pallas as pl
from jax.experimental.pallas import tpu as pltpu
from jax.sharding import Mesh
from jax.sharding import PartitionSpec as P


D = 4096
HD = 128
FS = ("y", "x")
BF = jnp.bfloat16
F32 = jnp.float32

moment_decay = 0.8
square_decay = 0.9
square_floor = 1.0
norm_floor = 0.01
step_rate = 0.01

VMEM = pltpu.CompilerParams(vmem_limit_bytes=48 * 1024 * 1024)


def swapped(x, axis):
    count = lax.axis_size(axis)
    return lax.ppermute(x, axis, [(i, i ^ 1) for i in range(count)])


def product_kernel(pieces_ref, basis_ref, out_ref):
    groups, chips, share, width = pieces_ref.shape
    ranks = out_ref.shape[-1]
    total = jnp.zeros((groups * share, 2 * ranks), F32)
    for z in range(chips):
        piece = pieces_ref[:, z].reshape(groups * share, width)
        total += jnp.dot(piece, basis_ref[z], preferred_element_type=F32)
    total = total.astype(BF)
    for c in range(2):
        out_ref[:, c] = total[:, c * ranks : (c + 1) * ranks].reshape(groups, share, ranks)


def product(pieces, basis):
    groups, _, share, _ = pieces.shape
    return pl.pallas_call(
        product_kernel,
        out_shape=jax.ShapeDtypeStruct((groups, 2, share, basis.shape[-1] // 2), BF),
        in_specs=[pl.BlockSpec(memory_space=pltpu.VMEM)] * 2,
        compiler_params=VMEM,
        name="product",
    )(pieces, basis)


def total_kernel(parts_ref, out_ref):
    total = parts_ref[0].astype(F32)
    for n in range(1, parts_ref.shape[0]):
        total += parts_ref[n].astype(F32)
    total = total.astype(BF)
    for n in range(out_ref.shape[0]):
        out_ref[n] = total


def totals(parts, copies):
    return pl.pallas_call(
        total_kernel,
        out_shape=jax.ShapeDtypeStruct((copies, *parts.shape[1:]), BF),
        in_specs=[pl.BlockSpec(memory_space=pltpu.VMEM)],
        compiler_params=VMEM,
        name="totals",
    )(parts)


def partial_kernel(low_ref, own_ref, other_ref, out_ref):
    core = lax.axis_index("c")
    rows, _, count, width = out_ref.shape
    contract = (((0,), (0,)), ((), ()))
    cots = jnp.concatenate([own_ref[...], other_ref[...]], axis=1)
    both = lax.dot_general(low_ref[...], cots, contract, preferred_element_type=F32).astype(out_ref.dtype)
    out_ref[:, core] = both[:, :width].reshape(rows, count, width)
    out_ref[:, 1 - core] = both[:, width:].reshape(rows, count, width)


def partials(low, own, other, rows, count):
    return pl.pallas_call(
        partial_kernel,
        out_shape=jax.ShapeDtypeStruct((rows, 2, count, own.shape[-1]), BF),
        in_specs=[pl.BlockSpec(memory_space=pltpu.VMEM)] * 3,
        compiler_params=VMEM,
        name="partials",
    )(low, own, other)


def moments_kernel(
    parts_ref,
    query_first_hbm,
    query_second_hbm,
    key_first_hbm,
    key_second_hbm,
    query_first_new_ref,
    query_second_new_ref,
    key_first_new_ref,
    key_second_new_ref,
    ratio_ref,
    olds_ref,
    arrived,
):
    rows = ratio_ref.shape[0]
    outs = ((query_first_new_ref, query_second_new_ref), (key_first_new_ref, key_second_new_ref))
    olds = (query_first_hbm, query_second_hbm, key_first_hbm, key_second_hbm)
    incoming = [pltpu.make_async_copy(old, olds_ref.at[n], arrived.at[n]) for n, old in enumerate(olds)]
    for copy in incoming:
        copy.start()
    sums = []
    for k in range(2):
        projected = parts_ref[k].astype(F32)
        for f in range(1, rows):
            projected += parts_ref[2 * f + k].astype(F32)
        sums.append(projected)
    for copy in incoming:
        copy.wait()
    for k, projected in enumerate(sums):
        first_new = moment_decay * olds_ref[2 * k] + (1.0 - moment_decay) * projected
        second_new = square_decay * olds_ref[2 * k + 1] + (1.0 - square_decay) * projected * projected
        outs[k][0][...] = first_new
        outs[k][1][...] = second_new
        ratio = (first_new / jnp.sqrt(second_new + square_floor)).astype(BF)
        for f in range(rows):
            ratio_ref[f, k] = ratio


def moments(parts, query_first, query_second, key_first, key_second):
    count, width = query_first.shape
    own = jax.ShapeDtypeStruct((count, width), F32)
    ratios = jax.ShapeDtypeStruct((parts.shape[0] // 2, 2, count, width), BF)
    return pl.pallas_call(
        moments_kernel,
        out_shape=(own, own, own, own, ratios),
        in_specs=[pl.BlockSpec(memory_space=pltpu.VMEM)] + [pl.BlockSpec(memory_space=pltpu.HBM)] * 4,
        scratch_shapes=[pltpu.VMEM((4, count, width), F32), pltpu.SemaphoreType.DMA((4,))],
        compiler_params=VMEM,
        name="moments",
    )(parts, query_first, query_second, key_first, key_second)


GROUP = 4


def finish_kernel(
    ratio_ref,
    own_ref,
    other_hbm,
    bulk_hbm,
    query_master_ref,
    key_master_ref,
    query_step_ref,
    query_weight_ref,
    query_copy_hbm,
    key_step_ref,
    key_weight_ref,
    key_copy_hbm,
    other_ref,
    masters_ref,
    update_ref,
    copies_ref,
    scales_ref,
    arrived,
    left,
):
    core, row = lax.axis_index("c"), lax.axis_index(FS)
    rows, _, _, width = ratio_ref.shape
    own_rows, ranks = own_ref.shape[2], 2 * own_ref.shape[3]
    incoming = [
        pltpu.make_async_copy(other_hbm, other_ref, arrived.at[0]),
        pltpu.make_async_copy(bulk_hbm.at[:, pl.ds(2, 2)], masters_ref, arrived.at[1]),
    ]
    copy_hbms = (query_copy_hbm, key_copy_hbm)

    def leaving(k, part):
        span = pl.ds(part * GROUP, GROUP)
        return pltpu.make_async_copy(copies_ref.at[k, span], copy_hbms[k].at[span], left.at[k, part])

    for copy in incoming:
        copy.start()

    def products(basis_ref, k, ratio, part, total):
        span = pl.ds(part * GROUP, GROUP)
        update = jnp.zeros((GROUP * own_rows, width), F32)
        for n in range(2):
            basis = basis_ref[span, n].reshape(GROUP * own_rows, ranks // 2)
            update += jnp.dot(basis, ratio[n * ranks // 2 : (n + 1) * ranks // 2], preferred_element_type=F32)
        update_ref[k, span] = update.reshape(GROUP, own_rows, width)
        return total + jnp.sum((update * update).reshape(GROUP * own_rows // 8, 8, width), axis=0)

    def scaled(k, total):
        scale = 1.0 / jnp.sqrt(jnp.sum(total, keepdims=True) / (D * HD) + norm_floor)
        scales_ref[k] = jnp.broadcast_to(scale, (8, width))

    def copied(k, part):
        scale = scales_ref[k][:1]
        for n in range(GROUP):
            f = part * GROUP + n
            step = update_ref[k, f] * scale
            copies_ref[k, f] = (masters_ref[f, k].astype(F32) - step_rate * step).astype(BF)

    def sent(k, part):
        for n in range(2):
            pl.when(k == n)(leaving(n, part).start)

    parts = rows // GROUP
    mine, theirs = core, 1 - core
    ratio = ratio_ref[:, mine].reshape(ranks, width)
    total = jnp.zeros((8, width), F32)
    for part in range(parts):
        total = products(own_ref, mine, ratio, part, total)
    scaled(mine, total)
    for copy in incoming:
        copy.wait()
    ratio = ratio_ref[:, theirs].reshape(ranks, width)
    total = jnp.zeros((8, width), F32)
    for part in range(parts):
        total = products(other_ref, theirs, ratio, part, total)
        copied(mine, part)
        sent(mine, part)
    scaled(theirs, total)
    for part in range(parts):
        copied(theirs, part)
        sent(theirs, part)
    outs = (
        (query_master_ref, query_step_ref, query_weight_ref),
        (key_master_ref, key_step_ref, key_weight_ref),
    )
    for k, (master_ref, step_ref, weight_ref) in enumerate(outs):
        scale = scales_ref[k][:1]
        step = update_ref[k, row] * scale
        step_ref[...] = step
        weight_ref[...] = master_ref[...] - step_rate * step
    for k in range(2):
        for part in range(parts):
            leaving(k, part).wait()


def finish(ratio, own, other, bulk, query_master, key_master):
    own_rows, width = query_master.shape
    rows = ratio.shape[0]
    mine = jax.ShapeDtypeStruct((own_rows, width), F32)
    copied = jax.ShapeDtypeStruct((rows, own_rows, width), BF)
    vmem, anywhere = pl.BlockSpec(memory_space=pltpu.VMEM), pl.BlockSpec(memory_space=pl.ANY)
    return pl.pallas_call(
        finish_kernel,
        out_shape=(mine, mine, copied) * 2,
        in_specs=[vmem, vmem, anywhere, anywhere, vmem, vmem],
        out_specs=(vmem, vmem, anywhere) * 2,
        scratch_shapes=[
            pltpu.VMEM(other.shape, BF),
            pltpu.VMEM((rows, 2, own_rows, width), BF),
            pltpu.VMEM((2, rows, own_rows, width), F32),
            pltpu.VMEM((2, rows, own_rows, width), BF),
            pltpu.VMEM((2, 8, width), F32),
            pltpu.SemaphoreType.DMA((2,)),
            pltpu.SemaphoreType.DMA((2, rows // GROUP)),
        ],
        compiler_params=VMEM,
        name="finish",
    )(ratio, own, other, bulk, query_master, key_master)


def body(
    saved_input,
    query_cot,
    key_cot,
    query_master,
    key_master,
    query_basis,
    key_basis,
    query_first,
    query_second,
    key_first,
    key_second,
):
    rows = lax.axis_size(FS)
    depth = lax.axis_size("z")
    tokens, width = query_cot.shape
    low_count = query_first.shape[0]
    ranks = query_basis.shape[1]
    share = tokens // depth
    core = lax.axis_index("c")
    first_core = core == 0

    pieces = lax.all_to_all(saved_input.reshape(depth, share, width), "z", 0, 0, tiled=True)
    own_rows = jnp.concatenate([query_basis, key_basis], axis=1).reshape(2, width, 2 * ranks)
    own_rows = jnp.where(first_core, own_rows[0], own_rows[1])
    basis = lax.all_gather(own_rows, "x", axis=0, tiled=False)
    own_basis = jnp.where(first_core, query_basis, key_basis)
    bulk = jnp.stack(
        [own_basis[:, :width], own_basis[:, width:], query_master.astype(BF), key_master.astype(BF)]
    )
    bulk = lax.all_gather(bulk.reshape(-1, width), FS, axis=0, tiled=True).reshape(rows, 4, -1, width)
    groups = lax.axis_size("y")
    pieces = pieces.reshape(groups, depth // groups, share, width)
    pieces = lax.all_to_all(pieces, "y", 0, 0, tiled=True)
    low = product(pieces, basis).reshape(2 * groups, share, ranks)
    low = lax.all_to_all(low, ("y", "c"), 0, 0, tiled=True)
    low = totals(low, depth)
    low = lax.all_to_all(low, "z", 0, 0, tiled=True).reshape(tokens, ranks)
    own_cot = jnp.where(first_core, query_cot, key_cot)
    other_cot = swapped(jnp.where(first_core, key_cot, query_cot), "c")

    partial = partials(low, own_cot, other_cot, rows, low_count)
    partial = partial.reshape(2 * rows, low_count, width)
    partial = lax.all_to_all(partial, (*FS, "c"), 0, 0, tiled=True)
    *news, ratio = moments(partial, query_first, query_second, key_first, key_second)
    ratio = lax.all_to_all(ratio, FS, 0, 0, tiled=True)

    own_basis = bulk[:, :2]
    other_basis = swapped(own_basis, "c")
    query_step, query_weight, query_copy, key_step, key_weight, key_copy = finish(
        ratio, own_basis, other_basis, bulk, query_master, key_master
    )
    return (
        query_step,
        query_weight,
        query_copy.reshape(D, width),
        news[0],
        news[1],
        key_step,
        key_weight,
        key_copy.reshape(D, width),
        news[2],
        news[3],
    )


def solution(mesh):
    torus = Mesh(mesh.devices.reshape(4, 4, 16, 2), ("y", "x", "z", "c"))
    tp = ("z", "c")
    split = P(FS, tp)
    rows = P(FS, None)
    copied = P(None, tp)
    in_specs = (split,) * 5 + (rows,) * 2 + (split,) * 4
    out_specs = (split, split, copied, split, split) * 2

    return jax.shard_map(body, mesh=torus, in_specs=in_specs, out_specs=out_specs, check_vma=False)
```

time: 178 us -> 152 us (0.85)
  starting transfers between devices: 45.6 us -> 30.5 us
  between operations: 0.89 us -> 14.2 us
  waiting for transfers between devices: 42.1 us -> 30.2 us
  blocking collectives: 73.3 us -> 62.2 us
  local copies, waits for them, and re-layouts: 5.96 us -> 2.76 us
    all_gather x2 -> x1, blocking collectives: 50.4 us -> 10.2 us  [body(): basis = lax.all_gather(own_rows, 'x', axis=0, tiled=False)]
    all_to_all x0 -> x2, blocking collectives: none -> 33.1 us  [the longest x1 23.4 us: body(): low = lax.all_to_all(low, ('y', 'c'), 0, 0, tiled=True)]
    all_to_all x3 -> x2, waiting for transfers between devices: 26.9 us -> 12.8 us  [the longest x1 12.8 us: body(): low = lax.all_to_all(low, 'z', 0, 0, tiled=True).reshape(tokens, ranks)]
    ppermute x4 -> x2, starting transfers between devices: 15.1 us -> 4.8 us  [swapped(): return lax.ppermute(x, axis, [(i, i ^ 1) for i in range(count)])]
    all_to_all x3 -> x2, starting transfers between devices: 14.8 us -> 9.85 us  [the longest x1 5.67 us: body(): low = lax.all_to_all(low, 'z', 0, 0, tiled=True).reshape(tokens, ranks)]
    all_to_all x1, blocking collectives: 22.9 us -> 18.9 us  [body(): partial = lax.all_to_all(partial, (*FS, 'c'), 0, 0, tiled=True)]
    broadcast_in_dim x2 -> x0, local copies, waits for them, and re-layouts: 2.89 us -> none  [sent_to_all(): jnp.broadcast_to(x[None], (count, *x.shape))]
    unnamed x24 -> x17, local copies, waits for them, and re-layouts: 3.05 us -> 0.96 us
  transfers between devices with their start and end apart: 8 -> 6, of which waited for: 4 -> 4; matrix products, arithmetic and copies ran while one was open for 1% -> 1% of each run, Pallas kernels for 1% -> 2%
where the time goes in v5:
time: 152 us; the launch traced here: 151 us
  blocking collectives  62.2 us (41%)
  starting transfers between devices  30.5 us (20%)
  waiting for transfers between devices  30.2 us (20%)
  between operations  14.2 us (9%)
  Pallas kernels  8.72 us (6%)
  local copies, waits for them, and re-layouts  2.76 us (2%)
  other arithmetic  2.74 us (2%)
    all_to_all x1, blocking collectives, body(): low = lax.all_to_all(low, ('y', 'c'), 0, 0, tiled=True)  23.4 us
    all_to_all x1, blocking collectives, body(): partial = lax.all_to_all(partial, (*FS, 'c'), 0, 0, tiled=True)  18.9 us
    all_to_all x1, starting transfers between devices, body(): lax.all_to_all(saved_input.reshape(depth, share, width), 'z', 0, 0, tiled...  15.8 us
    all_to_all x1, waiting for transfers between devices, body(): lax.all_to_all(saved_input.reshape(depth, share, width), 'z', 0, 0, tiled...  13.8 us
    all_to_all x1, waiting for transfers between devices, body(): low = lax.all_to_all(low, 'z', 0, 0, tiled=True).reshape(tokens, ranks)  12.8 us
    all_gather x1, blocking collectives, body(): basis = lax.all_gather(own_rows, 'x', axis=0, tiled=False)  10.2 us
    all_to_all x1, blocking collectives, body(): ratio = lax.all_to_all(ratio, FS, 0, 0, tiled=True)  9.63 us
    pallas_call x1, Pallas kernels, finish(): pl.pallas_call(finish_kernel, out_shape=(mine, mine, copied) * 2, in_spec...  6.38 us
  transfers between devices with their start and end apart: 6, of which 4 were waited for; matrix products, arithmetic and copies ran while one was open for 1% of the time, Pallas kernels for 2%

profile of v5, /device:TPU:1, one launch (start us, length us, event | category | flops | bytes accessed | tf_op | source)
XLA Modules:
  0.0 151.3 jit_solution(18140947353738830616)
XLA Ops:
  7.2 0.0 all-gather.3.cloned.1.call-start
  7.2 0.9 constant_dynamic-update-slice_fusion.1
  8.2 0.9 broadcast_select_fusion.2
  9.1 1.0 convert_bitcast_fusion
  10.1 0.7 pad_maximum_fusion
  10.9 0.0 all-gather.3.cloned.1.call-update
  10.9 15.8 %all-to-all-start = ((bf16[16,64,128]{2,1,0:T(8,128)(2,1)}), bf16[16,64,128]{2,1,0:T(8,128)(2,1)}, u32[]{:S(2)}, u32[]{:S(2)}) async-start(bf16[16,64,128]{2,1,0:T(8,128)(2,1)} %bitcast), calls=%async_computation | async-start | bytes 524288 | tf_op jit(solution)/shard_map/all_to_all | solution.py:288
  26.7 13.8 %all-to-all-done = bf16[16,64,128]{2,1,0:T(8,128)(2,1)} async-done(((bf16[16,64,128]{2,1,0:T(8,128)(2,1)}), bf16[16,64,128]{2,1,0:T(8,128)(2,1)}, u32[]{:S(2)}, u32[]{:S(2)}) %all-to-all-start) | async-done | bytes 262176 | tf_op jit(solution)/shard_map/all_to_all | solution.py:288
  40.5 4.2 %all-to-all-start.1 = ((bf16[4,4,64,128]{3,2,1,0:T(8,128)(2,1)}), bf16[4,4,64,128]{3,2,1,0:T(8,128)(2,1)S(1)}, u32[]{:S(2)}, u32[]{:S(2)}) async-start(bf16[4,4,64,128]{3,2,1,0:T(8,128)(2,1)} %bitcast.1), calls=%async_computation.1 | async-start | bytes 524288 | tf_op jit(solution)/shard_map/all_to_all | solution.py:299
  44.7 10.2 %all-gather = bf16[512,512]{1,0:T(8,128)(2,1)S(1)} all-gather(bf16[128,512]{1,0:T(8,128)(2,1)S(1)} %slice_select_fusion), channel_id=2, replica_groups=mesh['y'=4,'x'=4,'z'=16,'c'=2] {'x'}, dimensions={0}, use_global_device_ids=true | all-gather | bytes 655360 | tf_op jit(solution)/shard_map/all_gather | solution.py:291
  54.9 0.0 all-to-all-done.1.pieces_ref
  54.9 0.4 product.1
  55.3 23.4 %all_to_all.30.parts_ref = bf16[8,64,256]{2,1,0:T(8,128)(2,1)S(1)} all-to-all(bf16[8,64,256]{2,1,0:T(8,128)(2,1)S(1)} %bitcast.20), channel_id=1, replica_groups=mesh['y'=4,'x'=4,'z'=16,'c'=2] {'y','c'}, dimensions={0} | all-to-all | bytes 524288 | tf_op jit(solution)/shard_map/all_to_all | solution.py:301
  78.8 0.9 totals.1
  79.7 5.7 %all-to-all-start.3 = ((bf16[16,64,256]{2,1,0:T(8,128)(2,1)}), bf16[16,64,256]{2,1,0:T(8,128)(2,1)S(1)}, u32[]{:S(2)}, u32[]{:S(2)}) async-start(bf16[16,64,256]{2,1,0:T(8,128)(2,1)} %totals.1), calls=%async_computation.3 | async-start | bytes 1048576 | tf_op jit(solution)/shard_map/all_to_all | solution.py:303
  85.3 1.4 all-gather.3.cloned.1.call-done
  86.7 0.0 copy-start.6
  86.7 0.0 copy-start.7
  86.7 1.8 %slice.26.own_ref = bf16[16,2,256,128]{3,2,1,0:T(8,128)(2,1)S(1)} slice(bf16[16,4,256,128]{3,2,1,0:T(8,128)(2,1)} %bitcast.22), slice={[0:16], [0:2], [0:256], [0:128]} | slice | bytes 4194304 | tf_op jit(solution)/shard_map/slice | solution.py:313
  88.5 0.0 copy-start.2
  88.5 0.0 copy-start.3
  88.5 0.0 copy-start.4
  88.5 0.0 copy-start.5
  88.5 0.0 copy-start
  88.5 0.0 copy-start.1
  88.6 2.9 %collective-permute-start.1 = (bf16[16,2,256,128]{3,2,1,0:T(8,128)(2,1)S(1)}, bf16[16,2,256,128]{3,2,1,0:T(8,128)(2,1)}, u32[]{:S(2)}, u32[]{:S(2)}) collective-permute-start(bf16[16,2,256,128]{3,2,1,0:T(8,128)(2,1)S(1)} %slice.26.own_ref), channel_id=1, source_target_pairs={{0,1},{1,0},{2,3},{3,2},{4,5},{5,4},{6,7},{7,6},{8,9},{9,8},{10,11... | collective-permute-start | bytes 6291464 | tf_op jit(solution)/shard_map/ppermute | solution.py:27
  91.4 0.0 copy-done.6
  91.5 0.0 copy-done.7
  91.5 1.9 %collective-permute-start = (bf16[1024,128]{1,0:T(8,128)(2,1)S(1)}, bf16[1024,128]{1,0:T(8,128)(2,1)S(1)}, u32[]{:S(2)}, u32[]{:S(2)}) collective-permute-start(bf16[1024,128]{1,0:T(8,128)(2,1)S(1)} %get-tuple-element.32), channel_id=1, source_target_pairs={{0,1},{1,0},{2,3},{3,2},{4,5},{5,4},{6,7},{7,6},{8,9},{9,8},{10,11... | collective-permute-start | bytes 786440 | tf_op jit(solution)/shard_map/ppermute | solution.py:27
  93.4 2.1 %collective-permute-done.other_ref = bf16[1024,128]{1,0:T(8,128)(2,1)S(1)} collective-permute-done((bf16[1024,128]{1,0:T(8,128)(2,1)S(1)}, bf16[1024,128]{1,0:T(8,128)(2,1)S(1)}, u32[]{:S(2)}, u32[]{:S(2)}) %collective-permute-start) | collective-permute-done | bytes 262176 | tf_op jit(solution)/shard_map/ppermute | solution.py:27
  95.6 12.8 %all-to-all-done.3 = bf16[16,64,256]{2,1,0:T(8,128)(2,1)S(1)} async-done(((bf16[16,64,256]{2,1,0:T(8,128)(2,1)}), bf16[16,64,256]{2,1,0:T(8,128)(2,1)S(1)}, u32[]{:S(2)}, u32[]{:S(2)}) %all-to-all-start.3) | async-done | bytes 524320 | tf_op jit(solution)/shard_map/all_to_all | solution.py:303
  108.4 0.3 partials.1
  108.8 18.9 %all_to_all.31.parts_ref = bf16[32,16,128]{2,1,0:T(8,128)(2,1)S(1)} all-to-all(bf16[32,16,128]{2,1,0:T(8,128)(2,1)S(1)} %bitcast.21), channel_id=1, replica_groups=mesh['y'=4,'x'=4,'z'=16,'c'=2] {'y','x','c'}, dimensions={0} | all-to-all | bytes 262144 | tf_op jit(solution)/shard_map/all_to_all | solution.py:309
  127.7 0.0 copy-done.2
  127.7 0.0 copy-done.3
  127.7 0.0 copy-done.4
  127.7 0.0 copy-done.5
  127.7 0.7 moments.1
  128.4 9.6 %all_to_all.32.ratio_ref = bf16[16,2,16,128]{3,2,1,0:T(8,128)(2,1)S(1)} all-to-all(bf16[16,2,16,128]{3,2,1,0:T(8,128)(2,1)S(1)} %get-tuple-element.21), channel_id=1, replica_groups=mesh['y'=4,'x'=4,'z'=16,'c'=2] {'y','x'}, dimensions={0} | all-to-all | bytes 262144 | tf_op jit(solution)/shard_map/all_to_all | solution.py:311
  138.1 0.0 collective-permute-done.1.other_hbm
  138.1 0.0 copy-done
  138.1 0.0 copy-done.1
  138.1 6.4 %finish.1 = (f32[256,128]{1,0:T(8,128)}, f32[256,128]{1,0:T(8,128)}, bf16[16,256,128]{2,1,0:T(8,128)(2,1)}, f32[256,128]{1,0:T(8,128)}, f32[256,128]{1,0:T(8,128)}, /*index=5*/bf16[16,256,128]{2,1,0:T(8,128)(2,1)}) custom-call(bf16[16,2,16,128]{3,2,1,0:T(8,128)(2,1)S(1)} %all_to_all.32.ratio_ref, bf16[16,2,256,128]{3,2,1,0:T(8,128)(2,1)S(1)} %slice.26.own_ref, ...), custom_call_target="tpu_custom_call" | custom-call | tf_op jit(solution)/shard_map/finish/pallas_call | solution.py:247
  (3 shorter events, 0.1 us)
Async XLA Ops:
  7.2 79.5 %all-gather.3.cloned.1.call-start = ((), (), s32[]{:S(2)}) async-start(), calls=%async_computation.6 | async-start | bytes 4456448 | tf_op jit(solution)/shard_map/all_gather | solution.py:296
  10.9 29.6 %all-to-all-start = ((bf16[16,64,128]{2,1,0:T(8,128)(2,1)}), bf16[16,64,128]{2,1,0:T(8,128)(2,1)}, u32[]{:S(2)}, u32[]{:S(2)}) async-start(bf16[16,64,128]{2,1,0:T(8,128)(2,1)} %bitcast), calls=%async_computation | async-start | bytes 524288 | tf_op jit(solution)/shard_map/all_to_all | solution.py:288
  40.5 14.4 %all-to-all-start.1 = ((bf16[4,4,64,128]{3,2,1,0:T(8,128)(2,1)}), bf16[4,4,64,128]{3,2,1,0:T(8,128)(2,1)S(1)}, u32[]{:S(2)}, u32[]{:S(2)}) async-start(bf16[4,4,64,128]{3,2,1,0:T(8,128)(2,1)} %bitcast.1), calls=%async_computation.1 | async-start | bytes 524288 | tf_op jit(solution)/shard_map/all_to_all | solution.py:299
  79.7 28.8 %all-to-all-start.3 = ((bf16[16,64,256]{2,1,0:T(8,128)(2,1)}), bf16[16,64,256]{2,1,0:T(8,128)(2,1)S(1)}, u32[]{:S(2)}, u32[]{:S(2)}) async-start(bf16[16,64,256]{2,1,0:T(8,128)(2,1)} %totals.1), calls=%async_computation.3 | async-start | bytes 1048576 | tf_op jit(solution)/shard_map/all_to_all | solution.py:303
  86.7 4.8 %copy-start.6 = (bf16[1024,128]{1,0:T(8,128)(2,1)S(1)}, bf16[1024,128]{1,0:T(8,128)(2,1)}, u32[]{:S(2)}) copy-start(bf16[1024,128]{1,0:T(8,128)(2,1)} %param.13) | copy-start | bytes 786436
  86.7 4.8 %copy-start.7 = (bf16[1024,128]{1,0:T(8,128)(2,1)S(1)}, bf16[1024,128]{1,0:T(8,128)(2,1)}, u32[]{:S(2)}) copy-start(bf16[1024,128]{1,0:T(8,128)(2,1)} %param.12) | copy-start | bytes 786436
  88.5 39.2 %copy-start.2 = (f32[16,128]{1,0:T(8,128)S(1)}, f32[16,128]{1,0:T(8,128)}, u32[]{:S(2)}) copy-start(f32[16,128]{1,0:T(8,128)} %query_first_hbm.1) | copy-start | bytes 24580
  88.5 39.2 %copy-start.3 = (f32[16,128]{1,0:T(8,128)S(1)}, f32[16,128]{1,0:T(8,128)}, u32[]{:S(2)}) copy-start(f32[16,128]{1,0:T(8,128)} %query_second_hbm.1) | copy-start | bytes 24580
  88.5 39.2 %copy-start.4 = (f32[16,128]{1,0:T(8,128)S(1)}, f32[16,128]{1,0:T(8,128)}, u32[]{:S(2)}) copy-start(f32[16,128]{1,0:T(8,128)} %key_first_hbm.1) | copy-start | bytes 24580
  88.5 39.2 %copy-start.5 = (f32[16,128]{1,0:T(8,128)S(1)}, f32[16,128]{1,0:T(8,128)}, u32[]{:S(2)}) copy-start(f32[16,128]{1,0:T(8,128)} %key_second_hbm.1) | copy-start | bytes 24580
  88.5 49.5 %copy-start = (f32[256,128]{1,0:T(8,128)S(1)}, f32[256,128]{1,0:T(8,128)}, u32[]{:S(2)}) copy-start(f32[256,128]{1,0:T(8,128)} %key_master_ref.1) | copy-start | bytes 393220
  88.5 49.5 %copy-start.1 = (f32[256,128]{1,0:T(8,128)S(1)}, f32[256,128]{1,0:T(8,128)}, u32[]{:S(2)}) copy-start(f32[256,128]{1,0:T(8,128)} %query_master_ref.1) | copy-start | bytes 393220
  88.6 49.5 %collective-permute-start.1 = (bf16[16,2,256,128]{3,2,1,0:T(8,128)(2,1)S(1)}, bf16[16,2,256,128]{3,2,1,0:T(8,128)(2,1)}, u32[]{:S(2)}, u32[]{:S(2)}) collective-permute-start(bf16[16,2,256,128]{3,2,1,0:T(8,128)(2,1)S(1)} %slice.26.own_ref), channel_id=1, source_target_pairs={{0,1},{1,0},{2,3},{3,2},{4,5},{5,4},{6,7},{7,6},{8,9},{9,8},{10,11... | collective-permute-start | bytes 6291464 | tf_op jit(solution)/shard_map/ppermute | solution.py:27
  91.5 4.1 %collective-permute-start = (bf16[1024,128]{1,0:T(8,128)(2,1)S(1)}, bf16[1024,128]{1,0:T(8,128)(2,1)S(1)}, u32[]{:S(2)}, u32[]{:S(2)}) collective-permute-start(bf16[1024,128]{1,0:T(8,128)(2,1)S(1)} %get-tuple-element.32), channel_id=1, source_target_pairs={{0,1},{1,0},{2,3},{3,2},{4,5},{5,4},{6,7},{7,6},{8,9},{9,8},{10,11... | collective-permute-start | bytes 786440 | tf_op jit(solution)/shard_map/ppermute | solution.py:27
Sparse Core Ops, SparseCore 0:
  11.6 75.0 all-gather.2

commit v6 on v4

--- a/solution.py
+++ b/solution.py
@@ -124,7 +124,7 @@
     return pl.pallas_call(
         moments_kernel,
         out_shape=(own, own, own, own, ratios),
-        in_specs=[pl.BlockSpec(memory_space=pltpu.VMEM)] + [pl.BlockSpec(memory_space=pl.ANY)] * 4,
+        in_specs=[pl.BlockSpec(memory_space=pltpu.VMEM)] + [pl.BlockSpec(memory_space=pltpu.HBM)] * 4,
         scratch_shapes=[pltpu.VMEM((4, count, width), F32), pltpu.SemaphoreType.DMA((4,))],
         compiler_params=VMEM,
         name="moments",
@@ -143,11 +143,11 @@
     masters_hbm,
     query_master_ref,
     key_master_ref,
-    query_step_ref,
-    query_weight_ref,
+    query_step_hbm,
+    query_weight_hbm,
     query_copy_hbm,
-    key_step_ref,
-    key_weight_ref,
+    key_step_hbm,
+    key_weight_hbm,
     key_copy_hbm,
     other_top_ref,
     other_rest_ref,
@@ -155,9 +155,12 @@
     update_top_ref,
     update_rest_ref,
     copies_ref,
+    steps_ref,
+    weights_ref,
     scales_ref,
     arrived,
     left,
+    owned,
 ):
     core, row = lax.axis_index("c"), lax.axis_index(FS)
     rows, _, count, width = ratio_ref.shape
@@ -199,6 +202,25 @@
                 step = update_ref[k, f] * scale
                 copies_ref[k, f, span, :] = (masters_ref[f, k, span, :].astype(F32) - step_rate * step).astype(BF)
 
+    def owning(k):
+        return (
+            pltpu.make_async_copy(steps_ref.at[k], (query_step_hbm, key_step_hbm)[k], owned.at[k, 0]),
+            pltpu.make_async_copy(weights_ref.at[k], (query_weight_hbm, key_weight_hbm)[k], owned.at[k, 1]),
+        )
+
+    def own(k):
+        for n, master_ref in enumerate((query_master_ref, key_master_ref)):
+
+            @pl.when(k == n)
+            def _():
+                scale = scales_ref[n][:1]
+                for span, update_ref in ((tops, update_top_ref), (rests, update_rest_ref)):
+                    step = update_ref[n, row] * scale
+                    steps_ref[n, span, :] = step
+                    weights_ref[n, span, :] = master_ref[span, :] - step_rate * step
+                for copy in owning(n):
+                    copy.start()
+
     def sent(k, part):
         for n in range(2):
             pl.when(k == n)(leaving(n, part).start)
@@ -210,6 +232,7 @@
     for part in range(parts):
         total = products(own_top_ref, own_rest_ref, mine, ratio, part, total)
     scaled(mine, total)
+    own(mine)
     for copy in incoming:
         copy.wait()
     ratio = ratio_ref[:, theirs].reshape(ranks, width)
@@ -219,19 +242,13 @@
         copied(mine, part)
         sent(mine, part)
     scaled(theirs, total)
+    own(theirs)
     for part in range(parts):
         copied(theirs, part)
         sent(theirs, part)
-    outs = (
-        (query_master_ref, query_step_ref, query_weight_ref),
-        (key_master_ref, key_step_ref, key_weight_ref),
-    )
-    for k, (master_ref, step_ref, weight_ref) in enumerate(outs):
-        scale = scales_ref[k][:1]
-        for span, update_ref in ((tops, update_top_ref), (rests, update_rest_ref)):
-            step = update_ref[k, row] * scale
-            step_ref[span, :] = step
-            weight_ref[span, :] = master_ref[span, :] - step_rate * step
+    for k in range(2):
+        for copy in owning(k):
+            copy.wait()
     for k in range(2):
         for part in range(parts):
             leaving(k, part).wait()
@@ -248,7 +265,7 @@
         finish_kernel,
         out_shape=(mine, mine, copied) * 2,
         in_specs=[vmem, vmem, vmem, anywhere, anywhere, anywhere, vmem, vmem],
-        out_specs=(vmem, vmem, anywhere) * 2,
+        out_specs=(anywhere, anywhere, anywhere) * 2,
         scratch_shapes=[
             pltpu.VMEM(other_top.shape, BF),
             pltpu.VMEM(other_rest.shape, BF),
@@ -256,9 +273,12 @@
             pltpu.VMEM((2, rows, top, width), F32),
             pltpu.VMEM((2, rows, rest, width), F32),
             pltpu.VMEM((2, rows, own_rows, width), BF),
+            pltpu.VMEM((2, own_rows, width), F32),
+            pltpu.VMEM((2, own_rows, width), F32),
             pltpu.VMEM((2, 8, width), F32),
             pltpu.SemaphoreType.DMA((3,)),
             pltpu.SemaphoreType.DMA((2, rows // GROUP)),
+            pltpu.SemaphoreType.DMA((2, 2)),
         ],
         compiler_params=VMEM,
         name="finish",

time: 178 us -> 177 us (level)
  no operation moved by 1% of the time
where the time goes in v6:
time: 177 us; the launch traced here: 176 us
  blocking collectives  73.3 us (41%)
  starting transfers between devices  45.6 us (26%)
  waiting for transfers between devices  42.1 us (24%)
  Pallas kernels  7.52 us (4%)
  local copies, waits for them, and re-layouts  5.96 us (3%)
    all_gather x1, blocking collectives, body(): low = lax.all_gather(low, 'z', axis=0, tiled=True)  28 us
    all_to_all x1, blocking collectives, body(): partial = lax.all_to_all(partial, (*FS, 'c'), 0, 0, tiled=True)  22.9 us
    all_gather x1, blocking collectives, body(): lax.all_gather(own_basis[:TOP], FS, axis=0, tiled=True)  22.3 us
    all_to_all x2, waiting for transfers between devices, sent_to_all(): lax.all_to_all(jnp.broadcast_to(x[None], (count, *x.shape)), axis, 0, 0,...  20.1 us
    all_to_all x1, starting transfers between devices, body(): lax.all_to_all(saved_input.reshape(depth, share, width), 'z', 0, 0, tiled...  15.7 us
    ppermute x4, starting transfers between devices, swapped(): return lax.ppermute(x, axis, [(i, i ^ 1) for i in range(count)])  15.1 us
    all_to_all x1, waiting for transfers between devices, body(): lax.all_to_all(saved_input.reshape(depth, share, width), 'z', 0, 0, tiled...  12.8 us
    all_to_all x2, starting transfers between devices, sent_to_all(): lax.all_to_all(jnp.broadcast_to(x[None], (count, *x.shape)), axis, 0, 0,...  11.3 us
  transfers between devices with their start and end apart: 8, of which 4 were waited for; matrix products, arithmetic and copies ran while one was open for 1% of the time, Pallas kernels for 1%

profile of v6, /device:TPU:1, one launch (start us, length us, event | category | flops | bytes accessed | tf_op | source)
XLA Modules:
  0.0 176.5 jit_solution(14463896462499664221)
XLA Ops:
  0.6 15.7 %all-to-all-start = ((bf16[16,64,128]{2,1,0:T(8,128)(2,1)}), bf16[16,64,128]{2,1,0:T(8,128)(2,1)S(1)}, u32[]{:S(2)}, u32[]{:S(2)}) async-start(bf16[16,64,128]{2,1,0:T(8,128)(2,1)} %bitcast.13), calls=%async_computation | async-start | bytes 524288 | tf_op jit(solution)/shard_map/all_to_all | solution.py:313
  16.4 0.9 broadcast_select_fusion.2
  17.4 12.8 %all-to-all-done.own_ref = bf16[16,64,128]{2,1,0:T(8,128)(2,1)S(1)} async-done(((bf16[16,64,128]{2,1,0:T(8,128)(2,1)}), bf16[16,64,128]{2,1,0:T(8,128)(2,1)S(1)}, u32[]{:S(2)}, u32[]{:S(2)}) %all-to-all-start) | async-done | bytes 262176 | tf_op jit(solution)/shard_map/all_to_all | solution.py:313
  30.2 1.1 broadcast_in_dim.4
  31.3 0.0 copy-start.10
  31.3 0.0 copy-start.11
  31.3 6.9 %all-to-all-start.1 = ((bf16[16,144,256]{2,1,0:T(8,128)(2,1)}), bf16[16,144,256]{2,1,0:T(8,128)(2,1)S(1)}, u32[]{:S(2)}, u32[]{:S(2)}) async-start(bf16[16,144,256]{2,1,0:T(8,128)(2,1)} %broadcast_in_dim.4), calls=%async_computation.1 | async-start | bytes 2359296 | tf_op jit(solution)/shard_map/all_to_all | solution.py:27
  38.2 7.8 %collective-permute-start = (bf16[16,64,128]{2,1,0:T(8,128)(2,1)S(1)}, bf16[16,64,128]{2,1,0:T(8,128)(2,1)S(1)}, u32[]{:S(2)}, u32[]{:S(2)}) collective-permute-start(bf16[16,64,128]{2,1,0:T(8,128)(2,1)S(1)} %all-to-all-done.own_ref), channel_id=1, source_target_pairs={{0,1},{1,0},{2,3},{3,2},{4,5},{5,4},{6,7},{7,6},{8,9},{9,8},{10,11... | collective-permute-start | bytes 786440 | tf_op jit(solution)/shard_map/ppermute | solution.py:32
  46.0 0.0 copy-done.10
  46.0 0.0 copy-done.11
  46.0 1.9 %collective-permute-start.1 = (bf16[1024,128]{1,0:T(8,128)(2,1)S(1)}, bf16[1024,128]{1,0:T(8,128)(2,1)S(1)}, u32[]{:S(2)}, u32[]{:S(2)}) collective-permute-start(bf16[1024,128]{1,0:T(8,128)(2,1)S(1)} %get-tuple-element.32), channel_id=1, source_target_pairs={{0,1},{1,0},{2,3},{3,2},{4,5},{5,4},{6,7},{7,6},{8,9},{9,8},{10,11... | collective-permute-start | bytes 786440 | tf_op jit(solution)/shard_map/ppermute | solution.py:32
  48.0 22.3 %all_gather.6 = bf16[1792,256]{1,0:T(8,128)(2,1)S(1)} all-gather(bf16[112,256]{1,0:T(8,128)(2,1)S(1)} %slice.8), channel_id=1, replica_groups=mesh['y'=4,'x'=4,'z'=16,'c'=2] {'y','x'}, dimensions={0}, use_global_device_ids=true | all-gather | bytes 974848 | tf_op jit(solution)/shard_map/all_gather | solution.py:315
  70.3 0.0 all-to-all-done.1.rest_ref.own_rest_ref
  70.3 0.0 collective-permute-done.other_ref
  70.3 1.0 product.1
  71.4 0.0 copy-start.6
  71.4 0.0 copy-start.7
  71.4 0.0 copy-start.8
  71.4 0.0 copy-start.9
  71.4 0.0 copy-start.2
  71.4 0.0 copy-start.3
  71.4 28.0 %all_gather.7.low_ref = bf16[1024,256]{1,0:T(8,128)(2,1)S(1)} all-gather(bf16[64,256]{1,0:T(8,128)(2,1)S(1)} %product.1), channel_id=1, replica_groups=mesh['y'=4,'x'=4,'z'=16,'c'=2] {'z'}, dimensions={0}, use_global_device_ids=true | all-gather | bytes 557056 | tf_op jit(solution)/shard_map/all_gather | solution.py:322
  99.5 0.0 collective-permute-done.1.other_ref
  99.5 0.3 partials.1
  99.8 22.9 %all_to_all.25.parts_ref = bf16[32,16,128]{2,1,0:T(8,128)(2,1)S(1)} all-to-all(bf16[32,16,128]{2,1,0:T(8,128)(2,1)S(1)} %bitcast.12), channel_id=1, replica_groups=mesh['y'=4,'x'=4,'z'=16,'c'=2] {'y','x','c'}, dimensions={0} | all-to-all | bytes 262144 | tf_op jit(solution)/shard_map/all_to_all | solution.py:327
  122.7 0.0 copy-done.6
  122.7 0.0 copy-done.7
  122.8 0.0 copy-done.8
  122.8 0.0 copy-done.9
  122.8 0.8 moments.1
  123.6 3.5 %all-to-all-start.3 = ((bf16[16,2,16,128]{3,2,1,0:T(8,128)(2,1)}), bf16[16,2,16,128]{3,2,1,0:T(8,128)(2,1)S(1)}, u32[]{:S(2)}, u32[]{:S(2)}) async-start(bf16[16,2,16,128]{3,2,1,0:T(8,128)(2,1)} %get-tuple-element.21), calls=%async_computation.3 | async-start | bytes 262144 | tf_op jit(solution)/shard_map/all_to_all | solution.py:329
  127.1 0.0 copy-done.2
  127.1 0.0 copy-done.3
  127.2 6.7 %all-to-all-done.3.ratio_ref = bf16[16,2,16,128]{3,2,1,0:T(8,128)(2,1)S(1)} async-done(((bf16[16,2,16,128]{3,2,1,0:T(8,128)(2,1)}), bf16[16,2,16,128]{3,2,1,0:T(8,128)(2,1)S(1)}, u32[]{:S(2)}, u32[]{:S(2)}) %all-to-all-start.3) | async-done | bytes 131104 | tf_op jit(solution)/shard_map/all_to_all | solution.py:329
  133.9 0.0 copy-start.4
  133.9 1.8 %broadcast_in_dim.5 = bf16[16,2,256,128]{3,2,1,0:T(8,128)(2,1)} broadcast(bf16[2,256,128]{2,1,0:T(8,128)(2,1)S(1)} %pad_maximum_fusion), dimensions={1,2,3} | broadcast | bytes 2228224 | tf_op jit(solution)/shard_map/broadcast_in_dim | solution.py:27
  135.7 0.0 copy-done.4
  135.7 4.4 %all-to-all-start.4 = ((bf16[16,2,256,128]{3,2,1,0:T(8,128)(2,1)}), bf16[16,2,256,128]{3,2,1,0:T(8,128)(2,1)}, u32[]{:S(2)}, u32[]{:S(2)}) async-start(bf16[16,2,256,128]{3,2,1,0:T(8,128)(2,1)} %broadcast_in_dim.5), calls=%async_computation.4 | async-start | bytes 4194304 | tf_op jit(solution)/shard_map/all_to_all | solution.py:27
  140.1 3.5 %collective-permute-start.3 = (bf16[16,144,256]{2,1,0:T(8,128)(2,1)S(1)}, bf16[16,144,256]{2,1,0:T(8,128)(2,1)S(1)}, u32[]{:S(2)}, u32[]{:S(2)}) collective-permute-start(bf16[16,144,256]{2,1,0:T(8,128)(2,1)S(1)} %all-to-all-done.1.rest_ref.own_rest_ref), channel_id=1, source_target_pairs={{0,1},{1,0},{2,3},{3,2},{4,5},{5,4},{6,7},{7,6},{8,9},{9,8},{10,11... | collective-permute-start | bytes 3538952 | tf_op jit(solution)/shard_map/ppermute | solution.py:32
  143.6 1.9 %collective-permute-start.2 = (bf16[16,112,256]{2,1,0:T(8,128)(2,1)S(1)}, bf16[16,112,256]{2,1,0:T(8,128)(2,1)S(1)}, u32[]{:S(2)}, u32[]{:S(2)}) collective-permute-start(bf16[16,112,256]{2,1,0:T(8,128)(2,1)S(1)} %bitcast.10), channel_id=1, source_target_pairs={{0,1},{1,0},{2,3},{3,2},{4,5},{5,4},{6,7},{7,6},{8,9},{9,8},{10,11... | collective-permute-start | bytes 2752520 | tf_op jit(solution)/shard_map/ppermute | solution.py:32
  145.5 2.4 %collective-permute-done.2.other_top_hbm = bf16[16,112,256]{2,1,0:T(8,128)(2,1)S(1)} collective-permute-done((bf16[16,112,256]{2,1,0:T(8,128)(2,1)S(1)}, bf16[16,112,256]{2,1,0:T(8,128)(2,1)S(1)}, u32[]{:S(2)}, u32[]{:S(2)}) %collective-permute-start.2) | collective-permute-done | bytes 917536 | tf_op jit(solution)/shard_map/ppermute | solution.py:32
  148.0 0.0 copy-start
  148.0 0.9 copy-done
  148.9 20.1 %all-to-all-done.4.masters_hbm = bf16[16,2,256,128]{3,2,1,0:T(8,128)(2,1)} async-done(((bf16[16,2,256,128]{3,2,1,0:T(8,128)(2,1)}), bf16[16,2,256,128]{3,2,1,0:T(8,128)(2,1)}, u32[]{:S(2)}, u32[]{:S(2)}) %all-to-all-start.4) | async-done | bytes 2097184 | tf_op jit(solution)/shard_map/all_to_all | solution.py:27
  169.0 0.0 collective-permute-done.3.other_rest_hbm
  169.0 0.0 copy-start.1
  169.0 1.2 copy-done.1
  170.2 0.0 copy-start.5
  170.2 0.9 copy-done.5
  171.1 5.4 %finish.1 = (f32[256,128]{1,0:T(8,128)}, f32[256,128]{1,0:T(8,128)}, bf16[16,256,128]{2,1,0:T(8,128)(2,1)}, f32[256,128]{1,0:T(8,128)}, f32[256,128]{1,0:T(8,128)}, /*index=5*/bf16[16,256,128]{2,1,0:T(8,128)(2,1)}) custom-call(bf16[16,2,16,128]{3,2,1,0:T(8,128)(2,1)S(1)} %copy-done.5, bf16[16,112,256]{2,1,0:T(8,128)(2,1)S(1)} %bitcast.11, ...), custom_call_target="tpu_custom_call" | custom-call | tf_op jit(solution)/shard_map/finish/pallas_call | solution.py:264
  (5 shorter events, 0.1 us)
Async XLA Ops:
  0.6 29.5 %all-to-all-start = ((bf16[16,64,128]{2,1,0:T(8,128)(2,1)}), bf16[16,64,128]{2,1,0:T(8,128)(2,1)S(1)}, u32[]{:S(2)}, u32[]{:S(2)}) async-start(bf16[16,64,128]{2,1,0:T(8,128)(2,1)} %bitcast.13), calls=%async_computation | async-start | bytes 524288 | tf_op jit(solution)/shard_map/all_to_all | solution.py:313
  31.3 14.7 %copy-start.10 = (bf16[1024,128]{1,0:T(8,128)(2,1)S(1)}, bf16[1024,128]{1,0:T(8,128)(2,1)}, u32[]{:S(2)}) copy-start(bf16[1024,128]{1,0:T(8,128)(2,1)} %param.13) | copy-start | bytes 786436
  31.3 14.7 %copy-start.11 = (bf16[1024,128]{1,0:T(8,128)(2,1)S(1)}, bf16[1024,128]{1,0:T(8,128)(2,1)}, u32[]{:S(2)}) copy-start(bf16[1024,128]{1,0:T(8,128)(2,1)} %param.12) | copy-start | bytes 786436
  31.3 39.0 %all-to-all-start.1 = ((bf16[16,144,256]{2,1,0:T(8,128)(2,1)}), bf16[16,144,256]{2,1,0:T(8,128)(2,1)S(1)}, u32[]{:S(2)}, u32[]{:S(2)}) async-start(bf16[16,144,256]{2,1,0:T(8,128)(2,1)} %broadcast_in_dim.4), calls=%async_computation.1 | async-start | bytes 2359296 | tf_op jit(solution)/shard_map/all_to_all | solution.py:27
  38.2 32.1 %collective-permute-start = (bf16[16,64,128]{2,1,0:T(8,128)(2,1)S(1)}, bf16[16,64,128]{2,1,0:T(8,128)(2,1)S(1)}, u32[]{:S(2)}, u32[]{:S(2)}) collective-permute-start(bf16[16,64,128]{2,1,0:T(8,128)(2,1)S(1)} %all-to-all-done.own_ref), channel_id=1, source_target_pairs={{0,1},{1,0},{2,3},{3,2},{4,5},{5,4},{6,7},{7,6},{8,9},{9,8},{10,11... | collective-permute-start | bytes 786440 | tf_op jit(solution)/shard_map/ppermute | solution.py:32
  46.0 53.4 %collective-permute-start.1 = (bf16[1024,128]{1,0:T(8,128)(2,1)S(1)}, bf16[1024,128]{1,0:T(8,128)(2,1)S(1)}, u32[]{:S(2)}, u32[]{:S(2)}) collective-permute-start(bf16[1024,128]{1,0:T(8,128)(2,1)S(1)} %get-tuple-element.32), channel_id=1, source_target_pairs={{0,1},{1,0},{2,3},{3,2},{4,5},{5,4},{6,7},{7,6},{8,9},{9,8},{10,11... | collective-permute-start | bytes 786440 | tf_op jit(solution)/shard_map/ppermute | solution.py:32
  71.4 51.4 %copy-start.6 = (f32[16,128]{1,0:T(8,128)S(1)}, f32[16,128]{1,0:T(8,128)}, u32[]{:S(2)}) copy-start(f32[16,128]{1,0:T(8,128)} %query_first_hbm.1) | copy-start | bytes 24580
  71.4 51.4 %copy-start.7 = (f32[16,128]{1,0:T(8,128)S(1)}, f32[16,128]{1,0:T(8,128)}, u32[]{:S(2)}) copy-start(f32[16,128]{1,0:T(8,128)} %query_second_hbm.1) | copy-start | bytes 24580
  71.4 51.4 %copy-start.8 = (f32[16,128]{1,0:T(8,128)S(1)}, f32[16,128]{1,0:T(8,128)}, u32[]{:S(2)}) copy-start(f32[16,128]{1,0:T(8,128)} %key_first_hbm.1) | copy-start | bytes 24580
  71.4 51.4 %copy-start.9 = (f32[16,128]{1,0:T(8,128)S(1)}, f32[16,128]{1,0:T(8,128)}, u32[]{:S(2)}) copy-start(f32[16,128]{1,0:T(8,128)} %key_second_hbm.1) | copy-start | bytes 24580
  71.4 55.7 %copy-start.2 = (f32[256,128]{1,0:T(8,128)S(1)}, f32[256,128]{1,0:T(8,128)}, u32[]{:S(2)}) copy-start(f32[256,128]{1,0:T(8,128)} %key_master_ref.1) | copy-start | bytes 393220
  71.4 55.7 %copy-start.3 = (f32[256,128]{1,0:T(8,128)S(1)}, f32[256,128]{1,0:T(8,128)}, u32[]{:S(2)}) copy-start(f32[256,128]{1,0:T(8,128)} %query_master_ref.1) | copy-start | bytes 393220
  123.6 10.3 %all-to-all-start.3 = ((bf16[16,2,16,128]{3,2,1,0:T(8,128)(2,1)}), bf16[16,2,16,128]{3,2,1,0:T(8,128)(2,1)S(1)}, u32[]{:S(2)}, u32[]{:S(2)}) async-start(bf16[16,2,16,128]{3,2,1,0:T(8,128)(2,1)} %get-tuple-element.21), calls=%async_computation.3 | async-start | bytes 262144 | tf_op jit(solution)/shard_map/all_to_all | solution.py:329
  133.9 1.8 %copy-start.4 = (bf16[16,2,16,128]{3,2,1,0:T(8,128)(2,1)}, bf16[16,2,16,128]{3,2,1,0:T(8,128)(2,1)S(1)}, u32[]{:S(2)}) copy-start(bf16[16,2,16,128]{3,2,1,0:T(8,128)(2,1)S(1)} %all-to-all-done.3.ratio_ref) | copy-start | bytes 393220
  135.7 33.3 %all-to-all-start.4 = ((bf16[16,2,256,128]{3,2,1,0:T(8,128)(2,1)}), bf16[16,2,256,128]{3,2,1,0:T(8,128)(2,1)}, u32[]{:S(2)}, u32[]{:S(2)}) async-start(bf16[16,2,256,128]{3,2,1,0:T(8,128)(2,1)} %broadcast_in_dim.5), calls=%async_computation.4 | async-start | bytes 4194304 | tf_op jit(solution)/shard_map/all_to_all | solution.py:27
  140.1 28.9 %collective-permute-start.3 = (bf16[16,144,256]{2,1,0:T(8,128)(2,1)S(1)}, bf16[16,144,256]{2,1,0:T(8,128)(2,1)S(1)}, u32[]{:S(2)}, u32[]{:S(2)}) collective-permute-start(bf16[16,144,256]{2,1,0:T(8,128)(2,1)S(1)} %all-to-all-done.1.rest_ref.own_rest_ref), channel_id=1, source_target_pairs={{0,1},{1,0},{2,3},{3,2},{4,5},{5,4},{6,7},{7,6},{8,9},{9,8},{10,11... | collective-permute-start | bytes 3538952 | tf_op jit(solution)/shard_map/ppermute | solution.py:32
  143.6 4.4 %collective-permute-start.2 = (bf16[16,112,256]{2,1,0:T(8,128)(2,1)S(1)}, bf16[16,112,256]{2,1,0:T(8,128)(2,1)S(1)}, u32[]{:S(2)}, u32[]{:S(2)}) collective-permute-start(bf16[16,112,256]{2,1,0:T(8,128)(2,1)S(1)} %bitcast.10), channel_id=1, source_target_pairs={{0,1},{1,0},{2,3},{3,2},{4,5},{5,4},{6,7},{7,6},{8,9},{9,8},{10,11... | collective-permute-start | bytes 2752520 | tf_op jit(solution)/shard_map/ppermute | solution.py:32
  148.0 0.9 copy-start
  169.0 1.2 copy-start.1
  170.2 0.9 copy-start.5

commit v7 on v6

--- a/solution.py
+++ b/solution.py
@@ -135,11 +135,11 @@
 
 
 def finish_kernel(
-    ratio_ref,
+    ratio_hbm,
     own_top_ref,
     own_rest_ref,
     other_top_hbm,
-    other_rest_hbm,
+    other_rest_ref,
     masters_hbm,
     query_master_ref,
     key_master_ref,
@@ -149,8 +149,8 @@
     key_step_hbm,
     key_weight_hbm,
     key_copy_hbm,
+    ratio_ref,
     other_top_ref,
-    other_rest_ref,
     masters_ref,
     update_top_ref,
     update_rest_ref,
@@ -167,10 +167,15 @@
     ranks = rows * count
     top, rest = own_top_ref.shape[1], own_rest_ref.shape[1]
     tops, rests = pl.ds(0, top), pl.ds(top, rest)
+    parts = rows // GROUP
+    spans = [pl.ds(part * GROUP, GROUP) for part in range(parts)]
     incoming = [
-        pltpu.make_async_copy(other_top_hbm, other_top_ref, arrived.at[0]),
-        pltpu.make_async_copy(other_rest_hbm, other_rest_ref, arrived.at[1]),
-        pltpu.make_async_copy(masters_hbm, masters_ref, arrived.at[2]),
+        pltpu.make_async_copy(ratio_hbm, ratio_ref, arrived.at[0]),
+        pltpu.make_async_copy(other_top_hbm, other_top_ref, arrived.at[1]),
+    ]
+    incoming += [
+        pltpu.make_async_copy(masters_hbm.at[span], masters_ref.at[span], arrived.at[2 + part])
+        for part, span in enumerate(spans)
     ]
     copy_hbms = (query_copy_hbm, key_copy_hbm)
 
@@ -225,20 +230,20 @@
         for n in range(2):
             pl.when(k == n)(leaving(n, part).start)
 
-    parts = rows // GROUP
     mine, theirs = core, 1 - core
+    incoming[0].wait()
     ratio = ratio_ref[:, mine].reshape(ranks, width)
     total = jnp.zeros((8, width), F32)
     for part in range(parts):
         total = products(own_top_ref, own_rest_ref, mine, ratio, part, total)
     scaled(mine, total)
     own(mine)
-    for copy in incoming:
-        copy.wait()
+    incoming[1].wait()
     ratio = ratio_ref[:, theirs].reshape(ranks, width)
     total = jnp.zeros((8, width), F32)
     for part in range(parts):
         total = products(other_top_ref, other_rest_ref, theirs, ratio, part, total)
+        incoming[2 + part].wait()
         copied(mine, part)
         sent(mine, part)
     scaled(theirs, total)
@@ -264,11 +269,11 @@
     return pl.pallas_call(
         finish_kernel,
         out_shape=(mine, mine, copied) * 2,
-        in_specs=[vmem, vmem, vmem, anywhere, anywhere, anywhere, vmem, vmem],
+        in_specs=[anywhere, vmem, vmem, anywhere, vmem, anywhere, vmem, vmem],
         out_specs=(anywhere, anywhere, anywhere) * 2,
         scratch_shapes=[
+            pltpu.VMEM(ratio.shape, BF),
             pltpu.VMEM(other_top.shape, BF),
-            pltpu.VMEM(other_rest.shape, BF),
             pltpu.VMEM(masters.shape, BF),
             pltpu.VMEM((2, rows, top, width), F32),
             pltpu.VMEM((2, rows, rest, width), F32),
@@ -276,7 +281,7 @@
             pltpu.VMEM((2, own_rows, width), F32),
             pltpu.VMEM((2, own_rows, width), F32),
             pltpu.VMEM((2, 8, width), F32),
-            pltpu.SemaphoreType.DMA((3,)),
+            pltpu.SemaphoreType.DMA((2 + rows // GROUP,)),
             pltpu.SemaphoreType.DMA((2, rows // GROUP)),
             pltpu.SemaphoreType.DMA((2, 2)),
         ],
@@ -285,7 +290,7 @@
     )(ratio, own_top, own_rest, other_top, other_rest, masters, query_master, key_master)
 
 
-TOP = 112
+TOP = 120
 
 
 def body(

time: 177 us -> 175 us (0.989)
  no operation moved by 1% of the time
where the time goes in v7:
time: 175 us
  blocking collectives  72.8 us (42%)
  starting transfers between devices  45.6 us (26%)
  waiting for transfers between devices  42.1 us (24%)
  Pallas kernels  6.27 us (4%)
  local copies, waits for them, and re-layouts  5.96 us (3%)
    all_gather x1, blocking collectives, body(): low = lax.all_gather(low, 'z', axis=0, tiled=True)  27.3 us
    all_to_all x1, blocking collectives, body(): partial = lax.all_to_all(partial, (*FS, 'c'), 0, 0, tiled=True)  23 us
    all_gather x1, blocking collectives, body(): lax.all_gather(own_basis[:TOP], FS, axis=0, tiled=True)  22.4 us
    all_to_all x2, waiting for transfers between devices, sent_to_all(): lax.all_to_all(jnp.broadcast_to(x[None], (count, *x.shape)), axis, 0, 0,...  20 us
    all_to_all x1, starting transfers between devices, body(): lax.all_to_all(saved_input.reshape(depth, share, width), 'z', 0, 0, tiled...  15.7 us
    ppermute x4, starting transfers between devices, swapped(): return lax.ppermute(x, axis, [(i, i ^ 1) for i in range(count)])  15.1 us
    all_to_all x1, waiting for transfers between devices, body(): lax.all_to_all(saved_input.reshape(depth, share, width), 'z', 0, 0, tiled...  12.8 us
    all_to_all x2, starting transfers between devices, sent_to_all(): lax.all_to_all(jnp.broadcast_to(x[None], (count, *x.shape)), axis, 0, 0,...  11.3 us
  transfers between devices with their start and end apart: 8, of which 4 were waited for; matrix products, arithmetic and copies ran while one was open for 1% of the time, Pallas kernels for 1%

profile of v7, /device:TPU:1, one launch (start us, length us, event | category | flops | bytes accessed | tf_op | source)
XLA Modules:
  0.0 174.7 jit_solution(14418986001115653904)
XLA Ops:
  0.6 15.7 %all-to-all-start = ((bf16[16,64,128]{2,1,0:T(8,128)(2,1)}), bf16[16,64,128]{2,1,0:T(8,128)(2,1)S(1)}, u32[]{:S(2)}, u32[]{:S(2)}) async-start(bf16[16,64,128]{2,1,0:T(8,128)(2,1)} %bitcast.13), calls=%async_computation | async-start | bytes 524288 | tf_op jit(solution)/shard_map/all_to_all | solution.py:318
  16.4 0.9 broadcast_select_fusion.2
  17.4 12.8 %all-to-all-done.own_ref = bf16[16,64,128]{2,1,0:T(8,128)(2,1)S(1)} async-done(((bf16[16,64,128]{2,1,0:T(8,128)(2,1)}), bf16[16,64,128]{2,1,0:T(8,128)(2,1)S(1)}, u32[]{:S(2)}, u32[]{:S(2)}) %all-to-all-start) | async-done | bytes 262176 | tf_op jit(solution)/shard_map/all_to_all | solution.py:318
  30.2 1.1 broadcast_in_dim.4
  31.3 0.0 copy-start.10
  31.3 0.0 copy-start.11
  31.3 6.9 %all-to-all-start.1 = ((bf16[16,136,256]{2,1,0:T(8,128)(2,1)}), bf16[16,136,256]{2,1,0:T(8,128)(2,1)S(1)}, u32[]{:S(2)}, u32[]{:S(2)}) async-start(bf16[16,136,256]{2,1,0:T(8,128)(2,1)} %broadcast_in_dim.4), calls=%async_computation.1 | async-start | bytes 2228224 | tf_op jit(solution)/shard_map/all_to_all | solution.py:27
  38.1 7.8 %collective-permute-start = (bf16[16,64,128]{2,1,0:T(8,128)(2,1)S(1)}, bf16[16,64,128]{2,1,0:T(8,128)(2,1)S(1)}, u32[]{:S(2)}, u32[]{:S(2)}) collective-permute-start(bf16[16,64,128]{2,1,0:T(8,128)(2,1)S(1)} %all-to-all-done.own_ref), channel_id=1, source_target_pairs={{0,1},{1,0},{2,3},{3,2},{4,5},{5,4},{6,7},{7,6},{8,9},{9,8},{10,11... | collective-permute-start | bytes 786440 | tf_op jit(solution)/shard_map/ppermute | solution.py:32
  45.9 0.0 copy-done.10
  45.9 0.0 copy-done.11
  46.0 1.9 %collective-permute-start.1 = (bf16[1024,128]{1,0:T(8,128)(2,1)S(1)}, bf16[1024,128]{1,0:T(8,128)(2,1)S(1)}, u32[]{:S(2)}, u32[]{:S(2)}) collective-permute-start(bf16[1024,128]{1,0:T(8,128)(2,1)S(1)} %get-tuple-element.32), channel_id=1, source_target_pairs={{0,1},{1,0},{2,3},{3,2},{4,5},{5,4},{6,7},{7,6},{8,9},{9,8},{10,11... | collective-permute-start | bytes 786440 | tf_op jit(solution)/shard_map/ppermute | solution.py:32
  47.9 22.4 %all_gather.6 = bf16[1920,256]{1,0:T(8,128)(2,1)S(1)} all-gather(bf16[120,256]{1,0:T(8,128)(2,1)S(1)} %slice.8), channel_id=1, replica_groups=mesh['y'=4,'x'=4,'z'=16,'c'=2] {'y','x'}, dimensions={0}, use_global_device_ids=true | all-gather | bytes 1044480 | tf_op jit(solution)/shard_map/all_gather | solution.py:320
  70.3 0.0 all-to-all-done.1.rest_ref.own_rest_ref
  70.3 0.0 collective-permute-done.other_ref
  70.3 1.0 product.1
  71.4 0.0 copy-start.6
  71.4 0.0 copy-start.7
  71.4 0.0 copy-start.8
  71.4 0.0 copy-start.9
  71.4 0.0 copy-start.2
  71.5 0.0 copy-start.3
  71.5 27.3 %all_gather.7.low_ref = bf16[1024,256]{1,0:T(8,128)(2,1)S(1)} all-gather(bf16[64,256]{1,0:T(8,128)(2,1)S(1)} %product.1), channel_id=1, replica_groups=mesh['y'=4,'x'=4,'z'=16,'c'=2] {'z'}, dimensions={0}, use_global_device_ids=true | all-gather | bytes 557056 | tf_op jit(solution)/shard_map/all_gather | solution.py:327
  98.8 0.0 collective-permute-done.1.other_ref
  98.8 0.3 partials.1
  99.2 23.0 %all_to_all.25.parts_ref = bf16[32,16,128]{2,1,0:T(8,128)(2,1)S(1)} all-to-all(bf16[32,16,128]{2,1,0:T(8,128)(2,1)S(1)} %bitcast.12), channel_id=1, replica_groups=mesh['y'=4,'x'=4,'z'=16,'c'=2] {'y','x','c'}, dimensions={0} | all-to-all | bytes 262144 | tf_op jit(solution)/shard_map/all_to_all | solution.py:332
  122.2 0.0 copy-done.6
  122.2 0.0 copy-done.7
  122.2 0.0 copy-done.8
  122.2 0.0 copy-done.9
  122.2 0.8 moments.1
  123.0 3.5 %all-to-all-start.3 = ((bf16[16,2,16,128]{3,2,1,0:T(8,128)(2,1)}), bf16[16,2,16,128]{3,2,1,0:T(8,128)(2,1)S(1)}, u32[]{:S(2)}, u32[]{:S(2)}) async-start(bf16[16,2,16,128]{3,2,1,0:T(8,128)(2,1)} %get-tuple-element.21), calls=%async_computation.3 | async-start | bytes 262144 | tf_op jit(solution)/shard_map/all_to_all | solution.py:334
  126.5 0.0 copy-done.2
  126.6 0.0 copy-done.3
  126.6 6.7 %all-to-all-done.3.ratio_hbm = bf16[16,2,16,128]{3,2,1,0:T(8,128)(2,1)S(1)} async-done(((bf16[16,2,16,128]{3,2,1,0:T(8,128)(2,1)}), bf16[16,2,16,128]{3,2,1,0:T(8,128)(2,1)S(1)}, u32[]{:S(2)}, u32[]{:S(2)}) %all-to-all-start.3) | async-done | bytes 131104 | tf_op jit(solution)/shard_map/all_to_all | solution.py:334
  133.3 0.0 copy-start.4
  133.3 1.8 %broadcast_in_dim.5 = bf16[16,2,256,128]{3,2,1,0:T(8,128)(2,1)} broadcast(bf16[2,256,128]{2,1,0:T(8,128)(2,1)S(1)} %pad_maximum_fusion), dimensions={1,2,3} | broadcast | bytes 2228224 | tf_op jit(solution)/shard_map/broadcast_in_dim | solution.py:27
  135.1 0.0 copy-done.4
  135.1 4.4 %all-to-all-start.4 = ((bf16[16,2,256,128]{3,2,1,0:T(8,128)(2,1)}), bf16[16,2,256,128]{3,2,1,0:T(8,128)(2,1)}, u32[]{:S(2)}, u32[]{:S(2)}) async-start(bf16[16,2,256,128]{3,2,1,0:T(8,128)(2,1)} %broadcast_in_dim.5), calls=%async_computation.4 | async-start | bytes 4194304 | tf_op jit(solution)/shard_map/all_to_all | solution.py:27
  139.6 3.5 %collective-permute-start.3 = (bf16[16,136,256]{2,1,0:T(8,128)(2,1)S(1)}, bf16[16,136,256]{2,1,0:T(8,128)(2,1)S(1)}, u32[]{:S(2)}, u32[]{:S(2)}) collective-permute-start(bf16[16,136,256]{2,1,0:T(8,128)(2,1)S(1)} %all-to-all-done.1.rest_ref.own_rest_ref), channel_id=1, source_target_pairs={{0,1},{1,0},{2,3},{3,2},{4,5},{5,4},{6,7},{7,6},{8,9},{9,8},{10,11... | collective-permute-start | bytes 3342344 | tf_op jit(solution)/shard_map/ppermute | solution.py:32
  143.0 1.9 %collective-permute-start.2 = (bf16[16,120,256]{2,1,0:T(8,128)(2,1)S(1)}, bf16[16,120,256]{2,1,0:T(8,128)(2,1)S(1)}, u32[]{:S(2)}, u32[]{:S(2)}) collective-permute-start(bf16[16,120,256]{2,1,0:T(8,128)(2,1)S(1)} %bitcast.10), channel_id=1, source_target_pairs={{0,1},{1,0},{2,3},{3,2},{4,5},{5,4},{6,7},{7,6},{8,9},{9,8},{10,11... | collective-permute-start | bytes 2949128 | tf_op jit(solution)/shard_map/ppermute | solution.py:32
  145.0 2.5 %collective-permute-done.2.other_top_hbm = bf16[16,120,256]{2,1,0:T(8,128)(2,1)S(1)} collective-permute-done((bf16[16,120,256]{2,1,0:T(8,128)(2,1)S(1)}, bf16[16,120,256]{2,1,0:T(8,128)(2,1)S(1)}, u32[]{:S(2)}, u32[]{:S(2)}) %collective-permute-start.2) | collective-permute-done | bytes 983072 | tf_op jit(solution)/shard_map/ppermute | solution.py:32
  147.5 0.0 copy-start
  147.5 0.9 copy-done
  148.4 20.0 %all-to-all-done.4.masters_hbm = bf16[16,2,256,128]{3,2,1,0:T(8,128)(2,1)} async-done(((bf16[16,2,256,128]{3,2,1,0:T(8,128)(2,1)}), bf16[16,2,256,128]{3,2,1,0:T(8,128)(2,1)}, u32[]{:S(2)}, u32[]{:S(2)}) %all-to-all-start.4) | async-done | bytes 2097184 | tf_op jit(solution)/shard_map/all_to_all | solution.py:27
  168.5 0.0 collective-permute-done.3.other_rest_ref
  168.5 0.0 copy-start.1
  168.5 1.2 copy-done.1
  169.7 0.0 copy-start.5
  169.7 0.9 copy-done.5
  170.6 4.1 %finish.1 = (f32[256,128]{1,0:T(8,128)}, f32[256,128]{1,0:T(8,128)}, bf16[16,256,128]{2,1,0:T(8,128)(2,1)}, f32[256,128]{1,0:T(8,128)}, f32[256,128]{1,0:T(8,128)}, /*index=5*/bf16[16,256,128]{2,1,0:T(8,128)(2,1)}) custom-call(bf16[16,2,16,128]{3,2,1,0:T(8,128)(2,1)S(1)} %copy-done.5, bf16[16,120,256]{2,1,0:T(8,128)(2,1)S(1)} %bitcast.11, ...), custom_call_target="tpu_custom_call" | custom-call | tf_op jit(solution)/shard_map/finish/pallas_call | solution.py:269
  (5 shorter events, 0.1 us)
Async XLA Ops:
  0.6 29.5 %all-to-all-start = ((bf16[16,64,128]{2,1,0:T(8,128)(2,1)}), bf16[16,64,128]{2,1,0:T(8,128)(2,1)S(1)}, u32[]{:S(2)}, u32[]{:S(2)}) async-start(bf16[16,64,128]{2,1,0:T(8,128)(2,1)} %bitcast.13), calls=%async_computation | async-start | bytes 524288 | tf_op jit(solution)/shard_map/all_to_all | solution.py:318
  31.3 14.7 %copy-start.10 = (bf16[1024,128]{1,0:T(8,128)(2,1)S(1)}, bf16[1024,128]{1,0:T(8,128)(2,1)}, u32[]{:S(2)}) copy-start(bf16[1024,128]{1,0:T(8,128)(2,1)} %param.13) | copy-start | bytes 786436
  31.3 14.7 %copy-start.11 = (bf16[1024,128]{1,0:T(8,128)(2,1)S(1)}, bf16[1024,128]{1,0:T(8,128)(2,1)}, u32[]{:S(2)}) copy-start(bf16[1024,128]{1,0:T(8,128)(2,1)} %param.12) | copy-start | bytes 786436
  31.3 39.1 %all-to-all-start.1 = ((bf16[16,136,256]{2,1,0:T(8,128)(2,1)}), bf16[16,136,256]{2,1,0:T(8,128)(2,1)S(1)}, u32[]{:S(2)}, u32[]{:S(2)}) async-start(bf16[16,136,256]{2,1,0:T(8,128)(2,1)} %broadcast_in_dim.4), calls=%async_computation.1 | async-start | bytes 2228224 | tf_op jit(solution)/shard_map/all_to_all | solution.py:27
  38.1 32.2 %collective-permute-start = (bf16[16,64,128]{2,1,0:T(8,128)(2,1)S(1)}, bf16[16,64,128]{2,1,0:T(8,128)(2,1)S(1)}, u32[]{:S(2)}, u32[]{:S(2)}) collective-permute-start(bf16[16,64,128]{2,1,0:T(8,128)(2,1)S(1)} %all-to-all-done.own_ref), channel_id=1, source_target_pairs={{0,1},{1,0},{2,3},{3,2},{4,5},{5,4},{6,7},{7,6},{8,9},{9,8},{10,11... | collective-permute-start | bytes 786440 | tf_op jit(solution)/shard_map/ppermute | solution.py:32
  46.0 52.8 %collective-permute-start.1 = (bf16[1024,128]{1,0:T(8,128)(2,1)S(1)}, bf16[1024,128]{1,0:T(8,128)(2,1)S(1)}, u32[]{:S(2)}, u32[]{:S(2)}) collective-permute-start(bf16[1024,128]{1,0:T(8,128)(2,1)S(1)} %get-tuple-element.32), channel_id=1, source_target_pairs={{0,1},{1,0},{2,3},{3,2},{4,5},{5,4},{6,7},{7,6},{8,9},{9,8},{10,11... | collective-permute-start | bytes 786440 | tf_op jit(solution)/shard_map/ppermute | solution.py:32
  71.4 50.8 %copy-start.6 = (f32[16,128]{1,0:T(8,128)S(1)}, f32[16,128]{1,0:T(8,128)}, u32[]{:S(2)}) copy-start(f32[16,128]{1,0:T(8,128)} %query_first_hbm.1) | copy-start | bytes 24580
  71.4 50.8 %copy-start.7 = (f32[16,128]{1,0:T(8,128)S(1)}, f32[16,128]{1,0:T(8,128)}, u32[]{:S(2)}) copy-start(f32[16,128]{1,0:T(8,128)} %query_second_hbm.1) | copy-start | bytes 24580
  71.4 50.8 %copy-start.8 = (f32[16,128]{1,0:T(8,128)S(1)}, f32[16,128]{1,0:T(8,128)}, u32[]{:S(2)}) copy-start(f32[16,128]{1,0:T(8,128)} %key_first_hbm.1) | copy-start | bytes 24580
  71.4 50.8 %copy-start.9 = (f32[16,128]{1,0:T(8,128)S(1)}, f32[16,128]{1,0:T(8,128)}, u32[]{:S(2)}) copy-start(f32[16,128]{1,0:T(8,128)} %key_second_hbm.1) | copy-start | bytes 24580
  71.4 55.1 %copy-start.2 = (f32[256,128]{1,0:T(8,128)S(1)}, f32[256,128]{1,0:T(8,128)}, u32[]{:S(2)}) copy-start(f32[256,128]{1,0:T(8,128)} %key_master_ref.1) | copy-start | bytes 393220
  71.5 55.1 %copy-start.3 = (f32[256,128]{1,0:T(8,128)S(1)}, f32[256,128]{1,0:T(8,128)}, u32[]{:S(2)}) copy-start(f32[256,128]{1,0:T(8,128)} %query_master_ref.1) | copy-start | bytes 393220
  123.0 10.3 %all-to-all-start.3 = ((bf16[16,2,16,128]{3,2,1,0:T(8,128)(2,1)}), bf16[16,2,16,128]{3,2,1,0:T(8,128)(2,1)S(1)}, u32[]{:S(2)}, u32[]{:S(2)}) async-start(bf16[16,2,16,128]{3,2,1,0:T(8,128)(2,1)} %get-tuple-element.21), calls=%async_computation.3 | async-start | bytes 262144 | tf_op jit(solution)/shard_map/all_to_all | solution.py:334
  133.3 1.8 %copy-start.4 = (bf16[16,2,16,128]{3,2,1,0:T(8,128)(2,1)}, bf16[16,2,16,128]{3,2,1,0:T(8,128)(2,1)S(1)}, u32[]{:S(2)}) copy-start(bf16[16,2,16,128]{3,2,1,0:T(8,128)(2,1)S(1)} %all-to-all-done.3.ratio_hbm) | copy-start | bytes 393220
  135.1 33.3 %all-to-all-start.4 = ((bf16[16,2,256,128]{3,2,1,0:T(8,128)(2,1)}), bf16[16,2,256,128]{3,2,1,0:T(8,128)(2,1)}, u32[]{:S(2)}, u32[]{:S(2)}) async-start(bf16[16,2,256,128]{3,2,1,0:T(8,128)(2,1)} %broadcast_in_dim.5), calls=%async_computation.4 | async-start | bytes 4194304 | tf_op jit(solution)/shard_map/all_to_all | solution.py:27
  139.6 28.9 %collective-permute-start.3 = (bf16[16,136,256]{2,1,0:T(8,128)(2,1)S(1)}, bf16[16,136,256]{2,1,0:T(8,128)(2,1)S(1)}, u32[]{:S(2)}, u32[]{:S(2)}) collective-permute-start(bf16[16,136,256]{2,1,0:T(8,128)(2,1)S(1)} %all-to-all-done.1.rest_ref.own_rest_ref), channel_id=1, source_target_pairs={{0,1},{1,0},{2,3},{3,2},{4,5},{5,4},{6,7},{7,6},{8,9},{9,8},{10,11... | collective-permute-start | bytes 3342344 | tf_op jit(solution)/shard_map/ppermute | solution.py:32
  143.0 4.5 %collective-permute-start.2 = (bf16[16,120,256]{2,1,0:T(8,128)(2,1)S(1)}, bf16[16,120,256]{2,1,0:T(8,128)(2,1)S(1)}, u32[]{:S(2)}, u32[]{:S(2)}) collective-permute-start(bf16[16,120,256]{2,1,0:T(8,128)(2,1)S(1)} %bitcast.10), channel_id=1, source_target_pairs={{0,1},{1,0},{2,3},{3,2},{4,5},{5,4},{6,7},{7,6},{8,9},{9,8},{10,11... | collective-permute-start | bytes 2949128 | tf_op jit(solution)/shard_map/ppermute | solution.py:32
  147.5 0.9 copy-start
  168.5 1.2 copy-start.1
  169.7 0.9 copy-start.5
